TPU v7x, 512 devices: a whole 4x8x8 slice. The times are simulated.
512 devices in a mesh: fs: 64 (over z, y), tp: 8 (over x, core).
Axes of the slice: x: 4, y: 8, z: 8, core: 2. Of those that a mesh axis runs over, the one named last changes fastest.
Arguments:
- prompt: bfloat16 [8192, 2048], P('fs'), may hold values from -6 to 6
- norm_gain: float32 [2048], P('fs'), may hold values from 0.1 to 1.9
- gate_train: float32 [2048, 32768], P('fs', 'tp'), may hold values from -0.125 to 0.125
- up_train: float32 [2048, 32768], P('fs', 'tp'), may hold values from -0.125 to 0.125
- down_train: float32 [2048, 32768], P('fs', 'tp'), may hold values from -0.25 to 0.25
- common_gate_train: float32 [2048, 512], P('fs', 'tp'), may hold values from -0.125 to 0.125
- common_up_train: float32 [2048, 512], P('fs', 'tp'), may hold values from -0.125 to 0.125
- common_down_train: float32 [2048, 512], P('fs', 'tp'), may hold values from -0.25 to 0.25
- route_ids: int32 [8192, 6], P('fs'), may hold values from 0 to 63, all different within a row; in each aligned block of 128 rows (0 to 127, 128 to 255, ...) at most 16 rows name the same one
- route_weights: float32 [8192, 6], P('fs'), may hold values from 0.1 to 1
Outputs:
- mixture: bfloat16 [8192, 2048], P('fs', 'tp')
- gate_serve: bfloat16 [64, 512, 2048], P('fs', 'tp')
- up_serve: bfloat16 [64, 512, 2048], P('fs', 'tp')
- down_serve: bfloat16 [64, 512, 2048], P('fs', 'tp')
- common_gate_serve: bfloat16 [512, 2048], P('tp')
- common_up_serve: bfloat16 [512, 2048], P('tp')
- common_down_serve: bfloat16 [512, 2048], P('tp')
Inputs may be any that keep to these rules, and one draw needn't show every extreme that they name: `route_ids`: each row names 6 different experts. Among the rows of one index of fs no expert is named more than 16 times, and in every draw some expert is named exactly 16 times by the rows of some index.
All inputs are finite; a program needn't handle non-finite values.
Results may differ from a plain program's by a relative error of at most 0.011.
Values may be sent and summed in bfloat16 or wider, within the bound.
No kernel may reach another device: no remote copies, remote signals or barrier semaphores. Data moves between devices by JAX's collectives and lax.ppermute only.
A program may use at most 64 MiB of HBM per device.

v0:
```python
import jax
import jax.numpy as jnp
from jax import lax
from jax.experimental import pallas as pl
from jax.experimental.pallas import tpu as pltpu
from jax.sharding import PartitionSpec as P


E = 64
CAP = 16
TOP_K = 6
TOK = 128
D = 2048
N_FS = 64
N_TP = 8
U = 64
W32 = D // N_FS
COLS = D // N_TP
ROWS = E * CAP
LANES = 128
epsilon = 1e-06

f32 = jnp.float32
bf16 = jnp.bfloat16
VM = pl.BlockSpec(memory_space=pltpu.VMEM)
SM = pl.BlockSpec(memory_space=pltpu.SMEM)


def iota(shape, dim):
    return lax.broadcasted_iota(jnp.int32, shape, dim)


def half_roll(x):
    return pltpu.roll(x, 64, 1)


def call(body, outs, n_in, smem=0, scratch=(), far=(), keep=True):
    flat, tree = jax.tree.flatten(outs)
    kept = [pltpu.VMEM(o.shape, o.dtype) if keep is True or i in keep else o for i, o in enumerate(flat)]
    fn = pl.pallas_call(
        body,
        out_shape=jax.tree.unflatten(tree, kept),
        in_specs=[SM] * smem + [VM] * (n_in - smem),
        out_specs=jax.tree.map(lambda _: VM, outs),
        scratch_shapes=list(scratch),
        compiler_params=pltpu.CompilerParams(vmem_limit_bytes=16 * 2**20),
    )

    def run(*args):
        placed = [
            a if i < smem or i in far else pltpu.with_memory_space_constraint(a, pltpu.VMEM)
            for i, a in enumerate(args)
        ]
        return fn(*placed)

    return run


def dot(a, b):
    return jnp.dot(a, b, preferred_element_type=f32)


def dot_nt(a, b):
    return lax.dot_general(a, b, (((1,), (1,)), ((), ())), preferred_element_type=f32)


def gain_column(gain_ref):
    n = gain_ref.shape[1]
    eye = iota((n, n), 0) == iota((n, n), 1)
    spread = jnp.where(eye, jnp.broadcast_to(gain_ref[...], (n, n)), 0.0)
    return jnp.sum(spread, axis=1, keepdims=True)


def dispatch_body(m_ref, prompt_ref, ids_ref, gain_ref, cg_ref, cu_ref, cd_ref, send_ref, normed_ref, pos_ref):
    m = m_ref[0]
    values = prompt_ref[...].astype(f32)
    scale = lax.rsqrt(jnp.mean(values * values, axis=1, keepdims=True) + epsilon)
    normed_ref[...] = (values * scale).astype(bf16)
    experts = iota((E, TOK), 0)
    named = jnp.zeros((E, TOK), f32)
    for k in range(TOP_K):
        named = jnp.where(ids_ref[k : k + 1, :] == experts, 1.0, named)
    earlier = jnp.where(iota((TOK, TOK), 0) < iota((TOK, TOK), 1), 1.0, 0.0).astype(bf16)
    slot = dot(named.astype(bf16), earlier)
    pos = jnp.where(named > 0.0, slot, -1.0)
    pos_ref[...] = pos
    expand = jnp.where((iota((ROWS, E), 0) >> 4) == iota((ROWS, E), 1), 1.0, 0.0).astype(bf16)
    at = dot(expand, pos.astype(bf16))
    pick = jnp.where(at == (iota((ROWS, TOK), 0) & 15).astype(f32), 1.0, 0.0).astype(bf16)
    mine = normed_ref[:, pl.ds(pl.multiple_of(m * COLS, COLS), COLS)]
    rows = dot(pick, mine).astype(bf16)
    send_ref[:, 0:16, :] = rows[:, :LANES].reshape(E, CAP, LANES)
    send_ref[:, 16:32, :] = rows[:, LANES:].reshape(E, CAP, LANES)
    gain = gain_column(gain_ref)
    both = jnp.concatenate([cg_ref[...] * gain, cu_ref[...] * gain], axis=1)
    down = jnp.concatenate([cd_ref[0:16, :], cd_ref[16:32, :]], axis=1)
    piece = jnp.concatenate([both, down], axis=0).astype(bf16)
    send_ref[:, 32:80, :] = jnp.broadcast_to(piece[None], (N_FS, 48, LANES))


def prepare_body(m_ref, gain_ref, g_ref, u_ref, d_ref, *out_refs):
    m = m_ref[0]
    gain = gain_column(gain_ref)
    low = iota((W32, LANES), 1) < 64
    low16 = iota((16, LANES), 1) < 64
    for k in range(N_TP):
        to = m ^ k
        odd = (to & 1) == 1
        for j in range(8):
            at = pl.ds(pl.multiple_of(j * 512 + (to >> 1) * LANES, LANES), LANES)
            g = g_ref[:, at] * gain
            u = u_ref[:, at] * gain
            d = d_ref[:, at]
            g = jnp.where(odd, half_roll(g), g)
            u = jnp.where(odd, u, half_roll(u))
            out_refs[k][j, 0:32, :] = jnp.where(low, g, u).astype(bf16)
            d0, d1 = d[0:16, :], d[16:32, :]
            d0 = jnp.where(odd, half_roll(d0), d0)
            d1 = jnp.where(odd, d1, half_roll(d1))
            out_refs[k][j, 32:48, :] = jnp.where(low16, d0, d1).astype(bf16)


def assemble_body(m_ref, *refs):
    m = m_ref[0]
    out_ref = refs[-1]
    for k in range(N_TP):
        out_ref[pl.ds(pl.multiple_of((m ^ k) * 8, 8), 8)] = refs[k][...]


def silu(v):
    return v / (1.0 + jnp.exp(-v))


def packed_hidden(acc):
    half = acc.shape[0] // 2
    top, bottom = acc[:half], acc[half:]
    first = silu(top) * half_roll(top)
    second = silu(half_roll(bottom)) * bottom
    return jnp.where(iota((half, LANES), 1) < 64, first, second).astype(bf16)


def common_hidden_body(normed_ref, got_ref, out_ref):
    weights = got_ref[:, 32:64, :].reshape(D, LANES)
    out_ref[...] = packed_hidden(dot(normed_ref[...], weights))


def hidden_body(m_ref, own_ref, left_ref, right_ref, far_a_ref, far_b_ref, three_ref, far_ref, w_ref, common_ref, out_ref, acc_ref):
    m = m_ref[0]

    def joined(x):
        n = x.shape[0]
        return jnp.concatenate([x[:, 0:16, :].reshape(n * 16, LANES), x[:, 16:32, :].reshape(n * 16, LANES)], axis=1)

    def weights(q):
        return w_ref[pl.ds(pl.multiple_of((q & 7) * 8, 8), 8), 0:32, :].reshape(COLS, LANES)

    acc_ref[...] = dot(joined(own_ref[...]), weights(m))
    acc_ref[...] += dot(joined(left_ref[...]), weights(m - 2))
    acc_ref[...] += dot(joined(right_ref[...]), weights(m + 2))
    across = weights(m + 4)
    acc_ref[0:512, :] += dot(joined(far_a_ref[...]), across)
    acc_ref[512:1024, :] += dot(joined(far_b_ref[...]), across)
    other = m ^ 1
    acc_ref[...] += dot(joined(three_ref[0]), weights(other))
    acc_ref[...] += dot(joined(three_ref[1]), weights(other - 2))
    acc_ref[...] += dot(joined(three_ref[2]), weights(other + 2))
    acc_ref[...] += dot(joined(far_ref[...]), weights(other + 4))
    out_ref[0:512, :] = packed_hidden(acc_ref[...])
    out_ref[512:576, :] = common_ref[...]


def down_body(m_ref, own_ref, left_ref, right_ref, far_ref, partner_ref, w_ref, out_ref, common_ref):
    m = m_ref[0]
    low = iota((576, LANES), 1) < 64
    low_w = iota((256, LANES), 1) < 64
    tops, bottoms, mats, commons = [], [], [], []
    mine = (own_ref, left_ref, right_ref, far_ref)
    for i, shift in enumerate((0, -2, 2, 4)):
        a = mine[i][...].astype(f32)
        b = partner_ref[i].astype(f32)
        tops.append(jnp.where(low, a, half_roll(b)).astype(bf16))
        bottoms.append(jnp.where(low, half_roll(a), b).astype(bf16))
        q = (m + shift) & 7
        wa = w_ref[q].astype(f32)
        wb = w_ref[q ^ 1].astype(f32)
        first = jnp.where(low_w, wa, half_roll(wb)).astype(bf16)
        second = jnp.where(low_w, half_roll(wa), wb).astype(bf16)
        for base, into in ((0, mats), (128, commons)):
            parts = []
            for f in range(8):
                at = slice(base + 16 * f, base + 16 * f + 16)
                parts += [first[at], second[at]]
            into.append(jnp.concatenate(parts, axis=0))
    top = jnp.concatenate(tops, axis=1)
    bottom = jnp.concatenate(bottoms, axis=1)
    mat = jnp.concatenate(mats, axis=1)
    common = jnp.concatenate(commons, axis=1)
    for i, rows in enumerate((top, bottom)):
        r = dot_nt(rows[:512], mat).astype(bf16)
        at = slice(32 * i, 32 * i + 32)
        out_ref[at, 0:16, :] = r[:, :LANES].reshape(32, 16, LANES)
        out_ref[at, 16:32, :] = r[:, LANES:].reshape(32, 16, LANES)
        common_ref[64 * i : 64 * i + 64, :] = dot_nt(rows[512:576], common)


def mixing_body(pos_ref, ids_ref, weight_ref, hi_ref, lo_ref):
    experts = iota((E, TOK), 0)
    w = jnp.zeros((E, TOK), f32)
    for k in range(TOP_K):
        w = jnp.where(ids_ref[k : k + 1, :] == experts, weight_ref[k : k + 1, :], w)
    pos = jnp.transpose(pos_ref[...]).astype(bf16)
    w = jnp.transpose(w)
    expand = jnp.where(iota((E, ROWS), 0) == (iota((E, ROWS), 1) >> 4), 1.0, 0.0).astype(bf16)
    hit = dot(pos, expand) == (iota((TOK, ROWS), 1) & 15).astype(f32)
    hi = w.astype(bf16)
    lo = (w - hi.astype(f32)).astype(bf16)
    hi_ref[...] = jnp.where(hit, dot(hi, expand), 0.0).astype(bf16)
    lo_ref[...] = jnp.where(hit, dot(lo, expand), 0.0).astype(bf16)


def combine_body(hi_ref, lo_ref, got_ref, common_ref, out_ref):
    hi, lo = hi_ref[...], lo_ref[...]
    for h in range(2):
        rows = got_ref[:, 16 * h : 16 * h + 16, :].reshape(ROWS, LANES)
        at = slice(LANES * h, LANES * h + LANES)
        out_ref[:, at] = (dot(hi, rows) + dot(lo, rows) + common_ref[:, at]).astype(bf16)


def serve_body(base):
    def body(w_ref, g_ref, u_ref, d_ref):
        low = iota((LANES, LANES), 1) < 64
        for i in range(16):
            block = w_ref[4 * i : 4 * i + 4, base : base + 32, :].reshape(LANES, LANES).astype(f32)
            turned = jnp.transpose(block).astype(bf16)
            at = slice(LANES * i, LANES * i + LANES)
            g_ref[:, at] = turned[:64]
            u_ref[:, at] = turned[64:]
        for i in range(8):
            sides = []
            for s in range(2):
                straight, rolled = [], []
                for f in range(4):
                    x = w_ref[8 * i + 4 * s + f, base + 32 : base + 48, :].astype(f32)
                    y = half_roll(x)
                    straight += [x, y]
                    rolled += [y, x]
                sides.append(jnp.concatenate(rolled if s else straight, axis=0))
            turned = jnp.transpose(jnp.where(low, sides[0], sides[1])).astype(bf16)
            at = 256 * i
            d_ref[:, at : at + LANES] = turned[:64]
            d_ref[:, at + LANES : at + 2 * LANES] = turned[64:]

    return body


def shift(x, step):
    return lax.ppermute(x, "tp", [(i, (i + step) % N_TP) for i in range(N_TP)])


def swap(x, k):
    return lax.ppermute(x, "tp", [(i, i ^ k) for i in range(N_TP)])


def shape(*dims, dtype=bf16):
    return jax.ShapeDtypeStruct(dims, dtype)


def local(
    prompt,
    norm_gain,
    gate_train,
    up_train,
    down_train,
    common_gate_train,
    common_up_train,
    common_down_train,
    route_ids,
    route_weights,
):
    m = lax.axis_index("tp").astype(jnp.int32).reshape(1)
    ids = route_ids.T
    route_weights = route_weights.T
    gain = norm_gain.reshape(1, W32)

    send, normed, pos = call(
        dispatch_body, (shape(64, 80, LANES), shape(TOK, D), shape(E, TOK, dtype=f32)), 7, 1, far=range(8), keep=(1, 2)
    )(m, prompt, ids, gain, common_gate_train, common_up_train, common_down_train)
    got = lax.all_to_all(send, "fs", 0, 0, tiled=True)

    pieces = call(prepare_body, tuple(shape(8, 48, LANES) for _ in range(N_TP)), 5, 1, far=range(8))(
        m, gain, gate_train, up_train, down_train
    )
    crossed = [pieces[0]] + [swap(pieces[k], k) for k in range(1, N_TP)]
    spread = call(assemble_body, shape(64, 48, LANES), 9, 1, keep=())(m, *crossed)
    weights = lax.all_to_all(spread, "fs", 0, 0, tiled=True)

    own = got[:, 0:32, :]
    left = shift(own, 2)
    right = shift(own, -2)
    far_a = shift(left[:32], 2)
    far_b = shift(right[32:], -2)
    three = swap(jnp.stack([own, left, right]), 1)
    far = swap(jnp.concatenate([far_a, far_b]), 1)

    common_hidden = call(common_hidden_body, shape(64, LANES), 2)(normed, got)
    mix_hi, mix_lo = call(mixing_body, (shape(TOK, ROWS), shape(TOK, ROWS)), 3, far=(1, 2))(pos, ids, route_weights)

    down_send = jnp.concatenate(
        [weights[:, 32:48, :].reshape(8, 128, LANES), got[:, 64:80, :].reshape(8, 128, LANES)], axis=1
    )
    down_got = lax.all_to_all(down_send, "tp", 0, 0, tiled=True)

    hidden = call(
        hidden_body, shape(576, LANES), 10, 1, [pltpu.VMEM((ROWS, LANES), f32)]
    )(m, own, left, right, far_a, far_b, three, far, weights, common_hidden)
    h_left = shift(hidden, 2)
    h_right = shift(hidden, -2)
    h_far = shift(hidden, 4)
    partner = swap(jnp.stack([hidden, h_left, h_right, h_far]), 1)

    expert_out, common_out = call(
        down_body, (shape(64, 32, LANES), shape(TOK, COLS, dtype=f32)), 7, 1, keep=(1,)
    )(m, hidden, h_left, h_right, h_far, partner, down_got)
    returned = lax.all_to_all(expert_out, "fs", 0, 0, tiled=True)

    serve = tuple(shape(U, D) for _ in range(3))
    gate_serve, up_serve, down_serve = call(serve_body(0), serve, 1, keep=())(weights)
    commons = call(serve_body(32), serve, 1, keep=())(got)

    mixture = call(combine_body, shape(TOK, COLS), 4, keep=())(mix_hi, mix_lo, returned, common_out)
    return (mixture, gate_serve[None], up_serve[None], down_serve[None], *commons)


def solution(mesh):
    in_specs = (
        P("fs", None),
        P("fs"),
        P("fs", "tp"),
        P("fs", "tp"),
        P("fs", "tp"),
        P("fs", "tp"),
        P("fs", "tp"),
        P("fs", "tp"),
        P("fs", None),
        P("fs", None),
    )
    out_specs = (
        P("fs", "tp"),
        P("fs", "tp", None),
        P("fs", "tp", None),
        P("fs", "tp", None),
        P("tp", None),
        P("tp", None),
        P("tp", None),
    )

    return jax.shard_map(local, mesh=mesh, in_specs=in_specs, out_specs=out_specs, check_vma=False)
```

profile of v0, /device:TPU:6, one launch (start us, length us, event | category | flops | bytes accessed | tf_op | source)
XLA Modules:
  0.0 191.3 jit_solution(15672569844569604679)
XLA Ops:
  5.8 52.1 %all_to_all.20.got_ref.w_ref = bf16[64,80,128]{2,1,0:T(8,128)(2,1)S(1)} all-to-all(bf16[64,80,128]{2,1,0:T(8,128)(2,1)S(1)} %get-tuple-element.31), channel_id=1, replica_groups=mesh['fs'=64,'tp'=8] {'fs'}, dimensions={0} | all-to-all | bytes 2621440 | tf_op jit(solution)/shard_map/all_to_all | solution.py:288
  58.1 2.4 %collective-permute-start = (bf16[64,32,128]{2,1,0:T(8,128)(2,1)S(1)}, bf16[64,32,128]{2,1,0:T(8,128)(2,1)S(1)}, u32[]{:S(2)}, u32[]{:S(2)}) collective-permute-start(bf16[64,32,128]{2,1,0:T(8,128)(2,1)S(1)} %get-tuple-element.50.own_ref), channel_id=1, source_target_pairs={{0,2},{1,3},{2,4},{3,5},{4,6},{5,7},{6,0},{7,1},{8,10},{9,11},{10,... | collective-permute-start | bytes 1572872 | tf_op jit(solution)/shard_map/ppermute | solution.py:257
  60.5 3.5 %collective-permute-start.1 = (bf16[64,32,128]{2,1,0:T(8,128)(2,1)S(1)}, bf16[64,32,128]{2,1,0:T(8,128)(2,1)S(1)}, u32[]{:S(2)}, u32[]{:S(2)}) collective-permute-start(bf16[64,32,128]{2,1,0:T(8,128)(2,1)S(1)} %get-tuple-element.50.own_ref), channel_id=1, source_target_pairs={{0,6},{1,7},{2,0},{3,1},{4,2},{5,3},{6,4},{7,5},{8,14},{9,15},{10,... | collective-permute-start | bytes 1572872 | tf_op jit(solution)/shard_map/ppermute | solution.py:257
  64.7 1.9 %collective-permute-start.10 = (bf16[8,48,128]{2,1,0:T(8,128)(2,1)S(1)}, bf16[8,48,128]{2,1,0:T(8,128)(2,1)S(1)}, u32[]{:S(2)}, u32[]{:S(2)}) collective-permute-start(bf16[8,48,128]{2,1,0:T(8,128)(2,1)S(1)} %get-tuple-element.37), channel_id=1, source_target_pairs={{0,5},{1,4},{2,7},{3,6},{4,1},{5,0},{6,3},{7,2},{8,13},{9,12},{10,... | collective-permute-start | bytes 294920 | tf_op jit(solution)/shard_map/ppermute | solution.py:261
  66.7 3.6 %collective-permute-start.11 = (bf16[8,48,128]{2,1,0:T(8,128)(2,1)S(1)}, bf16[8,48,128]{2,1,0:T(8,128)(2,1)S(1)}, u32[]{:S(2)}, u32[]{:S(2)}) collective-permute-start(bf16[8,48,128]{2,1,0:T(8,128)(2,1)S(1)} %get-tuple-element.38), channel_id=1, source_target_pairs={{0,6},{1,7},{2,4},{3,5},{4,2},{5,3},{6,0},{7,1},{8,14},{9,15},{10,... | collective-permute-start | bytes 294920 | tf_op jit(solution)/shard_map/ppermute | solution.py:261
  70.3 4.3 %collective-permute-start.12 = (bf16[8,48,128]{2,1,0:T(8,128)(2,1)S(1)}, bf16[8,48,128]{2,1,0:T(8,128)(2,1)S(1)}, u32[]{:S(2)}, u32[]{:S(2)}) collective-permute-start(bf16[8,48,128]{2,1,0:T(8,128)(2,1)S(1)} %get-tuple-element.39), channel_id=1, source_target_pairs={{0,7},{1,6},{2,5},{3,4},{4,3},{5,2},{6,1},{7,0},{8,15},{9,14},{10,... | collective-permute-start | bytes 294920 | tf_op jit(solution)/shard_map/ppermute | solution.py:261
  74.6 3.5 %collective-permute-start.6 = (bf16[8,48,128]{2,1,0:T(8,128)(2,1)S(1)}, bf16[8,48,128]{2,1,0:T(8,128)(2,1)S(1)}, u32[]{:S(2)}, u32[]{:S(2)}) collective-permute-start(bf16[8,48,128]{2,1,0:T(8,128)(2,1)S(1)} %get-tuple-element.33), channel_id=1, source_target_pairs={{0,1},{1,0},{2,3},{3,2},{4,5},{5,4},{6,7},{7,6},{8,9},{9,8},{10,11... | collective-permute-start | bytes 294920 | tf_op jit(solution)/shard_map/ppermute | solution.py:261
  83.6 3.8 %collective-permute-start.9 = (bf16[8,48,128]{2,1,0:T(8,128)(2,1)S(1)}, bf16[8,48,128]{2,1,0:T(8,128)(2,1)S(1)}, u32[]{:S(2)}, u32[]{:S(2)}) collective-permute-start(bf16[8,48,128]{2,1,0:T(8,128)(2,1)S(1)} %get-tuple-element.36), channel_id=1, source_target_pairs={{0,4},{1,5},{2,6},{3,7},{4,0},{5,1},{6,2},{7,3},{8,12},{9,13},{10,... | collective-permute-start | bytes 294920 | tf_op jit(solution)/shard_map/ppermute | solution.py:261
  88.7 3.1 %collective-permute-start.4 = (bf16[3,64,32,128]{3,2,1,0:T(8,128)(2,1)}, bf16[3,64,32,128]{3,2,1,0:T(8,128)(2,1)}, u32[]{:S(2)}, u32[]{:S(2)}) collective-permute-start(bf16[3,64,32,128]{3,2,1,0:T(8,128)(2,1)} %pad_maximum_fusion), channel_id=1, source_target_pairs={{0,1},{1,0},{2,3},{3,2},{4,5},{5,4},{6,7},{7,6},{8,9},{9,8},{10,11... | collective-permute-start | bytes 4718600 | tf_op jit(solution)/shard_map/ppermute | solution.py:261
  92.8 8.3 %all-to-all-start.1 = ((bf16[64,48,128]{2,1,0:T(8,128)(2,1)}), bf16[64,48,128]{2,1,0:T(8,128)(2,1)S(1)}, u32[]{:S(2)}, u32[]{:S(2)}) async-start(bf16[64,48,128]{2,1,0:T(8,128)(2,1)} %copy-done), calls=%async_computation.1 | async-start | bytes 1572864 | tf_op jit(solution)/shard_map/all_to_all | solution.py:295
  101.1 3.7 %collective-permute-start.2 = (bf16[32,32,128]{2,1,0:T(8,128)(2,1)S(1)}, bf16[32,32,128]{2,1,0:T(8,128)(2,1)S(1)}, u32[]{:S(2)}, u32[]{:S(2)}) collective-permute-start(bf16[32,32,128]{2,1,0:T(8,128)(2,1)S(1)} %slice.21), channel_id=1, source_target_pairs={{0,2},{1,3},{2,4},{3,5},{4,6},{5,7},{6,0},{7,1},{8,10},{9,11},{10,... | collective-permute-start | bytes 786440 | tf_op jit(solution)/shard_map/ppermute | solution.py:257
  104.9 2.2 %collective-permute-start.3 = (bf16[32,32,128]{2,1,0:T(8,128)(2,1)S(1)}, bf16[32,32,128]{2,1,0:T(8,128)(2,1)S(1)}, u32[]{:S(2)}, u32[]{:S(2)}) collective-permute-start(bf16[32,32,128]{2,1,0:T(8,128)(2,1)S(1)} %slice.22), channel_id=1, source_target_pairs={{0,6},{1,7},{2,0},{3,1},{4,2},{5,3},{6,4},{7,5},{8,14},{9,15},{10,... | collective-permute-start | bytes 786440 | tf_op jit(solution)/shard_map/ppermute | solution.py:257
  107.1 4.7 %collective-permute-done.2.far_a_ref = bf16[32,32,128]{2,1,0:T(8,128)(2,1)S(1)} collective-permute-done((bf16[32,32,128]{2,1,0:T(8,128)(2,1)S(1)}, bf16[32,32,128]{2,1,0:T(8,128)(2,1)S(1)}, u32[]{:S(2)}, u32[]{:S(2)}) %collective-permute-start.2) | collective-permute-done | bytes 262176 | tf_op jit(solution)/shard_map/ppermute | solution.py:257
  111.8 4.3 %collective-permute-done.3.far_b_ref = bf16[32,32,128]{2,1,0:T(8,128)(2,1)S(1)} collective-permute-done((bf16[32,32,128]{2,1,0:T(8,128)(2,1)S(1)}, bf16[32,32,128]{2,1,0:T(8,128)(2,1)S(1)}, u32[]{:S(2)}, u32[]{:S(2)}) %collective-permute-start.3) | collective-permute-done | bytes 262176 | tf_op jit(solution)/shard_map/ppermute | solution.py:257
  119.9 6.0 %all-to-all-done.1.w_ref = bf16[64,48,128]{2,1,0:T(8,128)(2,1)S(1)} async-done(((bf16[64,48,128]{2,1,0:T(8,128)(2,1)}), bf16[64,48,128]{2,1,0:T(8,128)(2,1)S(1)}, u32[]{:S(2)}, u32[]{:S(2)}) %all-to-all-start.1) | async-done | bytes 786464 | tf_op jit(solution)/shard_map/all_to_all | solution.py:295
  128.0 2.9 %shard_map.158.own_ref = bf16[576,128]{1,0:T(8,128)(2,1)S(1)} custom-call(s32[1]{0:T(128)} %bitcast.m_ref, bf16[64,32,128]{2,1,0:T(8,128)(2,1)S(1)} %copy-done.2, bf16[64,32,128]{2,1,0:T(8,128)(2,1)S(1)} %collective-permute-done.left_ref, bf16[64,32,128]{2,1,0:T(8,128)(2,1)S(1)} %collective-permute-done.1.right_ref, ...), custom_call_target="tpu_custom_call" | custom-call | tf_op jit(solution)/shard_map/pallas_call | solution.py:54
  130.8 3.5 %collective-permute-start.15 = (bf16[576,128]{1,0:T(8,128)(2,1)S(1)}, bf16[576,128]{1,0:T(8,128)(2,1)S(1)}, u32[]{:S(2)}, u32[]{:S(2)}) collective-permute-start(bf16[576,128]{1,0:T(8,128)(2,1)S(1)} %shard_map.158.own_ref), channel_id=1, source_target_pairs={{0,4},{1,5},{2,6},{3,7},{4,0},{5,1},{6,2},{7,3},{8,12},{9,13},{10,... | collective-permute-start | bytes 442376 | tf_op jit(solution)/shard_map/ppermute | solution.py:257
  134.4 4.0 %collective-permute-start.13 = (bf16[576,128]{1,0:T(8,128)(2,1)S(1)}, bf16[576,128]{1,0:T(8,128)(2,1)S(1)}, u32[]{:S(2)}, u32[]{:S(2)}) collective-permute-start(bf16[576,128]{1,0:T(8,128)(2,1)S(1)} %shard_map.158.own_ref), channel_id=1, source_target_pairs={{0,2},{1,3},{2,4},{3,5},{4,6},{5,7},{6,0},{7,1},{8,10},{9,11},{10,... | collective-permute-start | bytes 442376 | tf_op jit(solution)/shard_map/ppermute | solution.py:257
  138.4 1.9 %collective-permute-start.14 = (bf16[576,128]{1,0:T(8,128)(2,1)S(1)}, bf16[576,128]{1,0:T(8,128)(2,1)S(1)}, u32[]{:S(2)}, u32[]{:S(2)}) collective-permute-start(bf16[576,128]{1,0:T(8,128)(2,1)S(1)} %shard_map.158.own_ref), channel_id=1, source_target_pairs={{0,6},{1,7},{2,0},{3,1},{4,2},{5,3},{6,4},{7,5},{8,14},{9,15},{10,... | collective-permute-start | bytes 442376 | tf_op jit(solution)/shard_map/ppermute | solution.py:257
  141.4 5.3 %collective-permute-done.14.right_ref = bf16[576,128]{1,0:T(8,128)(2,1)S(1)} collective-permute-done((bf16[576,128]{1,0:T(8,128)(2,1)S(1)}, bf16[576,128]{1,0:T(8,128)(2,1)S(1)}, u32[]{:S(2)}, u32[]{:S(2)}) %collective-permute-start.14) | collective-permute-done | bytes 147488 | tf_op jit(solution)/shard_map/ppermute | solution.py:257
  148.8 12.7 %all_to_all.21.w_ref = bf16[8,256,128]{2,1,0:T(8,128)(2,1)S(1)} all-to-all(bf16[8,256,128]{2,1,0:T(8,128)(2,1)S(1)} %pad_maximum_fusion.3), channel_id=1, replica_groups=mesh['fs'=64,'tp'=8] {'tp'}, dimensions={0} | all-to-all | bytes 1048576 | tf_op jit(solution)/shard_map/all_to_all | solution.py:311
  163.2 6.9 %all-to-all-start.3 = ((bf16[64,32,128]{2,1,0:T(8,128)(2,1)}), bf16[64,32,128]{2,1,0:T(8,128)(2,1)}, u32[]{:S(2)}, u32[]{:S(2)}) async-start(bf16[64,32,128]{2,1,0:T(8,128)(2,1)} %get-tuple-element.41), calls=%async_computation.3 | async-start | bytes 1048576 | tf_op jit(solution)/shard_map/all_to_all | solution.py:324
  173.0 16.2 %all-to-all-done.3.got_ref = bf16[64,32,128]{2,1,0:T(8,128)(2,1)} async-done(((bf16[64,32,128]{2,1,0:T(8,128)(2,1)}), bf16[64,32,128]{2,1,0:T(8,128)(2,1)}, u32[]{:S(2)}, u32[]{:S(2)}) %all-to-all-start.3) | async-done | bytes 524320 | tf_op jit(solution)/shard_map/all_to_all | solution.py:324
  189.2 2.1 %shard_map.160 = bf16[128,256]{1,0:T(8,128)(2,1)} custom-call(bf16[128,1024]{1,0:T(8,128)(2,1)S(1)} %get-tuple-element.29.hi_ref, bf16[128,1024]{1,0:T(8,128)(2,1)S(1)} %get-tuple-element.30.lo_ref, bf16[64,32,128]{2,1,0:T(8,128)(2,1)} %all-to-all-done.3.got_ref, f32[128,256]{1,0:T(8,128)S(1)} %get-tuple-element.42.common_ref), custom_call_target="tpu_custom_call" | custom-call | tf_op jit(solution)/shard_map/pallas_call | solution.py:54
  (71 shorter events, 27.3 us)
Async XLA Ops:
  5.8 52.3 %copy-start.5 = (bf16[128,2048]{1,0:T(8,128)(2,1)}, bf16[128,2048]{1,0:T(8,128)(2,1)S(1)}, u32[]{:S(2)}) copy-start(bf16[128,2048]{1,0:T(8,128)(2,1)S(1)} %get-tuple-element.40.normed_ref) | copy-start | bytes 1572868
  5.8 58.2 %copy-start.8 = (f32[32,4096]{1,0:T(8,128)S(1)}, f32[32,4096]{1,0:T(8,128)}, u32[]{:S(2)}) copy-start(f32[32,4096]{1,0:T(8,128)} %g_ref.1) | copy-start | bytes 1572868
  5.8 58.2 %copy-start.9 = (f32[32,4096]{1,0:T(8,128)S(1)}, f32[32,4096]{1,0:T(8,128)}, u32[]{:S(2)}) copy-start(f32[32,4096]{1,0:T(8,128)} %u_ref.1) | copy-start | bytes 1572868
  5.8 58.2 %copy-start.10 = (f32[32,4096]{1,0:T(8,128)S(1)}, f32[32,4096]{1,0:T(8,128)}, u32[]{:S(2)}) copy-start(f32[32,4096]{1,0:T(8,128)} %d_ref.1) | copy-start | bytes 1572868
  58.1 30.6 %copy-start.1 = (bf16[64,32,128]{2,1,0:T(8,128)(2,1)}, bf16[64,32,128]{2,1,0:T(8,128)(2,1)S(1)}, u32[]{:S(2)}) copy-start(bf16[64,32,128]{2,1,0:T(8,128)(2,1)S(1)} %get-tuple-element.50.own_ref) | copy-start | bytes 1572868
  58.1 23.5 %collective-permute-start = (bf16[64,32,128]{2,1,0:T(8,128)(2,1)S(1)}, bf16[64,32,128]{2,1,0:T(8,128)(2,1)S(1)}, u32[]{:S(2)}, u32[]{:S(2)}) collective-permute-start(bf16[64,32,128]{2,1,0:T(8,128)(2,1)S(1)} %get-tuple-element.50.own_ref), channel_id=1, source_target_pairs={{0,2},{1,3},{2,4},{3,5},{4,6},{5,7},{6,0},{7,1},{8,10},{9,11},{10,... | collective-permute-start | bytes 1572872 | tf_op jit(solution)/shard_map/ppermute | solution.py:257
  60.5 23.1 %collective-permute-start.1 = (bf16[64,32,128]{2,1,0:T(8,128)(2,1)S(1)}, bf16[64,32,128]{2,1,0:T(8,128)(2,1)S(1)}, u32[]{:S(2)}, u32[]{:S(2)}) collective-permute-start(bf16[64,32,128]{2,1,0:T(8,128)(2,1)S(1)} %get-tuple-element.50.own_ref), channel_id=1, source_target_pairs={{0,6},{1,7},{2,0},{3,1},{4,2},{5,3},{6,4},{7,5},{8,14},{9,15},{10,... | collective-permute-start | bytes 1572872 | tf_op jit(solution)/shard_map/ppermute | solution.py:257
  64.7 9.8 %collective-permute-start.10 = (bf16[8,48,128]{2,1,0:T(8,128)(2,1)S(1)}, bf16[8,48,128]{2,1,0:T(8,128)(2,1)S(1)}, u32[]{:S(2)}, u32[]{:S(2)}) collective-permute-start(bf16[8,48,128]{2,1,0:T(8,128)(2,1)S(1)} %get-tuple-element.37), channel_id=1, source_target_pairs={{0,5},{1,4},{2,7},{3,6},{4,1},{5,0},{6,3},{7,2},{8,13},{9,12},{10,... | collective-permute-start | bytes 294920 | tf_op jit(solution)/shard_map/ppermute | solution.py:261
  66.7 13.1 %collective-permute-start.11 = (bf16[8,48,128]{2,1,0:T(8,128)(2,1)S(1)}, bf16[8,48,128]{2,1,0:T(8,128)(2,1)S(1)}, u32[]{:S(2)}, u32[]{:S(2)}) collective-permute-start(bf16[8,48,128]{2,1,0:T(8,128)(2,1)S(1)} %get-tuple-element.38), channel_id=1, source_target_pairs={{0,6},{1,7},{2,4},{3,5},{4,2},{5,3},{6,0},{7,1},{8,14},{9,15},{10,... | collective-permute-start | bytes 294920 | tf_op jit(solution)/shard_map/ppermute | solution.py:261
  70.3 18.5 %collective-permute-start.12 = (bf16[8,48,128]{2,1,0:T(8,128)(2,1)S(1)}, bf16[8,48,128]{2,1,0:T(8,128)(2,1)S(1)}, u32[]{:S(2)}, u32[]{:S(2)}) collective-permute-start(bf16[8,48,128]{2,1,0:T(8,128)(2,1)S(1)} %get-tuple-element.39), channel_id=1, source_target_pairs={{0,7},{1,6},{2,5},{3,4},{4,3},{5,2},{6,1},{7,0},{8,15},{9,14},{10,... | collective-permute-start | bytes 294920 | tf_op jit(solution)/shard_map/ppermute | solution.py:261
  74.6 17.2 %collective-permute-start.6 = (bf16[8,48,128]{2,1,0:T(8,128)(2,1)S(1)}, bf16[8,48,128]{2,1,0:T(8,128)(2,1)S(1)}, u32[]{:S(2)}, u32[]{:S(2)}) collective-permute-start(bf16[8,48,128]{2,1,0:T(8,128)(2,1)S(1)} %get-tuple-element.33), channel_id=1, source_target_pairs={{0,1},{1,0},{2,3},{3,2},{4,5},{5,4},{6,7},{7,6},{8,9},{9,8},{10,11... | collective-permute-start | bytes 294920 | tf_op jit(solution)/shard_map/ppermute | solution.py:261
  79.7 12.1 %collective-permute-start.7 = (bf16[8,48,128]{2,1,0:T(8,128)(2,1)S(1)}, bf16[8,48,128]{2,1,0:T(8,128)(2,1)S(1)}, u32[]{:S(2)}, u32[]{:S(2)}) collective-permute-start(bf16[8,48,128]{2,1,0:T(8,128)(2,1)S(1)} %get-tuple-element.34), channel_id=1, source_target_pairs={{0,2},{1,3},{2,0},{3,1},{4,6},{5,7},{6,4},{7,5},{8,10},{9,11},{10,... | collective-permute-start | bytes 294920 | tf_op jit(solution)/shard_map/ppermute | solution.py:261
  81.6 10.2 %collective-permute-start.8 = (bf16[8,48,128]{2,1,0:T(8,128)(2,1)S(1)}, bf16[8,48,128]{2,1,0:T(8,128)(2,1)S(1)}, u32[]{:S(2)}, u32[]{:S(2)}) collective-permute-start(bf16[8,48,128]{2,1,0:T(8,128)(2,1)S(1)} %get-tuple-element.35), channel_id=1, source_target_pairs={{0,3},{1,2},{2,1},{3,0},{4,7},{5,6},{6,5},{7,4},{8,11},{9,10},{10,... | collective-permute-start | bytes 294920 | tf_op jit(solution)/shard_map/ppermute | solution.py:261
  83.6 8.3 %collective-permute-start.9 = (bf16[8,48,128]{2,1,0:T(8,128)(2,1)S(1)}, bf16[8,48,128]{2,1,0:T(8,128)(2,1)S(1)}, u32[]{:S(2)}, u32[]{:S(2)}) collective-permute-start(bf16[8,48,128]{2,1,0:T(8,128)(2,1)S(1)} %get-tuple-element.36), channel_id=1, source_target_pairs={{0,4},{1,5},{2,6},{3,7},{4,0},{5,1},{6,2},{7,3},{8,12},{9,13},{10,... | collective-permute-start | bytes 294920 | tf_op jit(solution)/shard_map/ppermute | solution.py:261
  88.7 37.3 %collective-permute-start.4 = (bf16[3,64,32,128]{3,2,1,0:T(8,128)(2,1)}, bf16[3,64,32,128]{3,2,1,0:T(8,128)(2,1)}, u32[]{:S(2)}, u32[]{:S(2)}) collective-permute-start(bf16[3,64,32,128]{3,2,1,0:T(8,128)(2,1)} %pad_maximum_fusion), channel_id=1, source_target_pairs={{0,1},{1,0},{2,3},{3,2},{4,5},{5,4},{6,7},{7,6},{8,9},{9,8},{10,11... | collective-permute-start | bytes 4718600 | tf_op jit(solution)/shard_map/ppermute | solution.py:261
  92.8 33.2 %all-to-all-start.1 = ((bf16[64,48,128]{2,1,0:T(8,128)(2,1)}), bf16[64,48,128]{2,1,0:T(8,128)(2,1)S(1)}, u32[]{:S(2)}, u32[]{:S(2)}) async-start(bf16[64,48,128]{2,1,0:T(8,128)(2,1)} %copy-done), calls=%async_computation.1 | async-start | bytes 1572864 | tf_op jit(solution)/shard_map/all_to_all | solution.py:295
  101.1 10.7 %collective-permute-start.2 = (bf16[32,32,128]{2,1,0:T(8,128)(2,1)S(1)}, bf16[32,32,128]{2,1,0:T(8,128)(2,1)S(1)}, u32[]{:S(2)}, u32[]{:S(2)}) collective-permute-start(bf16[32,32,128]{2,1,0:T(8,128)(2,1)S(1)} %slice.21), channel_id=1, source_target_pairs={{0,2},{1,3},{2,4},{3,5},{4,6},{5,7},{6,0},{7,1},{8,10},{9,11},{10,... | collective-permute-start | bytes 786440 | tf_op jit(solution)/shard_map/ppermute | solution.py:257
  104.9 11.2 %collective-permute-start.3 = (bf16[32,32,128]{2,1,0:T(8,128)(2,1)S(1)}, bf16[32,32,128]{2,1,0:T(8,128)(2,1)S(1)}, u32[]{:S(2)}, u32[]{:S(2)}) collective-permute-start(bf16[32,32,128]{2,1,0:T(8,128)(2,1)S(1)} %slice.22), channel_id=1, source_target_pairs={{0,6},{1,7},{2,0},{3,1},{4,2},{5,3},{6,4},{7,5},{8,14},{9,15},{10,... | collective-permute-start | bytes 786440 | tf_op jit(solution)/shard_map/ppermute | solution.py:257
  117.6 8.3 %collective-permute-start.5 = (bf16[64,32,128]{2,1,0:T(8,128)(2,1)}, bf16[64,32,128]{2,1,0:T(8,128)(2,1)}, u32[]{:S(2)}, u32[]{:S(2)}) collective-permute-start(bf16[64,32,128]{2,1,0:T(8,128)(2,1)} %pad_maximum_fusion.2), channel_id=1, source_target_pairs={{0,1},{1,0},{2,3},{3,2},{4,5},{5,4},{6,7},{7,6},{8,9},{9,8},{10,11... | collective-permute-start | bytes 1572872 | tf_op jit(solution)/shard_map/ppermute | solution.py:261
  130.8 9.5 %collective-permute-start.15 = (bf16[576,128]{1,0:T(8,128)(2,1)S(1)}, bf16[576,128]{1,0:T(8,128)(2,1)S(1)}, u32[]{:S(2)}, u32[]{:S(2)}) collective-permute-start(bf16[576,128]{1,0:T(8,128)(2,1)S(1)} %shard_map.158.own_ref), channel_id=1, source_target_pairs={{0,4},{1,5},{2,6},{3,7},{4,0},{5,1},{6,2},{7,3},{8,12},{9,13},{10,... | collective-permute-start | bytes 442376 | tf_op jit(solution)/shard_map/ppermute | solution.py:257
  134.4 7.0 %collective-permute-start.13 = (bf16[576,128]{1,0:T(8,128)(2,1)S(1)}, bf16[576,128]{1,0:T(8,128)(2,1)S(1)}, u32[]{:S(2)}, u32[]{:S(2)}) collective-permute-start(bf16[576,128]{1,0:T(8,128)(2,1)S(1)} %shard_map.158.own_ref), channel_id=1, source_target_pairs={{0,2},{1,3},{2,4},{3,5},{4,6},{5,7},{6,0},{7,1},{8,10},{9,11},{10,... | collective-permute-start | bytes 442376 | tf_op jit(solution)/shard_map/ppermute | solution.py:257
  138.4 8.2 %collective-permute-start.14 = (bf16[576,128]{1,0:T(8,128)(2,1)S(1)}, bf16[576,128]{1,0:T(8,128)(2,1)S(1)}, u32[]{:S(2)}, u32[]{:S(2)}) collective-permute-start(bf16[576,128]{1,0:T(8,128)(2,1)S(1)} %shard_map.158.own_ref), channel_id=1, source_target_pairs={{0,6},{1,7},{2,0},{3,1},{4,2},{5,3},{6,4},{7,5},{8,14},{9,15},{10,... | collective-permute-start | bytes 442376 | tf_op jit(solution)/shard_map/ppermute | solution.py:257
  146.8 14.7 %collective-permute-start.16 = (bf16[4,576,128]{2,1,0:T(8,128)(2,1)S(1)}, bf16[4,576,128]{2,1,0:T(8,128)(2,1)S(1)}, u32[]{:S(2)}, u32[]{:S(2)}) collective-permute-start(bf16[4,576,128]{2,1,0:T(8,128)(2,1)S(1)} %pad_maximum_fusion.1), channel_id=1, source_target_pairs={{0,1},{1,0},{2,3},{3,2},{4,5},{5,4},{6,7},{7,6},{8,9},{9,8},{10,11... | collective-permute-start | bytes 1769480 | tf_op jit(solution)/shard_map/ppermute | solution.py:261
  163.2 26.0 %all-to-all-start.3 = ((bf16[64,32,128]{2,1,0:T(8,128)(2,1)}), bf16[64,32,128]{2,1,0:T(8,128)(2,1)}, u32[]{:S(2)}, u32[]{:S(2)}) async-start(bf16[64,32,128]{2,1,0:T(8,128)(2,1)} %get-tuple-element.41), calls=%async_computation.3 | async-start | bytes 1048576 | tf_op jit(solution)/shard_map/all_to_all | solution.py:324
  (13 other events, 43.9 us)
where the time goes:
time: 194 us; the launch traced here: 191 us
  blocking collectives  64.8 us (33%)
  starting transfers between devices  64.4 us (33%)
  waiting for transfers between devices  39.2 us (20%)
  Pallas kernels  11.2 us (6%)
  local copies, waits for them, and re-layouts  8.34 us (4%)
  other arithmetic  2.31 us (1%)
    all_to_all x1, blocking collectives, local(): got = lax.all_to_all(send, 'fs', 0, 0, tiled=True)  52.1 us
    ppermute x10, starting transfers between devices, swap(): return lax.ppermute(x, 'tp', [(i, i ^ k) for i in range(N_TP)])  27.9 us
    ppermute x7, starting transfers between devices, shift(): return lax.ppermute(x, 'tp', [(i, (i + step) % N_TP) for i in range(N_TP)])  21.3 us
    all_to_all x1, waiting for transfers between devices, local(): returned = lax.all_to_all(expert_out, 'fs', 0, 0, tiled=True)  16.2 us
    ppermute x7, waiting for transfers between devices, shift(): return lax.ppermute(x, 'tp', [(i, (i + step) % N_TP) for i in range(N_TP)])  15.3 us
    all_to_all x1, blocking collectives, local(): down_got = lax.all_to_all(down_send, 'tp', 0, 0, tiled=True)  12.7 us
    pallas_call x10, Pallas kernels, run(): return fn(*placed)  11.2 us
    all_to_all x1, starting transfers between devices, local(): weights = lax.all_to_all(spread, 'fs', 0, 0, tiled=True)  8.26 us
  transfers between devices with their start and end apart: 19, of which 7 were waited for; matrix products, arithmetic and copies ran while one was open for 1% of the time, Pallas kernels for 2%

commit v1 on v0

--- a/solution.py
+++ b/solution.py
@@ -36,7 +36,7 @@
 
 def call(body, outs, n_in, smem=0, scratch=(), far=(), keep=True):
     flat, tree = jax.tree.flatten(outs)
-    kept = [pltpu.VMEM(o.shape, o.dtype) if keep is True or i in keep else o for i, o in enumerate(flat)]
+    kept = [pltpu.VMEM(o.shape, o.dtype) if keep is True or i in keep else pltpu.HBM(o.shape, o.dtype) for i, o in enumerate(flat)]
     fn = pl.pallas_call(
         body,
         out_shape=jax.tree.unflatten(tree, kept),
@@ -48,7 +48,7 @@
 
     def run(*args):
         placed = [
-            a if i < smem or i in far else pltpu.with_memory_space_constraint(a, pltpu.VMEM)
+            a if i < smem else pltpu.with_memory_space_constraint(a, pltpu.HBM if i in far else pltpu.VMEM)
             for i, a in enumerate(args)
         ]
         return fn(*placed)
@@ -144,8 +144,37 @@
     out_ref[...] = packed_hidden(dot(normed_ref[...], weights))
 
 
-def hidden_body(m_ref, own_ref, left_ref, right_ref, far_a_ref, far_b_ref, three_ref, far_ref, w_ref, common_ref, out_ref, acc_ref):
+def copy_body(*refs):
+    out_ref, at = refs[-1], 0
+    for ref in refs[:-1]:
+        out_ref[at : at + ref.shape[0]] = ref[...]
+        at += ref.shape[0]
+
+
+def part_body(at):
+    def body(in_ref, out_ref):
+        out_ref[...] = in_ref[at : at + out_ref.shape[0]]
+
+    return body
+
+
+def own_rows_body(got_ref, out_ref):
+    out_ref[...] = got_ref[:, 0:32, :]
+
+
+def down_block(w_ref, got_ref, q):
+    at = pl.ds(pl.multiple_of((q & 7) * 8, 8), 8)
+    return w_ref[at, 32:48, :].reshape(LANES, LANES), got_ref[at, 64:80, :].reshape(LANES, LANES)
+
+
+H_ROWS = 576
+PIECE = 256
+MESSAGE = H_ROWS + 2 * PIECE
+
+
+def hidden_body(m_ref, own_ref, left_ref, right_ref, across_ref, three_ref, far_ref, w_ref, got_ref, common_ref, *rest):
     m = m_ref[0]
+    to_refs, acc_ref = rest[:4], rest[4]
 
     def joined(x):
         n = x.shape[0]
@@ -157,32 +186,41 @@
     acc_ref[...] = dot(joined(own_ref[...]), weights(m))
     acc_ref[...] += dot(joined(left_ref[...]), weights(m - 2))
     acc_ref[...] += dot(joined(right_ref[...]), weights(m + 2))
-    across = weights(m + 4)
-    acc_ref[0:512, :] += dot(joined(far_a_ref[...]), across)
-    acc_ref[512:1024, :] += dot(joined(far_b_ref[...]), across)
+    acc_ref[...] += dot(joined(across_ref[...]), weights(m + 4))
     other = m ^ 1
-    acc_ref[...] += dot(joined(three_ref[0]), weights(other))
-    acc_ref[...] += dot(joined(three_ref[1]), weights(other - 2))
-    acc_ref[...] += dot(joined(three_ref[2]), weights(other + 2))
+    acc_ref[...] += dot(joined(three_ref[0:64]), weights(other))
+    acc_ref[...] += dot(joined(three_ref[64:128]), weights(other - 2))
+    acc_ref[...] += dot(joined(three_ref[128:192]), weights(other + 2))
     acc_ref[...] += dot(joined(far_ref[...]), weights(other + 4))
-    out_ref[0:512, :] = packed_hidden(acc_ref[...])
-    out_ref[512:576, :] = common_ref[...]
-
-
-def down_body(m_ref, own_ref, left_ref, right_ref, far_ref, partner_ref, w_ref, out_ref, common_ref):
-    m = m_ref[0]
-    low = iota((576, LANES), 1) < 64
-    low_w = iota((256, LANES), 1) < 64
+    hidden = packed_hidden(acc_ref[...])
+    for ref in to_refs:
+        ref[0:512, :] = hidden
+        ref[512:H_ROWS, :] = common_ref[...]
+    for ref, step in zip(to_refs, (0, 2, -2, 4)):
+        for i, q in enumerate((m + step, (m + step) ^ 1)):
+            at = H_ROWS + PIECE * i
+            routed, shared = down_block(w_ref, got_ref, q)
+            ref[at : at + LANES, :] = routed
+            ref[at + LANES : at + PIECE, :] = shared
+
+
+def pair_body(own_ref, left_ref, right_ref, far_ref, out_ref):
+    for i, ref in enumerate((own_ref, left_ref, right_ref, far_ref)):
+        out_ref[i, 0:H_ROWS, :] = ref[0:H_ROWS, :]
+        out_ref[i, H_ROWS : H_ROWS + PIECE, :] = ref[H_ROWS + PIECE : MESSAGE, :]
+
+
+def down_body(own_ref, left_ref, right_ref, far_ref, partner_ref, out_ref, common_ref):
+    low = iota((H_ROWS, LANES), 1) < 64
+    low_w = iota((PIECE, LANES), 1) < 64
     tops, bottoms, mats, commons = [], [], [], []
-    mine = (own_ref, left_ref, right_ref, far_ref)
-    for i, shift in enumerate((0, -2, 2, 4)):
-        a = mine[i][...].astype(f32)
-        b = partner_ref[i].astype(f32)
+    for i, ref in enumerate((own_ref, left_ref, right_ref, far_ref)):
+        a = ref[0:H_ROWS, :].astype(f32)
+        b = partner_ref[i, 0:H_ROWS, :].astype(f32)
         tops.append(jnp.where(low, a, half_roll(b)).astype(bf16))
         bottoms.append(jnp.where(low, half_roll(a), b).astype(bf16))
-        q = (m + shift) & 7
-        wa = w_ref[q].astype(f32)
-        wb = w_ref[q ^ 1].astype(f32)
+        wa = ref[H_ROWS : H_ROWS + PIECE, :].astype(f32)
+        wb = partner_ref[i, H_ROWS : H_ROWS + PIECE, :].astype(f32)
         first = jnp.where(low_w, wa, half_roll(wb)).astype(bf16)
         second = jnp.where(low_w, half_roll(wa), wb).astype(bf16)
         for base, into in ((0, mats), (128, commons)):
@@ -283,7 +321,7 @@
     gain = norm_gain.reshape(1, W32)
 
     send, normed, pos = call(
-        dispatch_body, (shape(64, 80, LANES), shape(TOK, D), shape(E, TOK, dtype=f32)), 7, 1, far=range(8), keep=(1, 2)
+        dispatch_body, (shape(64, 80, LANES), shape(TOK, D), shape(E, TOK, dtype=f32)), 7, 1, far=range(8), keep=(2,)
     )(m, prompt, ids, gain, common_gate_train, common_up_train, common_down_train)
     got = lax.all_to_all(send, "fs", 0, 0, tiled=True)
 
@@ -294,40 +332,45 @@
     spread = call(assemble_body, shape(64, 48, LANES), 9, 1, keep=())(m, *crossed)
     weights = lax.all_to_all(spread, "fs", 0, 0, tiled=True)
 
-    own = got[:, 0:32, :]
+    own = call(own_rows_body, shape(64, 32, LANES), 1)(got)
     left = shift(own, 2)
     right = shift(own, -2)
-    far_a = shift(left[:32], 2)
-    far_b = shift(right[32:], -2)
-    three = swap(jnp.stack([own, left, right]), 1)
-    far = swap(jnp.concatenate([far_a, far_b]), 1)
-
-    common_hidden = call(common_hidden_body, shape(64, LANES), 2)(normed, got)
-    mix_hi, mix_lo = call(mixing_body, (shape(TOK, ROWS), shape(TOK, ROWS)), 3, far=(1, 2))(pos, ids, route_weights)
-
-    down_send = jnp.concatenate(
-        [weights[:, 32:48, :].reshape(8, 128, LANES), got[:, 64:80, :].reshape(8, 128, LANES)], axis=1
+    far_a = shift(call(part_body(0), shape(32, 32, LANES), 1)(left), 2)
+    far_b = shift(call(part_body(32), shape(32, 32, LANES), 1)(right), -2)
+    three = call(copy_body, shape(192, 32, LANES), 3)(own, left, right)
+    three = swap(three, 1)
+    across = call(copy_body, shape(64, 32, LANES), 2)(far_a, far_b)
+    far = swap(across, 1)
+
+    common_hidden = call(common_hidden_body, shape(64, LANES), 2, far=(0,))(normed, got)
+    mix_hi, mix_lo = call(mixing_body, (shape(TOK, ROWS), shape(TOK, ROWS)), 3, far=(1, 2), keep=())(
+        pos, ids, route_weights
     )
-    down_got = lax.all_to_all(down_send, "tp", 0, 0, tiled=True)
-
-    hidden = call(
-        hidden_body, shape(576, LANES), 10, 1, [pltpu.VMEM((ROWS, LANES), f32)]
-    )(m, own, left, right, far_a, far_b, three, far, weights, common_hidden)
-    h_left = shift(hidden, 2)
-    h_right = shift(hidden, -2)
-    h_far = shift(hidden, 4)
-    partner = swap(jnp.stack([hidden, h_left, h_right, h_far]), 1)
+
+    mine, to_right, to_left, to_far = call(
+        hidden_body,
+        tuple(shape(MESSAGE, LANES) for _ in range(4)),
+        10,
+        1,
+        [pltpu.VMEM((ROWS, LANES), f32)],
+        far=(3, 4, 5, 6),
+    )(m, own, left, right, across, three, far, weights, got, common_hidden)
+    h_left = shift(to_right, 2)
+    h_right = shift(to_left, -2)
+    h_far = shift(to_far, 4)
+    pair = call(pair_body, shape(4, H_ROWS + PIECE, LANES), 4)(mine, h_left, h_right, h_far)
+    partner = swap(pair, 1)
 
     expert_out, common_out = call(
-        down_body, (shape(64, 32, LANES), shape(TOK, COLS, dtype=f32)), 7, 1, keep=(1,)
-    )(m, hidden, h_left, h_right, h_far, partner, down_got)
+        down_body, (shape(64, 32, LANES), shape(TOK, COLS, dtype=f32)), 5
+    )(mine, h_left, h_right, h_far, partner)
     returned = lax.all_to_all(expert_out, "fs", 0, 0, tiled=True)
 
     serve = tuple(shape(U, D) for _ in range(3))
     gate_serve, up_serve, down_serve = call(serve_body(0), serve, 1, keep=())(weights)
     commons = call(serve_body(32), serve, 1, keep=())(got)
 
-    mixture = call(combine_body, shape(TOK, COLS), 4, keep=())(mix_hi, mix_lo, returned, common_out)
+    mixture = call(combine_body, shape(TOK, COLS), 4, far=(0, 1), keep=())(mix_hi, mix_lo, returned, common_out)
     return (mixture, gate_serve[None], up_serve[None], down_serve[None], *commons)
 
 

time: 194 us -> 184 us (0.948)
  blocking collectives: 64.8 us -> 52.2 us
  Pallas kernels: 11.2 us -> 20.7 us
  local copies, waits for them, and re-layouts: 8.34 us -> 1.04 us
  waiting for transfers between devices: 39.2 us -> 43.2 us
  other arithmetic: 2.31 us -> 0 us
    all_to_all x1 -> x0, blocking collectives: 12.7 us -> none  [local(): down_got = lax.all_to_all(down_send, 'tp', 0, 0, tiled=True)]
    pallas_call x10 -> x16, Pallas kernels: 11.2 us -> 20.7 us  [run(): return fn(*placed)]
    unnamed x36 -> x4, local copies, waits for them, and re-layouts: 8.12 us -> 1.04 us
    ppermute x7, waiting for transfers between devices: 15.3 us -> 18.3 us  [shift(): return lax.ppermute(x, 'tp', [(i, (i + step) % N_TP) for i in range(N_TP)])]
    ppermute x10, waiting for transfers between devices: 1.64 us -> 4.38 us  [swap(): return lax.ppermute(x, 'tp', [(i, i ^ k) for i in range(N_TP)])]
    all_to_all x1, starting transfers between devices: 6.93 us -> 9.19 us  [local(): returned = lax.all_to_all(expert_out, 'fs', 0, 0, tiled=True)]
  transfers between devices with their start and end apart: 19 -> 19, of which waited for: 7 -> 8; matrix products, arithmetic and copies ran while one was open for 1% -> 0% of each run, Pallas kernels for 2% -> 6%
where the time goes in v1:
time: 184 us; the launch traced here: 183 us
  starting transfers between devices  64.6 us (35%)
  blocking collectives  52.2 us (28%)
  waiting for transfers between devices  43.2 us (23%)
  Pallas kernels  20.7 us (11%)
    all_to_all x1, blocking collectives, local(): got = lax.all_to_all(send, 'fs', 0, 0, tiled=True)  52.2 us
    ppermute x10, starting transfers between devices, swap(): return lax.ppermute(x, 'tp', [(i, i ^ k) for i in range(N_TP)])  26.8 us
    ppermute x7, starting transfers between devices, shift(): return lax.ppermute(x, 'tp', [(i, (i + step) % N_TP) for i in range(N_TP)])  21 us
    pallas_call x16, Pallas kernels, run(): return fn(*placed)  20.7 us
    ppermute x7, waiting for transfers between devices, shift(): return lax.ppermute(x, 'tp', [(i, (i + step) % N_TP) for i in range(N_TP)])  18.3 us
    all_to_all x1, waiting for transfers between devices, local(): returned = lax.all_to_all(expert_out, 'fs', 0, 0, tiled=True)  15.5 us
    all_to_all x1, starting transfers between devices, local(): returned = lax.all_to_all(expert_out, 'fs', 0, 0, tiled=True)  9.19 us
    all_to_all x1, starting transfers between devices, local(): weights = lax.all_to_all(spread, 'fs', 0, 0, tiled=True)  7.61 us
  transfers between devices with their start and end apart: 19, of which 8 were waited for; matrix products, arithmetic and copies ran while one was open for 0% of the time, Pallas kernels for 6%

profile of v1, /device:TPU:6, one launch (start us, length us, event | category | flops | bytes accessed | tf_op | source)
XLA Modules:
  0.0 182.6 jit_solution(9791408434475623970)
XLA Ops:
  0.6 2.8 %shard_map.153 = (bf16[64,80,128]{2,1,0:T(8,128)(2,1)}, bf16[128,2048]{1,0:T(8,128)(2,1)}, f32[64,128]{1,0:T(8,128)S(1)}) custom-call(s32[1]{0:T(128)} %bitcast.m_ref, bf16[128,2048]{1,0:T(8,128)(2,1)} %prompt_ref.1, s32[6,128]{1,0:T(8,128)} %bitcast.7, f32[1,32]{1,0:T(1,128)} %bitcast.10, f32[32,64]{1,0:T(8,128)} %cg_ref.1, f32[32,64]{1,0:T(8,128)} %cu_ref.1, ...), custom_call_target="tpu_custom_call" | custom-call | tf_op jit(solution)/shard_map/pallas_call | solution.py:54
  3.4 52.2 %all_to_all.15.got_ref.w_ref = bf16[64,80,128]{2,1,0:T(8,128)(2,1)S(1)} all-to-all(bf16[64,80,128]{2,1,0:T(8,128)(2,1)} %get-tuple-element.35), channel_id=1, replica_groups=mesh['fs'=64,'tp'=8] {'fs'}, dimensions={0} | all-to-all | bytes 2621440 | tf_op jit(solution)/shard_map/all_to_all | solution.py:326
  55.6 2.4 %collective-permute-start = (bf16[64,32,128]{2,1,0:T(8,128)(2,1)S(1)}, bf16[64,32,128]{2,1,0:T(8,128)(2,1)S(1)}, u32[]{:S(2)}, u32[]{:S(2)}) collective-permute-start(bf16[64,32,128]{2,1,0:T(8,128)(2,1)S(1)} %shard_map.155.refs_0_.own_ref), channel_id=1, source_target_pairs={{0,2},{1,3},{2,4},{3,5},{4,6},{5,7},{6,0},{7,1},{8,10},{9,11},{10,... | collective-permute-start | bytes 1572872 | tf_op jit(solution)/shard_map/ppermute | solution.py:295
  58.0 3.5 %collective-permute-start.1 = (bf16[64,32,128]{2,1,0:T(8,128)(2,1)S(1)}, bf16[64,32,128]{2,1,0:T(8,128)(2,1)S(1)}, u32[]{:S(2)}, u32[]{:S(2)}) collective-permute-start(bf16[64,32,128]{2,1,0:T(8,128)(2,1)S(1)} %shard_map.155.refs_0_.own_ref), channel_id=1, source_target_pairs={{0,6},{1,7},{2,0},{3,1},{4,2},{5,3},{6,4},{7,5},{8,14},{9,15},{10,... | collective-permute-start | bytes 1572872 | tf_op jit(solution)/shard_map/ppermute | solution.py:295
  65.5 3.6 %collective-permute-start.11 = (bf16[8,48,128]{2,1,0:T(8,128)(2,1)S(1)}, bf16[8,48,128]{2,1,0:T(8,128)(2,1)S(1)}, u32[]{:S(2)}, u32[]{:S(2)}) collective-permute-start(bf16[8,48,128]{2,1,0:T(8,128)(2,1)S(1)} %get-tuple-element.42), channel_id=1, source_target_pairs={{0,6},{1,7},{2,4},{3,5},{4,2},{5,3},{6,0},{7,1},{8,14},{9,15},{10,... | collective-permute-start | bytes 294920 | tf_op jit(solution)/shard_map/ppermute | solution.py:299
  69.1 4.3 %collective-permute-start.12 = (bf16[8,48,128]{2,1,0:T(8,128)(2,1)S(1)}, bf16[8,48,128]{2,1,0:T(8,128)(2,1)S(1)}, u32[]{:S(2)}, u32[]{:S(2)}) collective-permute-start(bf16[8,48,128]{2,1,0:T(8,128)(2,1)S(1)} %get-tuple-element.43), channel_id=1, source_target_pairs={{0,7},{1,6},{2,5},{3,4},{4,3},{5,2},{6,1},{7,0},{8,15},{9,14},{10,... | collective-permute-start | bytes 294920 | tf_op jit(solution)/shard_map/ppermute | solution.py:299
  73.4 2.2 %collective-permute-start.6 = (bf16[8,48,128]{2,1,0:T(8,128)(2,1)S(1)}, bf16[8,48,128]{2,1,0:T(8,128)(2,1)S(1)}, u32[]{:S(2)}, u32[]{:S(2)}) collective-permute-start(bf16[8,48,128]{2,1,0:T(8,128)(2,1)S(1)} %get-tuple-element.37), channel_id=1, source_target_pairs={{0,1},{1,0},{2,3},{3,2},{4,5},{5,4},{6,7},{7,6},{8,9},{9,8},{10,11... | collective-permute-start | bytes 294920 | tf_op jit(solution)/shard_map/ppermute | solution.py:299
  78.4 2.7 %collective-permute-start.8 = (bf16[8,48,128]{2,1,0:T(8,128)(2,1)S(1)}, bf16[8,48,128]{2,1,0:T(8,128)(2,1)S(1)}, u32[]{:S(2)}, u32[]{:S(2)}) collective-permute-start(bf16[8,48,128]{2,1,0:T(8,128)(2,1)S(1)} %get-tuple-element.39), channel_id=1, source_target_pairs={{0,3},{1,2},{2,1},{3,0},{4,7},{5,6},{6,5},{7,4},{8,11},{9,10},{10,... | collective-permute-start | bytes 294920 | tf_op jit(solution)/shard_map/ppermute | solution.py:299
  81.2 3.7 %collective-permute-start.9 = (bf16[8,48,128]{2,1,0:T(8,128)(2,1)S(1)}, bf16[8,48,128]{2,1,0:T(8,128)(2,1)S(1)}, u32[]{:S(2)}, u32[]{:S(2)}) collective-permute-start(bf16[8,48,128]{2,1,0:T(8,128)(2,1)S(1)} %get-tuple-element.40), channel_id=1, source_target_pairs={{0,4},{1,5},{2,6},{3,7},{4,0},{5,1},{6,2},{7,3},{8,12},{9,13},{10,... | collective-permute-start | bytes 294920 | tf_op jit(solution)/shard_map/ppermute | solution.py:299
  86.1 2.6 %collective-permute-start.4 = (bf16[192,32,128]{2,1,0:T(8,128)(2,1)}, bf16[192,32,128]{2,1,0:T(8,128)(2,1)}, u32[]{:S(2)}, u32[]{:S(2)}) collective-permute-start(bf16[192,32,128]{2,1,0:T(8,128)(2,1)} %shard_map.159), channel_id=1, source_target_pairs={{0,1},{1,0},{2,3},{3,2},{4,5},{5,4},{6,7},{7,6},{8,9},{9,8},{10,11... | collective-permute-start | bytes 4718600 | tf_op jit(solution)/shard_map/ppermute | solution.py:299
  90.9 7.6 %all-to-all-start.1 = ((bf16[64,48,128]{2,1,0:T(8,128)(2,1)}), bf16[64,48,128]{2,1,0:T(8,128)(2,1)S(1)}, u32[]{:S(2)}, u32[]{:S(2)}) async-start(bf16[64,48,128]{2,1,0:T(8,128)(2,1)} %shard_map.161), calls=%async_computation.1 | async-start | bytes 1572864 | tf_op jit(solution)/shard_map/all_to_all | solution.py:333
  98.5 3.7 %collective-permute-start.2 = (bf16[32,32,128]{2,1,0:T(8,128)(2,1)S(1)}, bf16[32,32,128]{2,1,0:T(8,128)(2,1)S(1)}, u32[]{:S(2)}, u32[]{:S(2)}) collective-permute-start(bf16[32,32,128]{2,1,0:T(8,128)(2,1)S(1)} %shard_map.156), channel_id=1, source_target_pairs={{0,2},{1,3},{2,4},{3,5},{4,6},{5,7},{6,0},{7,1},{8,10},{9,11},{10,... | collective-permute-start | bytes 786440 | tf_op jit(solution)/shard_map/ppermute | solution.py:295
  103.3 2.2 %collective-permute-start.3 = (bf16[32,32,128]{2,1,0:T(8,128)(2,1)S(1)}, bf16[32,32,128]{2,1,0:T(8,128)(2,1)S(1)}, u32[]{:S(2)}, u32[]{:S(2)}) collective-permute-start(bf16[32,32,128]{2,1,0:T(8,128)(2,1)S(1)} %shard_map.157), channel_id=1, source_target_pairs={{0,6},{1,7},{2,0},{3,1},{4,2},{5,3},{6,4},{7,5},{8,14},{9,15},{10,... | collective-permute-start | bytes 786440 | tf_op jit(solution)/shard_map/ppermute | solution.py:295
  105.5 3.7 %collective-permute-done.2.refs_0_ = bf16[32,32,128]{2,1,0:T(8,128)(2,1)S(1)} collective-permute-done((bf16[32,32,128]{2,1,0:T(8,128)(2,1)S(1)}, bf16[32,32,128]{2,1,0:T(8,128)(2,1)S(1)}, u32[]{:S(2)}, u32[]{:S(2)}) %collective-permute-start.2) | collective-permute-done | bytes 262176 | tf_op jit(solution)/shard_map/ppermute | solution.py:295
  109.1 5.2 %collective-permute-done.3.refs_1_ = bf16[32,32,128]{2,1,0:T(8,128)(2,1)S(1)} collective-permute-done((bf16[32,32,128]{2,1,0:T(8,128)(2,1)S(1)}, bf16[32,32,128]{2,1,0:T(8,128)(2,1)S(1)}, u32[]{:S(2)}, u32[]{:S(2)}) %collective-permute-start.3) | collective-permute-done | bytes 262176 | tf_op jit(solution)/shard_map/ppermute | solution.py:295
  118.6 5.0 %all-to-all-done.1.w_ref = bf16[64,48,128]{2,1,0:T(8,128)(2,1)S(1)} async-done(((bf16[64,48,128]{2,1,0:T(8,128)(2,1)}), bf16[64,48,128]{2,1,0:T(8,128)(2,1)S(1)}, u32[]{:S(2)}, u32[]{:S(2)}) %all-to-all-start.1) | async-done | bytes 786464 | tf_op jit(solution)/shard_map/all_to_all | solution.py:333
  123.6 3.2 %shard_map.163 = (bf16[1088,128]{1,0:T(8,128)(2,1)S(1)}, bf16[1088,128]{1,0:T(8,128)(2,1)S(1)}, bf16[1088,128]{1,0:T(8,128)(2,1)S(1)}, bf16[1088,128]{1,0:T(8,128)(2,1)S(1)}) custom-call(s32[1]{0:T(128)} %bitcast.m_ref, bf16[64,32,128]{2,1,0:T(8,128)(2,1)S(1)} %shard_map.155.refs_0_.own_ref, ...), custom_call_target="tpu_custom_call" | custom-call | tf_op jit(solution)/shard_map/pallas_call | solution.py:54
  126.8 3.1 %collective-permute-start.13 = (bf16[1088,128]{1,0:T(8,128)(2,1)S(1)}, bf16[1088,128]{1,0:T(8,128)(2,1)S(1)}, u32[]{:S(2)}, u32[]{:S(2)}) collective-permute-start(bf16[1088,128]{1,0:T(8,128)(2,1)S(1)} %get-tuple-element.46), channel_id=1, source_target_pairs={{0,2},{1,3},{2,4},{3,5},{4,6},{5,7},{6,0},{7,1},{8,10},{9,11},{10,... | collective-permute-start | bytes 835592 | tf_op jit(solution)/shard_map/ppermute | solution.py:295
  129.9 2.7 %collective-permute-start.14 = (bf16[1088,128]{1,0:T(8,128)(2,1)S(1)}, bf16[1088,128]{1,0:T(8,128)(2,1)S(1)}, u32[]{:S(2)}, u32[]{:S(2)}) collective-permute-start(bf16[1088,128]{1,0:T(8,128)(2,1)S(1)} %get-tuple-element.47), channel_id=1, source_target_pairs={{0,6},{1,7},{2,0},{3,1},{4,2},{5,3},{6,4},{7,5},{8,14},{9,15},{10,... | collective-permute-start | bytes 835592 | tf_op jit(solution)/shard_map/ppermute | solution.py:295
  132.7 3.5 %collective-permute-start.15 = (bf16[1088,128]{1,0:T(8,128)(2,1)S(1)}, bf16[1088,128]{1,0:T(8,128)(2,1)S(1)}, u32[]{:S(2)}, u32[]{:S(2)}) collective-permute-start(bf16[1088,128]{1,0:T(8,128)(2,1)S(1)} %get-tuple-element.48), channel_id=1, source_target_pairs={{0,4},{1,5},{2,6},{3,7},{4,0},{5,1},{6,2},{7,3},{8,12},{9,13},{10,... | collective-permute-start | bytes 835592 | tf_op jit(solution)/shard_map/ppermute | solution.py:295
  136.1 9.4 %collective-permute-done.14.right_ref = bf16[1088,128]{1,0:T(8,128)(2,1)S(1)} collective-permute-done((bf16[1088,128]{1,0:T(8,128)(2,1)S(1)}, bf16[1088,128]{1,0:T(8,128)(2,1)S(1)}, u32[]{:S(2)}, u32[]{:S(2)}) %collective-permute-start.14) | collective-permute-done | bytes 278560 | tf_op jit(solution)/shard_map/ppermute | solution.py:295
  147.5 2.3 %collective-permute-done.16.partner_ref = bf16[4,832,128]{2,1,0:T(8,128)(2,1)S(1)} collective-permute-done((bf16[4,832,128]{2,1,0:T(8,128)(2,1)S(1)}, bf16[4,832,128]{2,1,0:T(8,128)(2,1)S(1)}, u32[]{:S(2)}, u32[]{:S(2)}) %collective-permute-start.16) | collective-permute-done | bytes 852000 | tf_op jit(solution)/shard_map/ppermute | solution.py:299
  151.5 9.2 %all-to-all-start.2 = ((bf16[64,32,128]{2,1,0:T(8,128)(2,1)}), bf16[64,32,128]{2,1,0:T(8,128)(2,1)S(1)}, u32[]{:S(2)}, u32[]{:S(2)}) async-start(bf16[64,32,128]{2,1,0:T(8,128)(2,1)} %get-tuple-element.49), calls=%async_computation.2 | async-start | bytes 1048576 | tf_op jit(solution)/shard_map/all_to_all | solution.py:367
  165.0 15.5 %all-to-all-done.2.got_ref = bf16[64,32,128]{2,1,0:T(8,128)(2,1)S(1)} async-done(((bf16[64,32,128]{2,1,0:T(8,128)(2,1)}), bf16[64,32,128]{2,1,0:T(8,128)(2,1)S(1)}, u32[]{:S(2)}, u32[]{:S(2)}) %all-to-all-start.2) | async-done | bytes 524320 | tf_op jit(solution)/shard_map/all_to_all | solution.py:367
  (35 shorter events, 25.5 us)
Async XLA Ops:
  55.6 22.8 %collective-permute-start = (bf16[64,32,128]{2,1,0:T(8,128)(2,1)S(1)}, bf16[64,32,128]{2,1,0:T(8,128)(2,1)S(1)}, u32[]{:S(2)}, u32[]{:S(2)}) collective-permute-start(bf16[64,32,128]{2,1,0:T(8,128)(2,1)S(1)} %shard_map.155.refs_0_.own_ref), channel_id=1, source_target_pairs={{0,2},{1,3},{2,4},{3,5},{4,6},{5,7},{6,0},{7,1},{8,10},{9,11},{10,... | collective-permute-start | bytes 1572872 | tf_op jit(solution)/shard_map/ppermute | solution.py:295
  58.0 23.1 %collective-permute-start.1 = (bf16[64,32,128]{2,1,0:T(8,128)(2,1)S(1)}, bf16[64,32,128]{2,1,0:T(8,128)(2,1)S(1)}, u32[]{:S(2)}, u32[]{:S(2)}) collective-permute-start(bf16[64,32,128]{2,1,0:T(8,128)(2,1)S(1)} %shard_map.155.refs_0_.own_ref), channel_id=1, source_target_pairs={{0,6},{1,7},{2,0},{3,1},{4,2},{5,3},{6,4},{7,5},{8,14},{9,15},{10,... | collective-permute-start | bytes 1572872 | tf_op jit(solution)/shard_map/ppermute | solution.py:295
  63.6 9.8 %collective-permute-start.10 = (bf16[8,48,128]{2,1,0:T(8,128)(2,1)S(1)}, bf16[8,48,128]{2,1,0:T(8,128)(2,1)S(1)}, u32[]{:S(2)}, u32[]{:S(2)}) collective-permute-start(bf16[8,48,128]{2,1,0:T(8,128)(2,1)S(1)} %get-tuple-element.41), channel_id=1, source_target_pairs={{0,5},{1,4},{2,7},{3,6},{4,1},{5,0},{6,3},{7,2},{8,13},{9,12},{10,... | collective-permute-start | bytes 294920 | tf_op jit(solution)/shard_map/ppermute | solution.py:299
  65.5 11.0 %collective-permute-start.11 = (bf16[8,48,128]{2,1,0:T(8,128)(2,1)S(1)}, bf16[8,48,128]{2,1,0:T(8,128)(2,1)S(1)}, u32[]{:S(2)}, u32[]{:S(2)}) collective-permute-start(bf16[8,48,128]{2,1,0:T(8,128)(2,1)S(1)} %get-tuple-element.42), channel_id=1, source_target_pairs={{0,6},{1,7},{2,4},{3,5},{4,2},{5,3},{6,0},{7,1},{8,14},{9,15},{10,... | collective-permute-start | bytes 294920 | tf_op jit(solution)/shard_map/ppermute | solution.py:299
  69.1 17.0 %collective-permute-start.12 = (bf16[8,48,128]{2,1,0:T(8,128)(2,1)S(1)}, bf16[8,48,128]{2,1,0:T(8,128)(2,1)S(1)}, u32[]{:S(2)}, u32[]{:S(2)}) collective-permute-start(bf16[8,48,128]{2,1,0:T(8,128)(2,1)S(1)} %get-tuple-element.43), channel_id=1, source_target_pairs={{0,7},{1,6},{2,5},{3,4},{4,3},{5,2},{6,1},{7,0},{8,15},{9,14},{10,... | collective-permute-start | bytes 294920 | tf_op jit(solution)/shard_map/ppermute | solution.py:299
  73.4 15.3 %collective-permute-start.6 = (bf16[8,48,128]{2,1,0:T(8,128)(2,1)S(1)}, bf16[8,48,128]{2,1,0:T(8,128)(2,1)S(1)}, u32[]{:S(2)}, u32[]{:S(2)}) collective-permute-start(bf16[8,48,128]{2,1,0:T(8,128)(2,1)S(1)} %get-tuple-element.37), channel_id=1, source_target_pairs={{0,1},{1,0},{2,3},{3,2},{4,5},{5,4},{6,7},{7,6},{8,9},{9,8},{10,11... | collective-permute-start | bytes 294920 | tf_op jit(solution)/shard_map/ppermute | solution.py:299
  76.5 12.3 %collective-permute-start.7 = (bf16[8,48,128]{2,1,0:T(8,128)(2,1)S(1)}, bf16[8,48,128]{2,1,0:T(8,128)(2,1)S(1)}, u32[]{:S(2)}, u32[]{:S(2)}) collective-permute-start(bf16[8,48,128]{2,1,0:T(8,128)(2,1)S(1)} %get-tuple-element.38), channel_id=1, source_target_pairs={{0,2},{1,3},{2,0},{3,1},{4,6},{5,7},{6,4},{7,5},{8,10},{9,11},{10,... | collective-permute-start | bytes 294920 | tf_op jit(solution)/shard_map/ppermute | solution.py:299
  78.4 10.4 %collective-permute-start.8 = (bf16[8,48,128]{2,1,0:T(8,128)(2,1)S(1)}, bf16[8,48,128]{2,1,0:T(8,128)(2,1)S(1)}, u32[]{:S(2)}, u32[]{:S(2)}) collective-permute-start(bf16[8,48,128]{2,1,0:T(8,128)(2,1)S(1)} %get-tuple-element.39), channel_id=1, source_target_pairs={{0,3},{1,2},{2,1},{3,0},{4,7},{5,6},{6,5},{7,4},{8,11},{9,10},{10,... | collective-permute-start | bytes 294920 | tf_op jit(solution)/shard_map/ppermute | solution.py:299
  81.2 5.0 %copy-start = (bf16[64,32,128]{2,1,0:T(8,128)(2,1)}, bf16[64,32,128]{2,1,0:T(8,128)(2,1)S(1)}, u32[]{:S(2)}) copy-start(bf16[64,32,128]{2,1,0:T(8,128)(2,1)S(1)} %collective-permute-done.1.in_ref.refs_2_.right_ref) | copy-start | bytes 1572868
  81.2 8.7 %collective-permute-start.9 = (bf16[8,48,128]{2,1,0:T(8,128)(2,1)S(1)}, bf16[8,48,128]{2,1,0:T(8,128)(2,1)S(1)}, u32[]{:S(2)}, u32[]{:S(2)}) collective-permute-start(bf16[8,48,128]{2,1,0:T(8,128)(2,1)S(1)} %get-tuple-element.40), channel_id=1, source_target_pairs={{0,4},{1,5},{2,6},{3,7},{4,0},{5,1},{6,2},{7,3},{8,12},{9,13},{10,... | collective-permute-start | bytes 294920 | tf_op jit(solution)/shard_map/ppermute | solution.py:299
  86.1 37.5 %collective-permute-start.4 = (bf16[192,32,128]{2,1,0:T(8,128)(2,1)}, bf16[192,32,128]{2,1,0:T(8,128)(2,1)}, u32[]{:S(2)}, u32[]{:S(2)}) collective-permute-start(bf16[192,32,128]{2,1,0:T(8,128)(2,1)} %shard_map.159), channel_id=1, source_target_pairs={{0,1},{1,0},{2,3},{3,2},{4,5},{5,4},{6,7},{7,6},{8,9},{9,8},{10,11... | collective-permute-start | bytes 4718600 | tf_op jit(solution)/shard_map/ppermute | solution.py:299
  90.9 32.8 %all-to-all-start.1 = ((bf16[64,48,128]{2,1,0:T(8,128)(2,1)}), bf16[64,48,128]{2,1,0:T(8,128)(2,1)S(1)}, u32[]{:S(2)}, u32[]{:S(2)}) async-start(bf16[64,48,128]{2,1,0:T(8,128)(2,1)} %shard_map.161), calls=%async_computation.1 | async-start | bytes 1572864 | tf_op jit(solution)/shard_map/all_to_all | solution.py:333
  98.5 10.6 %collective-permute-start.2 = (bf16[32,32,128]{2,1,0:T(8,128)(2,1)S(1)}, bf16[32,32,128]{2,1,0:T(8,128)(2,1)S(1)}, u32[]{:S(2)}, u32[]{:S(2)}) collective-permute-start(bf16[32,32,128]{2,1,0:T(8,128)(2,1)S(1)} %shard_map.156), channel_id=1, source_target_pairs={{0,2},{1,3},{2,4},{3,5},{4,6},{5,7},{6,0},{7,1},{8,10},{9,11},{10,... | collective-permute-start | bytes 786440 | tf_op jit(solution)/shard_map/ppermute | solution.py:295
  102.2 1.0 copy-start.1
  103.3 11.1 %collective-permute-start.3 = (bf16[32,32,128]{2,1,0:T(8,128)(2,1)S(1)}, bf16[32,32,128]{2,1,0:T(8,128)(2,1)S(1)}, u32[]{:S(2)}, u32[]{:S(2)}) collective-permute-start(bf16[32,32,128]{2,1,0:T(8,128)(2,1)S(1)} %shard_map.157), channel_id=1, source_target_pairs={{0,6},{1,7},{2,0},{3,1},{4,2},{5,3},{6,4},{7,5},{8,14},{9,15},{10,... | collective-permute-start | bytes 786440 | tf_op jit(solution)/shard_map/ppermute | solution.py:295
  115.3 8.3 %collective-permute-start.5 = (bf16[64,32,128]{2,1,0:T(8,128)(2,1)}, bf16[64,32,128]{2,1,0:T(8,128)(2,1)}, u32[]{:S(2)}, u32[]{:S(2)}) collective-permute-start(bf16[64,32,128]{2,1,0:T(8,128)(2,1)} %shard_map.158.across_ref), channel_id=1, source_target_pairs={{0,1},{1,0},{2,3},{3,2},{4,5},{5,4},{6,7},{7,6},{8,9},{9,8},{10,11... | collective-permute-start | bytes 1572872 | tf_op jit(solution)/shard_map/ppermute | solution.py:299
  126.8 9.3 %collective-permute-start.13 = (bf16[1088,128]{1,0:T(8,128)(2,1)S(1)}, bf16[1088,128]{1,0:T(8,128)(2,1)S(1)}, u32[]{:S(2)}, u32[]{:S(2)}) collective-permute-start(bf16[1088,128]{1,0:T(8,128)(2,1)S(1)} %get-tuple-element.46), channel_id=1, source_target_pairs={{0,2},{1,3},{2,4},{3,5},{4,6},{5,7},{6,0},{7,1},{8,10},{9,11},{10,... | collective-permute-start | bytes 835592 | tf_op jit(solution)/shard_map/ppermute | solution.py:295
  129.9 15.6 %collective-permute-start.14 = (bf16[1088,128]{1,0:T(8,128)(2,1)S(1)}, bf16[1088,128]{1,0:T(8,128)(2,1)S(1)}, u32[]{:S(2)}, u32[]{:S(2)}) collective-permute-start(bf16[1088,128]{1,0:T(8,128)(2,1)S(1)} %get-tuple-element.47), channel_id=1, source_target_pairs={{0,6},{1,7},{2,0},{3,1},{4,2},{5,3},{6,4},{7,5},{8,14},{9,15},{10,... | collective-permute-start | bytes 835592 | tf_op jit(solution)/shard_map/ppermute | solution.py:295
  132.7 12.9 %collective-permute-start.15 = (bf16[1088,128]{1,0:T(8,128)(2,1)S(1)}, bf16[1088,128]{1,0:T(8,128)(2,1)S(1)}, u32[]{:S(2)}, u32[]{:S(2)}) collective-permute-start(bf16[1088,128]{1,0:T(8,128)(2,1)S(1)} %get-tuple-element.48), channel_id=1, source_target_pairs={{0,4},{1,5},{2,6},{3,7},{4,0},{5,1},{6,2},{7,3},{8,12},{9,13},{10,... | collective-permute-start | bytes 835592 | tf_op jit(solution)/shard_map/ppermute | solution.py:295
  145.6 4.3 %collective-permute-start.16 = (bf16[4,832,128]{2,1,0:T(8,128)(2,1)S(1)}, bf16[4,832,128]{2,1,0:T(8,128)(2,1)S(1)}, u32[]{:S(2)}, u32[]{:S(2)}) collective-permute-start(bf16[4,832,128]{2,1,0:T(8,128)(2,1)S(1)} %shard_map.164), channel_id=1, source_target_pairs={{0,1},{1,0},{2,3},{3,2},{4,5},{5,4},{6,7},{7,6},{8,9},{9,8},{10,11... | collective-permute-start | bytes 2555912 | tf_op jit(solution)/shard_map/ppermute | solution.py:299
  151.5 29.0 %all-to-all-start.2 = ((bf16[64,32,128]{2,1,0:T(8,128)(2,1)}), bf16[64,32,128]{2,1,0:T(8,128)(2,1)S(1)}, u32[]{:S(2)}, u32[]{:S(2)}) async-start(bf16[64,32,128]{2,1,0:T(8,128)(2,1)} %get-tuple-element.49), calls=%async_computation.2 | async-start | bytes 1048576 | tf_op jit(solution)/shard_map/all_to_all | solution.py:367

commit v2 on v1

v2 whole, which is shorter than its diff:
```python
import jax
import jax.numpy as jnp
from jax import lax
from jax.experimental import pallas as pl
from jax.experimental.pallas import tpu as pltpu
from jax.sharding import PartitionSpec as P


E = 64
CAP = 16
TOP_K = 6
TOK = 128
D = 2048
N_FS = 64
N_TP = 8
U = 64
W32 = D // N_FS
COLS = D // N_TP
ROWS = E * CAP
LANES = 128
PARTS = 8
COLUMNS = [[8 * z + y for y in range(8)] for z in range(8)]
epsilon = 1e-06

f32 = jnp.float32
bf16 = jnp.bfloat16
VM = pl.BlockSpec(memory_space=pltpu.VMEM)
SM = pl.BlockSpec(memory_space=pltpu.SMEM)


def iota(shape, dim):
    return lax.broadcasted_iota(jnp.int32, shape, dim)


def half_roll(x):
    return pltpu.roll(x, 64, 1)


def call(body, outs, n_in, smem=0, scratch=(), far=(), keep=True):
    flat, tree = jax.tree.flatten(outs)
    kept = [pltpu.VMEM(o.shape, o.dtype) if keep is True or i in keep else pltpu.HBM(o.shape, o.dtype) for i, o in enumerate(flat)]
    fn = pl.pallas_call(
        body,
        out_shape=jax.tree.unflatten(tree, kept),
        in_specs=[SM] * smem + [VM] * (n_in - smem),
        out_specs=jax.tree.map(lambda _: VM, outs),
        scratch_shapes=list(scratch),
        compiler_params=pltpu.CompilerParams(vmem_limit_bytes=16 * 2**20),
    )

    def run(*args):
        placed = [
            a if i < smem else pltpu.with_memory_space_constraint(a, pltpu.HBM if i in far else pltpu.VMEM)
            for i, a in enumerate(args)
        ]
        return fn(*placed)

    return run


def dot(a, b):
    return jnp.dot(a, b, preferred_element_type=f32)


def dot_nt(a, b):
    return lax.dot_general(a, b, (((1,), (1,)), ((), ())), preferred_element_type=f32)


def gain_column(gain_ref):
    n = gain_ref.shape[1]
    eye = iota((n, n), 0) == iota((n, n), 1)
    spread = jnp.where(eye, jnp.broadcast_to(gain_ref[...], (n, n)), 0.0)
    return jnp.sum(spread, axis=1, keepdims=True)


def dispatch_body(m_ref, prompt_ref, ids_ref, gain_ref, cg_ref, cu_ref, cd_ref, send_ref, normed_ref, pos_ref):
    m = m_ref[0]
    gain = gain_column(gain_ref)
    both = jnp.concatenate([cg_ref[...] * gain, cu_ref[...] * gain], axis=1)
    down = jnp.concatenate([cd_ref[0:16, :], cd_ref[16:32, :]], axis=1)
    piece = jnp.concatenate([both, down, jnp.zeros((16, LANES), f32)], axis=0)
    parts = piece.reshape(PARTS, 8, LANES).astype(bf16)
    for z in range(N_FS // PARTS):
        send_ref[PARTS * z : PARTS * z + PARTS, 32:40, :] = parts
    values = prompt_ref[...].astype(f32)
    scale = lax.rsqrt(jnp.mean(values * values, axis=1, keepdims=True) + epsilon)
    normed_ref[...] = (values * scale).astype(bf16)
    experts = iota((E, TOK), 0)
    named = jnp.zeros((E, TOK), f32)
    for k in range(TOP_K):
        named = jnp.where(ids_ref[k : k + 1, :] == experts, 1.0, named)
    earlier = jnp.where(iota((TOK, TOK), 0) < iota((TOK, TOK), 1), 1.0, 0.0).astype(bf16)
    slot = dot(named.astype(bf16), earlier)
    pos = jnp.where(named > 0.0, slot, -1.0)
    pos_ref[...] = pos
    expand = jnp.where((iota((ROWS, E), 0) >> 4) == iota((ROWS, E), 1), 1.0, 0.0).astype(bf16)
    at = dot(expand, pos.astype(bf16))
    pick = jnp.where(at == (iota((ROWS, TOK), 0) & 15).astype(f32), 1.0, 0.0).astype(bf16)
    mine = normed_ref[:, pl.ds(pl.multiple_of(m * COLS, COLS), COLS)]
    rows = dot(pick, mine).astype(bf16)
    send_ref[:, 0:16, :] = rows[:, :LANES].reshape(E, CAP, LANES)
    send_ref[:, 16:32, :] = rows[:, LANES:].reshape(E, CAP, LANES)


def split_body(got_ref, own_ref, parts_ref):
    own_ref[...] = got_ref[:, 0:32, :]
    parts = got_ref[:, 32:40, :]
    for y in range(PARTS):
        parts_ref[y] = parts


def join_body(parts_ref, out_ref):
    pieces = [parts_ref[p].astype(f32) for p in range(6)]
    out_ref[...] = jnp.concatenate(pieces, axis=1).astype(bf16)


STEPS = (0, 2, -2, 4)


def prepare_body(m_ref, gain_ref, g_ref, u_ref, d_ref, keep_ref, swap_ref):
    m = m_ref[0]
    gain = gain_column(gain_ref)
    low = iota((W32, LANES), 1) < 64
    low16 = iota((16, LANES), 1) < 64
    for i, step in enumerate(STEPS):
        for out_ref, to in ((keep_ref, (m + step) & 7), (swap_ref, ((m + step) & 7) ^ 1)):
            odd = (to & 1) == 1
            for j in range(8):
                at = pl.ds(pl.multiple_of(j * 512 + (to >> 1) * LANES, LANES), LANES)
                g = g_ref[:, at] * gain
                u = u_ref[:, at] * gain
                d = d_ref[:, at]
                g = jnp.where(odd, half_roll(g), g)
                u = jnp.where(odd, u, half_roll(u))
                out_ref[i, j, 0:32, :] = jnp.where(low, g, u).astype(bf16)
                d0, d1 = d[0:16, :], d[16:32, :]
                d0 = jnp.where(odd, half_roll(d0), d0)
                d1 = jnp.where(odd, d1, half_roll(d1))
                out_ref[i, j, 32:48, :] = jnp.where(low16, d0, d1).astype(bf16)


def repack_body(keep_ref, swapped_ref, *out_refs):
    for i, out_ref in enumerate(out_refs):
        out_ref[0:8] = keep_ref[i + 1]
        out_ref[8:16] = swapped_ref[i + 1]


def assemble_body(m_ref, keep_ref, swapped_ref, left_ref, right_ref, far_ref, out_ref):
    m = m_ref[0]

    def put(t, x):
        out_ref[pl.ds(pl.multiple_of(t * 8, 8), 8)] = x

    put(m, keep_ref[0])
    put(m ^ 1, swapped_ref[0])
    for step, ref in zip(STEPS[1:], (left_ref, right_ref, far_ref)):
        t = (m - step) & 7
        put(t, ref[0:8])
        put(t ^ 1, ref[8:16])


def silu(v):
    return v / (1.0 + jnp.exp(-v))


def packed_hidden(acc):
    half = acc.shape[0] // 2
    top, bottom = acc[:half], acc[half:]
    first = silu(top) * half_roll(top)
    second = silu(half_roll(bottom)) * bottom
    return jnp.where(iota((half, LANES), 1) < 64, first, second).astype(bf16)


def copy_body(*refs):
    out_ref, at = refs[-1], 0
    for ref in refs[:-1]:
        out_ref[at : at + ref.shape[0]] = ref[...]
        at += ref.shape[0]


def part_body(at):
    def body(in_ref, out_ref):
        out_ref[...] = in_ref[at : at + out_ref.shape[0]]

    return body


def down_block(w_ref, q):
    return w_ref[pl.ds(pl.multiple_of((q & 7) * 8, 8), 8), 32:48, :].reshape(LANES, LANES)


def write_messages(m, rows, w_ref, refs):
    n = rows.shape[0]
    for ref, step in zip(refs, STEPS):
        ref[0:n, :] = rows
        ref[n : n + LANES, :] = down_block(w_ref, m + step)
        ref[n + LANES : n + 2 * LANES, :] = down_block(w_ref, (m + step) ^ 1)


def common_hidden_body(m_ref, normed_ref, w_ref, *to_refs):
    weights = w_ref[:, 0:32, :].reshape(D, LANES)
    write_messages(m_ref[0], packed_hidden(dot(normed_ref[...], weights)), w_ref, to_refs)


def hidden_body(m_ref, own_ref, left_ref, right_ref, across_ref, three_ref, far_ref, w_ref, *rest):
    m = m_ref[0]
    to_refs, acc_ref = rest[:4], rest[4]

    def joined(x):
        n = x.shape[0]
        return jnp.concatenate([x[:, 0:16, :].reshape(n * 16, LANES), x[:, 16:32, :].reshape(n * 16, LANES)], axis=1)

    def weights(q):
        return w_ref[pl.ds(pl.multiple_of((q & 7) * 8, 8), 8), 0:32, :].reshape(COLS, LANES)

    acc_ref[...] = dot(joined(own_ref[...]), weights(m))
    acc_ref[...] += dot(joined(left_ref[...]), weights(m - 2))
    acc_ref[...] += dot(joined(right_ref[...]), weights(m + 2))
    acc_ref[...] += dot(joined(across_ref[...]), weights(m + 4))
    other = m ^ 1
    acc_ref[...] += dot(joined(three_ref[0:64]), weights(other))
    acc_ref[...] += dot(joined(three_ref[64:128]), weights(other - 2))
    acc_ref[...] += dot(joined(three_ref[128:192]), weights(other + 2))
    acc_ref[...] += dot(joined(far_ref[...]), weights(other + 4))
    write_messages(m, packed_hidden(acc_ref[...]), w_ref, to_refs)


def pair_body(*refs):
    out_ref = refs[-1]
    n = out_ref.shape[1] - LANES
    for i, ref in enumerate(refs[:-1]):
        out_ref[i, 0:n, :] = ref[0:n, :]
        out_ref[i, n : n + LANES, :] = ref[n + LANES : n + 2 * LANES, :]


def down_parts(refs, partner_ref):
    n = partner_ref.shape[1] - LANES
    low = iota((n, LANES), 1) < 64
    low_w = iota((LANES, LANES), 1) < 64
    tops, bottoms, mats = [], [], []
    for i, ref in enumerate(refs):
        a = ref[0:n, :].astype(f32)
        b = partner_ref[i, 0:n, :].astype(f32)
        tops.append(jnp.where(low, a, half_roll(b)).astype(bf16))
        bottoms.append(jnp.where(low, half_roll(a), b).astype(bf16))
        wa = ref[n : n + LANES, :].astype(f32)
        wb = partner_ref[i, n : n + LANES, :].astype(f32)
        first = jnp.where(low_w, wa, half_roll(wb)).astype(bf16)
        second = jnp.where(low_w, half_roll(wa), wb).astype(bf16)
        parts = []
        for f in range(8):
            at = slice(16 * f, 16 * f + 16)
            parts += [first[at], second[at]]
        mats.append(jnp.concatenate(parts, axis=0))
    return tuple(jnp.concatenate(x, axis=1) for x in (tops, bottoms, mats))


def down_body(own_ref, left_ref, right_ref, far_ref, partner_ref, out_ref):
    top, bottom, mat = down_parts((own_ref, left_ref, right_ref, far_ref), partner_ref)
    for i, rows in enumerate((top, bottom)):
        r = dot_nt(rows, mat).astype(bf16)
        at = slice(32 * i, 32 * i + 32)
        out_ref[at, 0:16, :] = r[:, :LANES].reshape(32, 16, LANES)
        out_ref[at, 16:32, :] = r[:, LANES:].reshape(32, 16, LANES)


def common_down_body(own_ref, left_ref, right_ref, far_ref, partner_ref, out_ref):
    top, bottom, mat = down_parts((own_ref, left_ref, right_ref, far_ref), partner_ref)
    out_ref[0:64, :] = dot_nt(top, mat)
    out_ref[64:128, :] = dot_nt(bottom, mat)


def mixing_body(pos_ref, ids_ref, weight_ref, hi_ref, lo_ref):
    experts = iota((E, TOK), 0)
    w = jnp.zeros((E, TOK), f32)
    for k in range(TOP_K):
        w = jnp.where(ids_ref[k : k + 1, :] == experts, weight_ref[k : k + 1, :], w)
    pos = jnp.transpose(pos_ref[...]).astype(bf16)
    w = jnp.transpose(w)
    expand = jnp.where(iota((E, ROWS), 0) == (iota((E, ROWS), 1) >> 4), 1.0, 0.0).astype(bf16)
    hit = dot(pos, expand) == (iota((TOK, ROWS), 1) & 15).astype(f32)
    hi = w.astype(bf16)
    lo = (w - hi.astype(f32)).astype(bf16)
    hi_ref[...] = jnp.where(hit, dot(hi, expand), 0.0).astype(bf16)
    lo_ref[...] = jnp.where(hit, dot(lo, expand), 0.0).astype(bf16)


def combine_body(hi_ref, lo_ref, got_ref, common_ref, out_ref):
    hi, lo = hi_ref[...], lo_ref[...]
    for h in range(2):
        rows = got_ref[:, 16 * h : 16 * h + 16, :].reshape(ROWS, LANES)
        at = slice(LANES * h, LANES * h + LANES)
        out_ref[:, at] = (dot(hi, rows) + dot(lo, rows) + common_ref[:, at]).astype(bf16)


def serve_body(w_ref, g_ref, u_ref, d_ref):
    low = iota((LANES, LANES), 1) < 64
    for i in range(16):
        block = w_ref[4 * i : 4 * i + 4, 0:32, :].reshape(LANES, LANES).astype(f32)
        turned = jnp.transpose(block).astype(bf16)
        at = slice(LANES * i, LANES * i + LANES)
        g_ref[:, at] = turned[:64]
        u_ref[:, at] = turned[64:]
    for i in range(8):
        sides = []
        for s in range(2):
            straight, rolled = [], []
            for f in range(4):
                x = w_ref[8 * i + 4 * s + f, 32:48, :].astype(f32)
                y = half_roll(x)
                straight += [x, y]
                rolled += [y, x]
            sides.append(jnp.concatenate(rolled if s else straight, axis=0))
        turned = jnp.transpose(jnp.where(low, sides[0], sides[1])).astype(bf16)
        at = 256 * i
        d_ref[:, at : at + LANES] = turned[:64]
        d_ref[:, at + LANES : at + 2 * LANES] = turned[64:]


def shift(x, step):
    return lax.ppermute(x, "tp", [(i, (i + step) % N_TP) for i in range(N_TP)])


def swap(x, k):
    return lax.ppermute(x, "tp", [(i, i ^ k) for i in range(N_TP)])


def shape(*dims, dtype=bf16):
    return jax.ShapeDtypeStruct(dims, dtype)


def local(
    prompt,
    norm_gain,
    gate_train,
    up_train,
    down_train,
    common_gate_train,
    common_up_train,
    common_down_train,
    route_ids,
    route_weights,
):
    m = lax.axis_index("tp").astype(jnp.int32).reshape(1)
    ids = route_ids.T
    route_weights = route_weights.T
    gain = norm_gain.reshape(1, W32)

    send, normed, pos = call(
        dispatch_body, (shape(64, 40, LANES), shape(TOK, D), shape(E, TOK, dtype=f32)), 7, 1, far=range(8), keep=(2,)
    )(m, prompt, ids, gain, common_gate_train, common_up_train, common_down_train)
    got = lax.all_to_all(send, "fs", 0, 0, tiled=True)

    half = shape(4, 8, 48, LANES)
    kept, to_partner = call(prepare_body, (half, half), 5, 1, far=range(8))(m, gain, gate_train, up_train, down_train)
    swapped = swap(to_partner, 1)
    message = shape(16, 48, LANES)
    to_right, to_left, to_far = call(repack_body, (message, message, message), 2)(kept, swapped)
    w_far = shift(to_far, 4)
    w_left = shift(to_right, 2)
    w_right = shift(to_left, -2)
    spread = call(assemble_body, shape(64, 48, LANES), 6, 1, keep=())(m, kept, swapped, w_left, w_right, w_far)
    weights = lax.all_to_all(spread, "fs", 0, 0, tiled=True)

    own, common_send = call(split_body, (shape(64, 32, LANES), shape(8, 64, 8, LANES)), 1, keep=(0,))(got)
    left = shift(own, 2)
    right = shift(own, -2)
    far_a = shift(call(part_body(0), shape(32, 32, LANES), 1)(left), 2)
    far_b = shift(call(part_body(32), shape(32, 32, LANES), 1)(right), -2)
    three = call(copy_body, shape(192, 32, LANES), 3)(own, left, right)
    three = swap(three, 1)
    across = call(copy_body, shape(64, 32, LANES), 2)(far_a, far_b)
    far = swap(across, 1)

    common = lax.all_to_all(common_send, "fs", 0, 0, axis_index_groups=COLUMNS, tiled=True)
    common = call(join_body, shape(64, 48, LANES), 1)(common)

    mix_hi, mix_lo = call(mixing_body, (shape(TOK, ROWS), shape(TOK, ROWS)), 3, far=(1, 2))(pos, ids, route_weights)

    message = shape(512 + 2 * LANES, LANES)
    mine, to_right, to_left, to_far = call(
        hidden_body, (message,) * 4, 8, 1, [pltpu.VMEM((ROWS, LANES), f32)], far=(3, 4, 5, 6)
    )(m, own, left, right, across, three, far, weights)
    h_far = shift(to_far, 4)
    h_left = shift(to_right, 2)
    h_right = shift(to_left, -2)
    pair = call(pair_body, shape(4, 512 + LANES, LANES), 4)(mine, h_left, h_right, h_far)
    partner = swap(pair, 1)
    expert_out = call(down_body, shape(64, 32, LANES), 5, keep=())(mine, h_left, h_right, h_far, partner)
    returned = lax.all_to_all(expert_out, "fs", 0, 0, tiled=True)

    message = shape(64 + 2 * LANES, LANES)
    mine, to_right, to_left, to_far = call(common_hidden_body, (message,) * 4, 3, 1, far=(1,))(m, normed, common)
    c_far = shift(to_far, 4)
    c_left = shift(to_right, 2)
    c_right = shift(to_left, -2)
    pair = call(pair_body, shape(4, 64 + LANES, LANES), 4)(mine, c_left, c_right, c_far)
    partner = swap(pair, 1)
    common_out = call(common_down_body, shape(TOK, COLS, dtype=f32), 5)(mine, c_left, c_right, c_far, partner)

    serve = tuple(shape(U, D) for _ in range(3))
    gate_serve, up_serve, down_serve = call(serve_body, serve, 1, keep=())(weights)
    commons = call(serve_body, serve, 1, keep=())(common)

    mixture = call(combine_body, shape(TOK, COLS), 4, keep=())(mix_hi, mix_lo, returned, common_out)
    return (mixture, gate_serve[None], up_serve[None], down_serve[None], *commons)


def solution(mesh):
    in_specs = (
        P("fs", None),
        P("fs"),
        P("fs", "tp"),
        P("fs", "tp"),
        P("fs", "tp"),
        P("fs", "tp"),
        P("fs", "tp"),
        P("fs", "tp"),
        P("fs", None),
        P("fs", None),
    )
    out_specs = (
        P("fs", "tp"),
        P("fs", "tp", None),
        P("fs", "tp", None),
        P("fs", "tp", None),
        P("tp", None),
        P("tp", None),
        P("tp", None),
    )

    return jax.shard_map(local, mesh=mesh, in_specs=in_specs, out_specs=out_specs, check_vma=False)
```

time: 184 us -> 167 us (0.908)
  the two profiles are of different devices: /device:TPU:6 before, /device:TPU:1 now
where the time goes in v2:
time: 167 us; the launch traced here: 166 us
  starting transfers between devices  109 us (65%)
  waiting for transfers between devices  35.9 us (21%)
  Pallas kernels  19.4 us (12%)
    ppermute x13, starting transfers between devices, shift(): return lax.ppermute(x, 'tp', [(i, (i + step) % N_TP) for i in range(N_TP)])  42.2 us
    ppermute x13, waiting for transfers between devices, shift(): return lax.ppermute(x, 'tp', [(i, (i + step) % N_TP) for i in range(N_TP)])  31.3 us
    pallas_call x20, Pallas kernels, run(): return fn(*placed)  19.4 us
    ppermute x5, starting transfers between devices, swap(): return lax.ppermute(x, 'tp', [(i, i ^ k) for i in range(N_TP)])  18.4 us
    all_to_all x1, starting transfers between devices, local(): got = lax.all_to_all(send, 'fs', 0, 0, tiled=True)  17.1 us
    all_to_all x1, starting transfers between devices, local(): returned = lax.all_to_all(expert_out, 'fs', 0, 0, tiled=True)  12.6 us
    all_to_all x1, starting transfers between devices, local(): weights = lax.all_to_all(spread, 'fs', 0, 0, tiled=True)  12.4 us
    all_to_all x1, starting transfers between devices, local(): lax.all_to_all(common_send, 'fs', 0, 0, axis_index_groups=COLUMNS, tiled=...  6.21 us
  transfers between devices with their start and end apart: 22, of which 12 were waited for; matrix products, arithmetic and copies ran while one was open for 0% of the time, Pallas kernels for 10%

profile of v2, /device:TPU:1, one launch (start us, length us, event | category | flops | bytes accessed | tf_op | source)
XLA Modules:
  0.0 165.9 jit_solution(7637284224213856365)
XLA Ops:
  3.2 17.1 %all-to-all-start = ((bf16[64,40,128]{2,1,0:T(8,128)(2,1)}), bf16[64,40,128]{2,1,0:T(8,128)(2,1)S(1)}, u32[]{:S(2)}, u32[]{:S(2)}) async-start(bf16[64,40,128]{2,1,0:T(8,128)(2,1)} %get-tuple-element.36), calls=%async_computation | async-start | bytes 1310720 | tf_op jit(solution)/shard_map/all_to_all | solution.py:352
  26.6 3.1 %collective-permute-start.7 = (bf16[16,48,128]{2,1,0:T(8,128)(2,1)S(1)}, bf16[16,48,128]{2,1,0:T(8,128)(2,1)S(1)}, u32[]{:S(2)}, u32[]{:S(2)}) collective-permute-start(bf16[16,48,128]{2,1,0:T(8,128)(2,1)S(1)} %get-tuple-element.40), channel_id=1, source_target_pairs={{0,2},{1,3},{2,4},{3,5},{4,6},{5,7},{6,0},{7,1},{8,10},{9,11},{10,... | collective-permute-start | bytes 589832 | tf_op jit(solution)/shard_map/ppermute | solution.py:321
  29.8 3.4 %collective-permute-start.8 = (bf16[16,48,128]{2,1,0:T(8,128)(2,1)S(1)}, bf16[16,48,128]{2,1,0:T(8,128)(2,1)S(1)}, u32[]{:S(2)}, u32[]{:S(2)}) collective-permute-start(bf16[16,48,128]{2,1,0:T(8,128)(2,1)S(1)} %get-tuple-element.41), channel_id=1, source_target_pairs={{0,6},{1,7},{2,0},{3,1},{4,2},{5,3},{6,4},{7,5},{8,14},{9,15},{10,... | collective-permute-start | bytes 589832 | tf_op jit(solution)/shard_map/ppermute | solution.py:321
  33.1 3.4 %collective-permute-start.9 = (bf16[16,48,128]{2,1,0:T(8,128)(2,1)S(1)}, bf16[16,48,128]{2,1,0:T(8,128)(2,1)S(1)}, u32[]{:S(2)}, u32[]{:S(2)}) collective-permute-start(bf16[16,48,128]{2,1,0:T(8,128)(2,1)S(1)} %get-tuple-element.42), channel_id=1, source_target_pairs={{0,4},{1,5},{2,6},{3,7},{4,0},{5,1},{6,2},{7,3},{8,12},{9,13},{10,... | collective-permute-start | bytes 589832 | tf_op jit(solution)/shard_map/ppermute | solution.py:321
  37.5 4.6 %collective-permute-done.9.far_ref = bf16[16,48,128]{2,1,0:T(8,128)(2,1)S(1)} collective-permute-done((bf16[16,48,128]{2,1,0:T(8,128)(2,1)S(1)}, bf16[16,48,128]{2,1,0:T(8,128)(2,1)S(1)}, u32[]{:S(2)}, u32[]{:S(2)}) %collective-permute-start.9) | collective-permute-done | bytes 196640 | tf_op jit(solution)/shard_map/ppermute | solution.py:321
  43.0 12.4 %all-to-all-start.1 = ((bf16[64,48,128]{2,1,0:T(8,128)(2,1)}), bf16[64,48,128]{2,1,0:T(8,128)(2,1)S(1)}, u32[]{:S(2)}, u32[]{:S(2)}) async-start(bf16[64,48,128]{2,1,0:T(8,128)(2,1)} %shard_map.162), calls=%async_computation.1 | async-start | bytes 1572864 | tf_op jit(solution)/shard_map/all_to_all | solution.py:363
  56.6 3.3 %collective-permute-start = (bf16[64,32,128]{2,1,0:T(8,128)(2,1)S(1)}, bf16[64,32,128]{2,1,0:T(8,128)(2,1)S(1)}, u32[]{:S(2)}, u32[]{:S(2)}) collective-permute-start(bf16[64,32,128]{2,1,0:T(8,128)(2,1)S(1)} %get-tuple-element.37.refs_0_.own_ref), channel_id=1, source_target_pairs={{0,2},{1,3},{2,4},{3,5},{4,6},{5,7},{6,0},{7,1},{8,10},{9,11},{10,... | collective-permute-start | bytes 1572872 | tf_op jit(solution)/shard_map/ppermute | solution.py:321
  60.0 3.1 %collective-permute-start.1 = (bf16[64,32,128]{2,1,0:T(8,128)(2,1)S(1)}, bf16[64,32,128]{2,1,0:T(8,128)(2,1)S(1)}, u32[]{:S(2)}, u32[]{:S(2)}) collective-permute-start(bf16[64,32,128]{2,1,0:T(8,128)(2,1)S(1)} %get-tuple-element.37.refs_0_.own_ref), channel_id=1, source_target_pairs={{0,6},{1,7},{2,0},{3,1},{4,2},{5,3},{6,4},{7,5},{8,14},{9,15},{10,... | collective-permute-start | bytes 1572872 | tf_op jit(solution)/shard_map/ppermute | solution.py:321
  63.1 8.0 %collective-permute-done.in_ref.refs_1_.left_ref = bf16[64,32,128]{2,1,0:T(8,128)(2,1)S(1)} collective-permute-done((bf16[64,32,128]{2,1,0:T(8,128)(2,1)S(1)}, bf16[64,32,128]{2,1,0:T(8,128)(2,1)S(1)}, u32[]{:S(2)}, u32[]{:S(2)}) %collective-permute-start) | collective-permute-done | bytes 524320 | tf_op jit(solution)/shard_map/ppermute | solution.py:321
  74.6 4.8 %collective-permute-start.4 = (bf16[192,32,128]{2,1,0:T(8,128)(2,1)}, bf16[192,32,128]{2,1,0:T(8,128)(2,1)}, u32[]{:S(2)}, u32[]{:S(2)}) collective-permute-start(bf16[192,32,128]{2,1,0:T(8,128)(2,1)} %shard_map.159), channel_id=1, source_target_pairs={{0,1},{1,0},{2,3},{3,2},{4,5},{5,4},{6,7},{7,6},{8,9},{9,8},{10,11... | collective-permute-start | bytes 4718600 | tf_op jit(solution)/shard_map/ppermute | solution.py:325
  79.4 6.2 %all-to-all-start.3 = ((bf16[8,64,8,128]{3,2,1,0:T(8,128)(2,1)}), bf16[8,64,8,128]{3,2,1,0:T(8,128)(2,1)S(1)}, u32[]{:S(2)}, u32[]{:S(2)}) async-start(bf16[8,64,8,128]{3,2,1,0:T(8,128)(2,1)} %get-tuple-element.48), calls=%async_computation.3 | async-start | bytes 2097152 | tf_op jit(solution)/shard_map/all_to_all | solution.py:375
  87.8 4.4 %collective-permute-start.3 = (bf16[32,32,128]{2,1,0:T(8,128)(2,1)S(1)}, bf16[32,32,128]{2,1,0:T(8,128)(2,1)S(1)}, u32[]{:S(2)}, u32[]{:S(2)}) collective-permute-start(bf16[32,32,128]{2,1,0:T(8,128)(2,1)S(1)} %shard_map.157), channel_id=1, source_target_pairs={{0,6},{1,7},{2,0},{3,1},{4,2},{5,3},{6,4},{7,5},{8,14},{9,15},{10,... | collective-permute-start | bytes 786440 | tf_op jit(solution)/shard_map/ppermute | solution.py:321
  92.2 4.1 %collective-permute-done.2.refs_0_ = bf16[32,32,128]{2,1,0:T(8,128)(2,1)S(1)} collective-permute-done((bf16[32,32,128]{2,1,0:T(8,128)(2,1)S(1)}, bf16[32,32,128]{2,1,0:T(8,128)(2,1)S(1)}, u32[]{:S(2)}, u32[]{:S(2)}) %collective-permute-start.2) | collective-permute-done | bytes 262176 | tf_op jit(solution)/shard_map/ppermute | solution.py:321
  97.3 3.3 %collective-permute-start.5 = (bf16[64,32,128]{2,1,0:T(8,128)(2,1)S(1)}, bf16[64,32,128]{2,1,0:T(8,128)(2,1)S(1)}, u32[]{:S(2)}, u32[]{:S(2)}) collective-permute-start(bf16[64,32,128]{2,1,0:T(8,128)(2,1)S(1)} %shard_map.158.across_ref), channel_id=1, source_target_pairs={{0,1},{1,0},{2,3},{3,2},{4,5},{5,4},{6,7},{7,6},{8,9},{9,8},{10,11... | collective-permute-start | bytes 1572872 | tf_op jit(solution)/shard_map/ppermute | solution.py:325
  103.0 3.2 %shard_map.163 = (bf16[768,128]{1,0:T(8,128)(2,1)S(1)}, bf16[768,128]{1,0:T(8,128)(2,1)S(1)}, bf16[768,128]{1,0:T(8,128)(2,1)S(1)}, bf16[768,128]{1,0:T(8,128)(2,1)S(1)}) custom-call(s32[1]{0:T(128)} %bitcast.m_ref, bf16[64,32,128]{2,1,0:T(8,128)(2,1)S(1)} %get-tuple-element.37.refs_0_.own_ref, ...), custom_call_target="tpu_custom_call" | custom-call | tf_op jit(solution)/shard_map/pallas_call | solution.py:56
  106.1 3.3 %collective-permute-start.10 = (bf16[768,128]{1,0:T(8,128)(2,1)S(1)}, bf16[768,128]{1,0:T(8,128)(2,1)S(1)}, u32[]{:S(2)}, u32[]{:S(2)}) collective-permute-start(bf16[768,128]{1,0:T(8,128)(2,1)S(1)} %get-tuple-element.44), channel_id=1, source_target_pairs={{0,2},{1,3},{2,4},{3,5},{4,6},{5,7},{6,0},{7,1},{8,10},{9,11},{10,... | collective-permute-start | bytes 589832 | tf_op jit(solution)/shard_map/ppermute | solution.py:321
  109.4 4.0 %collective-permute-start.11 = (bf16[768,128]{1,0:T(8,128)(2,1)S(1)}, bf16[768,128]{1,0:T(8,128)(2,1)S(1)}, u32[]{:S(2)}, u32[]{:S(2)}) collective-permute-start(bf16[768,128]{1,0:T(8,128)(2,1)S(1)} %get-tuple-element.45), channel_id=1, source_target_pairs={{0,6},{1,7},{2,0},{3,1},{4,2},{5,3},{6,4},{7,5},{8,14},{9,15},{10,... | collective-permute-start | bytes 589832 | tf_op jit(solution)/shard_map/ppermute | solution.py:321
  117.3 5.3 %collective-permute-done.12.refs_3_.far_ref = bf16[768,128]{1,0:T(8,128)(2,1)S(1)} collective-permute-done((bf16[768,128]{1,0:T(8,128)(2,1)S(1)}, bf16[768,128]{1,0:T(8,128)(2,1)S(1)}, u32[]{:S(2)}, u32[]{:S(2)}) %collective-permute-start.12) | collective-permute-done | bytes 196640 | tf_op jit(solution)/shard_map/ppermute | solution.py:321
  122.6 3.4 %collective-permute-start.13 = (bf16[4,640,128]{2,1,0:T(8,128)(2,1)S(1)}, bf16[4,640,128]{2,1,0:T(8,128)(2,1)S(1)}, u32[]{:S(2)}, u32[]{:S(2)}) collective-permute-start(bf16[4,640,128]{2,1,0:T(8,128)(2,1)S(1)} %shard_map.164), channel_id=1, source_target_pairs={{0,1},{1,0},{2,3},{3,2},{4,5},{5,4},{6,7},{7,6},{8,9},{9,8},{10,11... | collective-permute-start | bytes 1966088 | tf_op jit(solution)/shard_map/ppermute | solution.py:325
  129.3 12.6 %all-to-all-start.2 = ((bf16[64,32,128]{2,1,0:T(8,128)(2,1)}), bf16[64,32,128]{2,1,0:T(8,128)(2,1)S(1)}, u32[]{:S(2)}, u32[]{:S(2)}) async-start(bf16[64,32,128]{2,1,0:T(8,128)(2,1)} %shard_map.165), calls=%async_computation.2 | async-start | bytes 1048576 | tf_op jit(solution)/shard_map/all_to_all | solution.py:390
  143.5 3.3 %collective-permute-start.14 = (bf16[320,128]{1,0:T(8,128)(2,1)S(1)}, bf16[320,128]{1,0:T(8,128)(2,1)S(1)}, u32[]{:S(2)}, u32[]{:S(2)}) collective-permute-start(bf16[320,128]{1,0:T(8,128)(2,1)S(1)} %get-tuple-element.50), channel_id=1, source_target_pairs={{0,2},{1,3},{2,4},{3,5},{4,6},{5,7},{6,0},{7,1},{8,10},{9,11},{10,... | collective-permute-start | bytes 245768 | tf_op jit(solution)/shard_map/ppermute | solution.py:321
  146.7 3.2 %collective-permute-start.15 = (bf16[320,128]{1,0:T(8,128)(2,1)S(1)}, bf16[320,128]{1,0:T(8,128)(2,1)S(1)}, u32[]{:S(2)}, u32[]{:S(2)}) collective-permute-start(bf16[320,128]{1,0:T(8,128)(2,1)S(1)} %get-tuple-element.51), channel_id=1, source_target_pairs={{0,6},{1,7},{2,0},{3,1},{4,2},{5,3},{6,4},{7,5},{8,14},{9,15},{10,... | collective-permute-start | bytes 245768 | tf_op jit(solution)/shard_map/ppermute | solution.py:321
  152.4 4.5 %collective-permute-done.16.refs_3_.far_ref = bf16[320,128]{1,0:T(8,128)(2,1)S(1)} collective-permute-done((bf16[320,128]{1,0:T(8,128)(2,1)S(1)}, bf16[320,128]{1,0:T(8,128)(2,1)S(1)}, u32[]{:S(2)}, u32[]{:S(2)}) %collective-permute-start.16) | collective-permute-done | bytes 81952 | tf_op jit(solution)/shard_map/ppermute | solution.py:321
  157.0 4.0 %collective-permute-start.17 = (bf16[4,192,128]{2,1,0:T(8,128)(2,1)S(1)}, bf16[4,192,128]{2,1,0:T(8,128)(2,1)S(1)}, u32[]{:S(2)}, u32[]{:S(2)}) collective-permute-start(bf16[4,192,128]{2,1,0:T(8,128)(2,1)S(1)} %shard_map.168), channel_id=1, source_target_pairs={{0,1},{1,0},{2,3},{3,2},{4,5},{5,4},{6,7},{7,6},{8,9},{9,8},{10,11... | collective-permute-start | bytes 589832 | tf_op jit(solution)/shard_map/ppermute | solution.py:325
  (46 shorter events, 36.7 us)
Async XLA Ops:
  3.2 39.9 %all-to-all-start = ((bf16[64,40,128]{2,1,0:T(8,128)(2,1)}), bf16[64,40,128]{2,1,0:T(8,128)(2,1)S(1)}, u32[]{:S(2)}, u32[]{:S(2)}) async-start(bf16[64,40,128]{2,1,0:T(8,128)(2,1)} %get-tuple-element.36), calls=%async_computation | async-start | bytes 1310720 | tf_op jit(solution)/shard_map/all_to_all | solution.py:352
  22.4 4.2 %collective-permute-start.6 = (bf16[4,8,48,128]{3,2,1,0:T(8,128)(2,1)S(1)}, bf16[4,8,48,128]{3,2,1,0:T(8,128)(2,1)S(1)}, u32[]{:S(2)}, u32[]{:S(2)}) collective-permute-start(bf16[4,8,48,128]{3,2,1,0:T(8,128)(2,1)S(1)} %get-tuple-element.39), channel_id=1, source_target_pairs={{0,1},{1,0},{2,3},{3,2},{4,5},{5,4},{6,7},{7,6},{8,9},{9,8},{10,11... | collective-permute-start | bytes 1179656 | tf_op jit(solution)/shard_map/ppermute | solution.py:325
  26.6 10.0 %collective-permute-start.7 = (bf16[16,48,128]{2,1,0:T(8,128)(2,1)S(1)}, bf16[16,48,128]{2,1,0:T(8,128)(2,1)S(1)}, u32[]{:S(2)}, u32[]{:S(2)}) collective-permute-start(bf16[16,48,128]{2,1,0:T(8,128)(2,1)S(1)} %get-tuple-element.40), channel_id=1, source_target_pairs={{0,2},{1,3},{2,4},{3,5},{4,6},{5,7},{6,0},{7,1},{8,10},{9,11},{10,... | collective-permute-start | bytes 589832 | tf_op jit(solution)/shard_map/ppermute | solution.py:321
  29.8 7.7 %collective-permute-start.8 = (bf16[16,48,128]{2,1,0:T(8,128)(2,1)S(1)}, bf16[16,48,128]{2,1,0:T(8,128)(2,1)S(1)}, u32[]{:S(2)}, u32[]{:S(2)}) collective-permute-start(bf16[16,48,128]{2,1,0:T(8,128)(2,1)S(1)} %get-tuple-element.41), channel_id=1, source_target_pairs={{0,6},{1,7},{2,0},{3,1},{4,2},{5,3},{6,4},{7,5},{8,14},{9,15},{10,... | collective-permute-start | bytes 589832 | tf_op jit(solution)/shard_map/ppermute | solution.py:321
  33.1 8.9 %collective-permute-start.9 = (bf16[16,48,128]{2,1,0:T(8,128)(2,1)S(1)}, bf16[16,48,128]{2,1,0:T(8,128)(2,1)S(1)}, u32[]{:S(2)}, u32[]{:S(2)}) collective-permute-start(bf16[16,48,128]{2,1,0:T(8,128)(2,1)S(1)} %get-tuple-element.42), channel_id=1, source_target_pairs={{0,4},{1,5},{2,6},{3,7},{4,0},{5,1},{6,2},{7,3},{8,12},{9,13},{10,... | collective-permute-start | bytes 589832 | tf_op jit(solution)/shard_map/ppermute | solution.py:321
  43.0 36.4 %all-to-all-start.1 = ((bf16[64,48,128]{2,1,0:T(8,128)(2,1)}), bf16[64,48,128]{2,1,0:T(8,128)(2,1)S(1)}, u32[]{:S(2)}, u32[]{:S(2)}) async-start(bf16[64,48,128]{2,1,0:T(8,128)(2,1)} %shard_map.162), calls=%async_computation.1 | async-start | bytes 1572864 | tf_op jit(solution)/shard_map/all_to_all | solution.py:363
  56.6 14.5 %collective-permute-start = (bf16[64,32,128]{2,1,0:T(8,128)(2,1)S(1)}, bf16[64,32,128]{2,1,0:T(8,128)(2,1)S(1)}, u32[]{:S(2)}, u32[]{:S(2)}) collective-permute-start(bf16[64,32,128]{2,1,0:T(8,128)(2,1)S(1)} %get-tuple-element.37.refs_0_.own_ref), channel_id=1, source_target_pairs={{0,2},{1,3},{2,4},{3,5},{4,6},{5,7},{6,0},{7,1},{8,10},{9,11},{10,... | collective-permute-start | bytes 1572872 | tf_op jit(solution)/shard_map/ppermute | solution.py:321
  60.0 13.3 %collective-permute-start.1 = (bf16[64,32,128]{2,1,0:T(8,128)(2,1)S(1)}, bf16[64,32,128]{2,1,0:T(8,128)(2,1)S(1)}, u32[]{:S(2)}, u32[]{:S(2)}) collective-permute-start(bf16[64,32,128]{2,1,0:T(8,128)(2,1)S(1)} %get-tuple-element.37.refs_0_.own_ref), channel_id=1, source_target_pairs={{0,6},{1,7},{2,0},{3,1},{4,2},{5,3},{6,4},{7,5},{8,14},{9,15},{10,... | collective-permute-start | bytes 1572872 | tf_op jit(solution)/shard_map/ppermute | solution.py:321
  73.3 14.5 %copy-start = (bf16[64,32,128]{2,1,0:T(8,128)(2,1)}, bf16[64,32,128]{2,1,0:T(8,128)(2,1)S(1)}, u32[]{:S(2)}) copy-start(bf16[64,32,128]{2,1,0:T(8,128)(2,1)S(1)} %collective-permute-done.1.in_ref.refs_2_.right_ref) | copy-start | bytes 1572868
  74.6 27.6 %collective-permute-start.4 = (bf16[192,32,128]{2,1,0:T(8,128)(2,1)}, bf16[192,32,128]{2,1,0:T(8,128)(2,1)}, u32[]{:S(2)}, u32[]{:S(2)}) collective-permute-start(bf16[192,32,128]{2,1,0:T(8,128)(2,1)} %shard_map.159), channel_id=1, source_target_pairs={{0,1},{1,0},{2,3},{3,2},{4,5},{5,4},{6,7},{7,6},{8,9},{9,8},{10,11... | collective-permute-start | bytes 4718600 | tf_op jit(solution)/shard_map/ppermute | solution.py:325
  79.4 49.9 %all-to-all-start.3 = ((bf16[8,64,8,128]{3,2,1,0:T(8,128)(2,1)}), bf16[8,64,8,128]{3,2,1,0:T(8,128)(2,1)S(1)}, u32[]{:S(2)}, u32[]{:S(2)}) async-start(bf16[8,64,8,128]{3,2,1,0:T(8,128)(2,1)} %get-tuple-element.48), calls=%async_computation.3 | async-start | bytes 2097152 | tf_op jit(solution)/shard_map/all_to_all | solution.py:375
  85.6 10.7 %collective-permute-start.2 = (bf16[32,32,128]{2,1,0:T(8,128)(2,1)S(1)}, bf16[32,32,128]{2,1,0:T(8,128)(2,1)S(1)}, u32[]{:S(2)}, u32[]{:S(2)}) collective-permute-start(bf16[32,32,128]{2,1,0:T(8,128)(2,1)S(1)} %shard_map.156), channel_id=1, source_target_pairs={{0,2},{1,3},{2,4},{3,5},{4,6},{5,7},{6,0},{7,1},{8,10},{9,11},{10,... | collective-permute-start | bytes 786440 | tf_op jit(solution)/shard_map/ppermute | solution.py:321
  87.8 9.5 %collective-permute-start.3 = (bf16[32,32,128]{2,1,0:T(8,128)(2,1)S(1)}, bf16[32,32,128]{2,1,0:T(8,128)(2,1)S(1)}, u32[]{:S(2)}, u32[]{:S(2)}) collective-permute-start(bf16[32,32,128]{2,1,0:T(8,128)(2,1)S(1)} %shard_map.157), channel_id=1, source_target_pairs={{0,6},{1,7},{2,0},{3,1},{4,2},{5,3},{6,4},{7,5},{8,14},{9,15},{10,... | collective-permute-start | bytes 786440 | tf_op jit(solution)/shard_map/ppermute | solution.py:321
  97.3 4.9 %copy-start.1 = (bf16[64,32,128]{2,1,0:T(8,128)(2,1)}, bf16[64,32,128]{2,1,0:T(8,128)(2,1)S(1)}, u32[]{:S(2)}) copy-start(bf16[64,32,128]{2,1,0:T(8,128)(2,1)S(1)} %shard_map.158.across_ref) | copy-start | bytes 1572868
  97.3 4.9 %collective-permute-start.5 = (bf16[64,32,128]{2,1,0:T(8,128)(2,1)S(1)}, bf16[64,32,128]{2,1,0:T(8,128)(2,1)S(1)}, u32[]{:S(2)}, u32[]{:S(2)}) collective-permute-start(bf16[64,32,128]{2,1,0:T(8,128)(2,1)S(1)} %shard_map.158.across_ref), channel_id=1, source_target_pairs={{0,1},{1,0},{2,3},{3,2},{4,5},{5,4},{6,7},{7,6},{8,9},{9,8},{10,11... | collective-permute-start | bytes 1572872 | tf_op jit(solution)/shard_map/ppermute | solution.py:325
  106.1 10.4 %collective-permute-start.10 = (bf16[768,128]{1,0:T(8,128)(2,1)S(1)}, bf16[768,128]{1,0:T(8,128)(2,1)S(1)}, u32[]{:S(2)}, u32[]{:S(2)}) collective-permute-start(bf16[768,128]{1,0:T(8,128)(2,1)S(1)} %get-tuple-element.44), channel_id=1, source_target_pairs={{0,2},{1,3},{2,4},{3,5},{4,6},{5,7},{6,0},{7,1},{8,10},{9,11},{10,... | collective-permute-start | bytes 589832 | tf_op jit(solution)/shard_map/ppermute | solution.py:321
  109.4 7.8 %collective-permute-start.11 = (bf16[768,128]{1,0:T(8,128)(2,1)S(1)}, bf16[768,128]{1,0:T(8,128)(2,1)S(1)}, u32[]{:S(2)}, u32[]{:S(2)}) collective-permute-start(bf16[768,128]{1,0:T(8,128)(2,1)S(1)} %get-tuple-element.45), channel_id=1, source_target_pairs={{0,6},{1,7},{2,0},{3,1},{4,2},{5,3},{6,4},{7,5},{8,14},{9,15},{10,... | collective-permute-start | bytes 589832 | tf_op jit(solution)/shard_map/ppermute | solution.py:321
  113.4 9.2 %collective-permute-start.12 = (bf16[768,128]{1,0:T(8,128)(2,1)S(1)}, bf16[768,128]{1,0:T(8,128)(2,1)S(1)}, u32[]{:S(2)}, u32[]{:S(2)}) collective-permute-start(bf16[768,128]{1,0:T(8,128)(2,1)S(1)} %get-tuple-element.46), channel_id=1, source_target_pairs={{0,4},{1,5},{2,6},{3,7},{4,0},{5,1},{6,2},{7,3},{8,12},{9,13},{10,... | collective-permute-start | bytes 589832 | tf_op jit(solution)/shard_map/ppermute | solution.py:321
  122.6 5.1 %collective-permute-start.13 = (bf16[4,640,128]{2,1,0:T(8,128)(2,1)S(1)}, bf16[4,640,128]{2,1,0:T(8,128)(2,1)S(1)}, u32[]{:S(2)}, u32[]{:S(2)}) collective-permute-start(bf16[4,640,128]{2,1,0:T(8,128)(2,1)S(1)} %shard_map.164), channel_id=1, source_target_pairs={{0,1},{1,0},{2,3},{3,2},{4,5},{5,4},{6,7},{7,6},{8,9},{9,8},{10,11... | collective-permute-start | bytes 1966088 | tf_op jit(solution)/shard_map/ppermute | solution.py:325
  129.3 35.6 %all-to-all-start.2 = ((bf16[64,32,128]{2,1,0:T(8,128)(2,1)}), bf16[64,32,128]{2,1,0:T(8,128)(2,1)S(1)}, u32[]{:S(2)}, u32[]{:S(2)}) async-start(bf16[64,32,128]{2,1,0:T(8,128)(2,1)} %shard_map.165), calls=%async_computation.2 | async-start | bytes 1048576 | tf_op jit(solution)/shard_map/all_to_all | solution.py:390
  143.5 9.0 %collective-permute-start.14 = (bf16[320,128]{1,0:T(8,128)(2,1)S(1)}, bf16[320,128]{1,0:T(8,128)(2,1)S(1)}, u32[]{:S(2)}, u32[]{:S(2)}) collective-permute-start(bf16[320,128]{1,0:T(8,128)(2,1)S(1)} %get-tuple-element.50), channel_id=1, source_target_pairs={{0,2},{1,3},{2,4},{3,5},{4,6},{5,7},{6,0},{7,1},{8,10},{9,11},{10,... | collective-permute-start | bytes 245768 | tf_op jit(solution)/shard_map/ppermute | solution.py:321
  146.7 5.7 %collective-permute-start.15 = (bf16[320,128]{1,0:T(8,128)(2,1)S(1)}, bf16[320,128]{1,0:T(8,128)(2,1)S(1)}, u32[]{:S(2)}, u32[]{:S(2)}) collective-permute-start(bf16[320,128]{1,0:T(8,128)(2,1)S(1)} %get-tuple-element.51), channel_id=1, source_target_pairs={{0,6},{1,7},{2,0},{3,1},{4,2},{5,3},{6,4},{7,5},{8,14},{9,15},{10,... | collective-permute-start | bytes 245768 | tf_op jit(solution)/shard_map/ppermute | solution.py:321
  150.0 7.0 %collective-permute-start.16 = (bf16[320,128]{1,0:T(8,128)(2,1)S(1)}, bf16[320,128]{1,0:T(8,128)(2,1)S(1)}, u32[]{:S(2)}, u32[]{:S(2)}) collective-permute-start(bf16[320,128]{1,0:T(8,128)(2,1)S(1)} %get-tuple-element.52), channel_id=1, source_target_pairs={{0,4},{1,5},{2,6},{3,7},{4,0},{5,1},{6,2},{7,3},{8,12},{9,13},{10,... | collective-permute-start | bytes 245768 | tf_op jit(solution)/shard_map/ppermute | solution.py:321
  157.0 7.5 %collective-permute-start.17 = (bf16[4,192,128]{2,1,0:T(8,128)(2,1)S(1)}, bf16[4,192,128]{2,1,0:T(8,128)(2,1)S(1)}, u32[]{:S(2)}, u32[]{:S(2)}) collective-permute-start(bf16[4,192,128]{2,1,0:T(8,128)(2,1)S(1)} %shard_map.168), channel_id=1, source_target_pairs={{0,1},{1,0},{2,3},{3,2},{4,5},{5,4},{6,7},{7,6},{8,9},{9,8},{10,11... | collective-permute-start | bytes 589832 | tf_op jit(solution)/shard_map/ppermute | solution.py:325
  (1 other events, 0.8 us)

commit v3 on v2

--- a/solution.py
+++ b/solution.py
@@ -102,16 +102,15 @@
     send_ref[:, 16:32, :] = rows[:, LANES:].reshape(E, CAP, LANES)
 
 
-def split_body(got_ref, own_ref, parts_ref):
+def own_rows_body(got_ref, own_ref, part_ref):
     own_ref[...] = got_ref[:, 0:32, :]
-    parts = got_ref[:, 32:40, :]
+    part_ref[...] = got_ref[:, 32:40, :]
+
+
+def spread_body(part_ref, parts_ref):
+    parts = part_ref[...]
     for y in range(PARTS):
         parts_ref[y] = parts
-
-
-def join_body(parts_ref, out_ref):
-    pieces = [parts_ref[p].astype(f32) for p in range(6)]
-    out_ref[...] = jnp.concatenate(pieces, axis=1).astype(bf16)
 
 
 STEPS = (0, 2, -2, 4)
@@ -141,19 +140,17 @@
 
 def repack_body(keep_ref, swapped_ref, *out_refs):
     for i, out_ref in enumerate(out_refs):
-        out_ref[0:8] = keep_ref[i + 1]
-        out_ref[8:16] = swapped_ref[i + 1]
-
-
-def assemble_body(m_ref, keep_ref, swapped_ref, left_ref, right_ref, far_ref, out_ref):
+        out_ref[0:8] = keep_ref[i]
+        out_ref[8:16] = swapped_ref[i]
+
+
+def assemble_body(m_ref, own_ref, left_ref, right_ref, far_ref, out_ref):
     m = m_ref[0]
 
     def put(t, x):
         out_ref[pl.ds(pl.multiple_of(t * 8, 8), 8)] = x
 
-    put(m, keep_ref[0])
-    put(m ^ 1, swapped_ref[0])
-    for step, ref in zip(STEPS[1:], (left_ref, right_ref, far_ref)):
+    for step, ref in zip(STEPS, (own_ref, left_ref, right_ref, far_ref)):
         t = (m - step) & 7
         put(t, ref[0:8])
         put(t ^ 1, ref[8:16])
@@ -197,7 +194,9 @@
         ref[n + LANES : n + 2 * LANES, :] = down_block(w_ref, (m + step) ^ 1)
 
 
-def common_hidden_body(m_ref, normed_ref, w_ref, *to_refs):
+def common_hidden_body(m_ref, normed_ref, parts_ref, w_ref, *to_refs):
+    pieces = [parts_ref[p].astype(f32) for p in range(6)]
+    w_ref[...] = jnp.concatenate(pieces, axis=1).astype(bf16)
     weights = w_ref[:, 0:32, :].reshape(D, LANES)
     write_messages(m_ref[0], packed_hidden(dot(normed_ref[...], weights)), w_ref, to_refs)
 
@@ -347,22 +346,27 @@
     gain = norm_gain.reshape(1, W32)
 
     send, normed, pos = call(
-        dispatch_body, (shape(64, 40, LANES), shape(TOK, D), shape(E, TOK, dtype=f32)), 7, 1, far=range(8), keep=(2,)
+        dispatch_body, (shape(64, 40, LANES), shape(TOK, D), shape(E, TOK, dtype=f32)), 7, 1, far=range(8), keep=()
     )(m, prompt, ids, gain, common_gate_train, common_up_train, common_down_train)
     got = lax.all_to_all(send, "fs", 0, 0, tiled=True)
 
     half = shape(4, 8, 48, LANES)
-    kept, to_partner = call(prepare_body, (half, half), 5, 1, far=range(8))(m, gain, gate_train, up_train, down_train)
+    kept, to_partner = call(prepare_body, (half, half), 5, 1, far=(1,))(
+        m, gain, gate_train, up_train, down_train
+    )
     swapped = swap(to_partner, 1)
     message = shape(16, 48, LANES)
-    to_right, to_left, to_far = call(repack_body, (message, message, message), 2)(kept, swapped)
+    w_own, to_right, to_left, to_far = call(repack_body, (message,) * 4, 2)(kept, swapped)
     w_far = shift(to_far, 4)
     w_left = shift(to_right, 2)
     w_right = shift(to_left, -2)
-    spread = call(assemble_body, shape(64, 48, LANES), 6, 1, keep=())(m, kept, swapped, w_left, w_right, w_far)
+    spread = call(assemble_body, shape(64, 48, LANES), 5, 1, keep=())(
+        m, w_own, w_left, w_right, w_far
+    )
     weights = lax.all_to_all(spread, "fs", 0, 0, tiled=True)
 
-    own, common_send = call(split_body, (shape(64, 32, LANES), shape(8, 64, 8, LANES)), 1, keep=(0,))(got)
+    own, part = call(own_rows_body, (shape(64, 32, LANES), shape(64, 8, LANES)), 1, keep=(0,))(got)
+    common_send = call(spread_body, shape(8, 64, 8, LANES), 1, far=(0,), keep=())(part)
     left = shift(own, 2)
     right = shift(own, -2)
     far_a = shift(call(part_body(0), shape(32, 32, LANES), 1)(left), 2)
@@ -373,13 +377,14 @@
     far = swap(across, 1)
 
     common = lax.all_to_all(common_send, "fs", 0, 0, axis_index_groups=COLUMNS, tiled=True)
-    common = call(join_body, shape(64, 48, LANES), 1)(common)
-
-    mix_hi, mix_lo = call(mixing_body, (shape(TOK, ROWS), shape(TOK, ROWS)), 3, far=(1, 2))(pos, ids, route_weights)
+
+    mix_hi, mix_lo = call(mixing_body, (shape(TOK, ROWS), shape(TOK, ROWS)), 3, far=(0, 1, 2), keep=())(
+        pos, ids, route_weights
+    )
 
     message = shape(512 + 2 * LANES, LANES)
     mine, to_right, to_left, to_far = call(
-        hidden_body, (message,) * 4, 8, 1, [pltpu.VMEM((ROWS, LANES), f32)], far=(3, 4, 5, 6)
+        hidden_body, (message,) * 4, 8, 1, [pltpu.VMEM((ROWS, LANES), f32)], far=(1, 5)
     )(m, own, left, right, across, three, far, weights)
     h_far = shift(to_far, 4)
     h_left = shift(to_right, 2)
@@ -390,13 +395,17 @@
     returned = lax.all_to_all(expert_out, "fs", 0, 0, tiled=True)
 
     message = shape(64 + 2 * LANES, LANES)
-    mine, to_right, to_left, to_far = call(common_hidden_body, (message,) * 4, 3, 1, far=(1,))(m, normed, common)
+    common, mine, to_right, to_left, to_far = call(
+        common_hidden_body, (shape(64, 48, LANES),) + (message,) * 4, 3, 1, far=(1,)
+    )(m, normed, common)
     c_far = shift(to_far, 4)
     c_left = shift(to_right, 2)
     c_right = shift(to_left, -2)
     pair = call(pair_body, shape(4, 64 + LANES, LANES), 4)(mine, c_left, c_right, c_far)
     partner = swap(pair, 1)
-    common_out = call(common_down_body, shape(TOK, COLS, dtype=f32), 5)(mine, c_left, c_right, c_far, partner)
+    common_out = call(common_down_body, shape(TOK, COLS, dtype=f32), 5)(
+        mine, c_left, c_right, c_far, partner
+    )
 
     serve = tuple(shape(U, D) for _ in range(3))
     gate_serve, up_serve, down_serve = call(serve_body, serve, 1, keep=())(weights)

time: 167 us -> 168 us (level)
  no operation moved by 1% of the time
where the time goes in v3:
time: 168 us; the launch traced here: 167 us
  starting transfers between devices  109 us (65%)
  waiting for transfers between devices  35.9 us (21%)
  Pallas kernels  20.9 us (12%)
    ppermute x13, starting transfers between devices, shift(): return lax.ppermute(x, 'tp', [(i, (i + step) % N_TP) for i in range(N_TP)])  42.2 us
    ppermute x13, waiting for transfers between devices, shift(): return lax.ppermute(x, 'tp', [(i, (i + step) % N_TP) for i in range(N_TP)])  31.3 us
    pallas_call x20, Pallas kernels, run(): return fn(*placed)  20.9 us
    ppermute x5, starting transfers between devices, swap(): return lax.ppermute(x, 'tp', [(i, i ^ k) for i in range(N_TP)])  18.4 us
    all_to_all x1, starting transfers between devices, local(): got = lax.all_to_all(send, 'fs', 0, 0, tiled=True)  17.1 us
    all_to_all x1, starting transfers between devices, local(): returned = lax.all_to_all(expert_out, 'fs', 0, 0, tiled=True)  12.6 us
    all_to_all x1, starting transfers between devices, local(): weights = lax.all_to_all(spread, 'fs', 0, 0, tiled=True)  12.4 us
    all_to_all x1, starting transfers between devices, local(): lax.all_to_all(common_send, 'fs', 0, 0, axis_index_groups=COLUMNS, tiled=...  6.2 us
  transfers between devices with their start and end apart: 22, of which 12 were waited for; matrix products, arithmetic and copies ran while one was open for 0% of the time, Pallas kernels for 10%

profile of v3, /device:TPU:1, one launch (start us, length us, event | category | flops | bytes accessed | tf_op | source)
XLA Modules:
  0.0 166.7 jit_solution(10924615100310710832)
XLA Ops:
  3.3 17.1 %all-to-all-start = ((bf16[64,40,128]{2,1,0:T(8,128)(2,1)}), bf16[64,40,128]{2,1,0:T(8,128)(2,1)S(1)}, u32[]{:S(2)}, u32[]{:S(2)}) async-start(bf16[64,40,128]{2,1,0:T(8,128)(2,1)} %get-tuple-element.38), calls=%async_computation | async-start | bytes 1310720 | tf_op jit(solution)/shard_map/all_to_all | solution.py:351
  26.1 3.1 %collective-permute-start.7 = (bf16[16,48,128]{2,1,0:T(8,128)(2,1)S(1)}, bf16[16,48,128]{2,1,0:T(8,128)(2,1)S(1)}, u32[]{:S(2)}, u32[]{:S(2)}) collective-permute-start(bf16[16,48,128]{2,1,0:T(8,128)(2,1)S(1)} %get-tuple-element.43), channel_id=1, source_target_pairs={{0,2},{1,3},{2,4},{3,5},{4,6},{5,7},{6,0},{7,1},{8,10},{9,11},{10,... | collective-permute-start | bytes 589832 | tf_op jit(solution)/shard_map/ppermute | solution.py:320
  29.3 3.4 %collective-permute-start.8 = (bf16[16,48,128]{2,1,0:T(8,128)(2,1)S(1)}, bf16[16,48,128]{2,1,0:T(8,128)(2,1)S(1)}, u32[]{:S(2)}, u32[]{:S(2)}) collective-permute-start(bf16[16,48,128]{2,1,0:T(8,128)(2,1)S(1)} %get-tuple-element.44), channel_id=1, source_target_pairs={{0,6},{1,7},{2,0},{3,1},{4,2},{5,3},{6,4},{7,5},{8,14},{9,15},{10,... | collective-permute-start | bytes 589832 | tf_op jit(solution)/shard_map/ppermute | solution.py:320
  32.6 3.4 %collective-permute-start.9 = (bf16[16,48,128]{2,1,0:T(8,128)(2,1)S(1)}, bf16[16,48,128]{2,1,0:T(8,128)(2,1)S(1)}, u32[]{:S(2)}, u32[]{:S(2)}) collective-permute-start(bf16[16,48,128]{2,1,0:T(8,128)(2,1)S(1)} %get-tuple-element.45), channel_id=1, source_target_pairs={{0,4},{1,5},{2,6},{3,7},{4,0},{5,1},{6,2},{7,3},{8,12},{9,13},{10,... | collective-permute-start | bytes 589832 | tf_op jit(solution)/shard_map/ppermute | solution.py:320
  36.9 4.6 %collective-permute-done.9.far_ref = bf16[16,48,128]{2,1,0:T(8,128)(2,1)S(1)} collective-permute-done((bf16[16,48,128]{2,1,0:T(8,128)(2,1)S(1)}, bf16[16,48,128]{2,1,0:T(8,128)(2,1)S(1)}, u32[]{:S(2)}, u32[]{:S(2)}) %collective-permute-start.9) | collective-permute-done | bytes 196640 | tf_op jit(solution)/shard_map/ppermute | solution.py:320
  42.5 12.4 %all-to-all-start.1 = ((bf16[64,48,128]{2,1,0:T(8,128)(2,1)}), bf16[64,48,128]{2,1,0:T(8,128)(2,1)S(1)}, u32[]{:S(2)}, u32[]{:S(2)}) async-start(bf16[64,48,128]{2,1,0:T(8,128)(2,1)} %shard_map.162), calls=%async_computation.1 | async-start | bytes 1572864 | tf_op jit(solution)/shard_map/all_to_all | solution.py:366
  55.7 3.3 %collective-permute-start = (bf16[64,32,128]{2,1,0:T(8,128)(2,1)S(1)}, bf16[64,32,128]{2,1,0:T(8,128)(2,1)S(1)}, u32[]{:S(2)}, u32[]{:S(2)}) collective-permute-start(bf16[64,32,128]{2,1,0:T(8,128)(2,1)S(1)} %get-tuple-element.39.refs_0_.own_ref), channel_id=1, source_target_pairs={{0,2},{1,3},{2,4},{3,5},{4,6},{5,7},{6,0},{7,1},{8,10},{9,11},{10,... | collective-permute-start | bytes 1572872 | tf_op jit(solution)/shard_map/ppermute | solution.py:320
  59.0 3.1 %collective-permute-start.1 = (bf16[64,32,128]{2,1,0:T(8,128)(2,1)S(1)}, bf16[64,32,128]{2,1,0:T(8,128)(2,1)S(1)}, u32[]{:S(2)}, u32[]{:S(2)}) collective-permute-start(bf16[64,32,128]{2,1,0:T(8,128)(2,1)S(1)} %get-tuple-element.39.refs_0_.own_ref), channel_id=1, source_target_pairs={{0,6},{1,7},{2,0},{3,1},{4,2},{5,3},{6,4},{7,5},{8,14},{9,15},{10,... | collective-permute-start | bytes 1572872 | tf_op jit(solution)/shard_map/ppermute | solution.py:320
  62.2 8.0 %collective-permute-done.in_ref.refs_1_.left_ref = bf16[64,32,128]{2,1,0:T(8,128)(2,1)S(1)} collective-permute-done((bf16[64,32,128]{2,1,0:T(8,128)(2,1)S(1)}, bf16[64,32,128]{2,1,0:T(8,128)(2,1)S(1)}, u32[]{:S(2)}, u32[]{:S(2)}) %collective-permute-start) | collective-permute-done | bytes 524320 | tf_op jit(solution)/shard_map/ppermute | solution.py:320
  73.6 4.8 %collective-permute-start.4 = (bf16[192,32,128]{2,1,0:T(8,128)(2,1)}, bf16[192,32,128]{2,1,0:T(8,128)(2,1)}, u32[]{:S(2)}, u32[]{:S(2)}) collective-permute-start(bf16[192,32,128]{2,1,0:T(8,128)(2,1)} %shard_map.159), channel_id=1, source_target_pairs={{0,1},{1,0},{2,3},{3,2},{4,5},{5,4},{6,7},{7,6},{8,9},{9,8},{10,11... | collective-permute-start | bytes 4718600 | tf_op jit(solution)/shard_map/ppermute | solution.py:324
  80.5 6.2 %all-to-all-start.3 = ((bf16[8,64,8,128]{3,2,1,0:T(8,128)(2,1)}), bf16[8,64,8,128]{3,2,1,0:T(8,128)(2,1)S(1)}, u32[]{:S(2)}, u32[]{:S(2)}) async-start(bf16[8,64,8,128]{3,2,1,0:T(8,128)(2,1)} %shard_map.166), calls=%async_computation.3 | async-start | bytes 2097152 | tf_op jit(solution)/shard_map/all_to_all | solution.py:379
  88.8 4.4 %collective-permute-start.3 = (bf16[32,32,128]{2,1,0:T(8,128)(2,1)S(1)}, bf16[32,32,128]{2,1,0:T(8,128)(2,1)S(1)}, u32[]{:S(2)}, u32[]{:S(2)}) collective-permute-start(bf16[32,32,128]{2,1,0:T(8,128)(2,1)S(1)} %shard_map.157), channel_id=1, source_target_pairs={{0,6},{1,7},{2,0},{3,1},{4,2},{5,3},{6,4},{7,5},{8,14},{9,15},{10,... | collective-permute-start | bytes 786440 | tf_op jit(solution)/shard_map/ppermute | solution.py:320
  93.2 4.1 %collective-permute-done.2.refs_0_ = bf16[32,32,128]{2,1,0:T(8,128)(2,1)S(1)} collective-permute-done((bf16[32,32,128]{2,1,0:T(8,128)(2,1)S(1)}, bf16[32,32,128]{2,1,0:T(8,128)(2,1)S(1)}, u32[]{:S(2)}, u32[]{:S(2)}) %collective-permute-start.2) | collective-permute-done | bytes 262176 | tf_op jit(solution)/shard_map/ppermute | solution.py:320
  98.3 3.3 %collective-permute-start.5 = (bf16[64,32,128]{2,1,0:T(8,128)(2,1)S(1)}, bf16[64,32,128]{2,1,0:T(8,128)(2,1)S(1)}, u32[]{:S(2)}, u32[]{:S(2)}) collective-permute-start(bf16[64,32,128]{2,1,0:T(8,128)(2,1)S(1)} %shard_map.158.across_ref), channel_id=1, source_target_pairs={{0,1},{1,0},{2,3},{3,2},{4,5},{5,4},{6,7},{7,6},{8,9},{9,8},{10,11... | collective-permute-start | bytes 1572872 | tf_op jit(solution)/shard_map/ppermute | solution.py:324
  106.1 3.3 %collective-permute-start.10 = (bf16[768,128]{1,0:T(8,128)(2,1)S(1)}, bf16[768,128]{1,0:T(8,128)(2,1)S(1)}, u32[]{:S(2)}, u32[]{:S(2)}) collective-permute-start(bf16[768,128]{1,0:T(8,128)(2,1)S(1)} %get-tuple-element.47), channel_id=1, source_target_pairs={{0,2},{1,3},{2,4},{3,5},{4,6},{5,7},{6,0},{7,1},{8,10},{9,11},{10,... | collective-permute-start | bytes 589832 | tf_op jit(solution)/shard_map/ppermute | solution.py:320
  109.4 4.0 %collective-permute-start.11 = (bf16[768,128]{1,0:T(8,128)(2,1)S(1)}, bf16[768,128]{1,0:T(8,128)(2,1)S(1)}, u32[]{:S(2)}, u32[]{:S(2)}) collective-permute-start(bf16[768,128]{1,0:T(8,128)(2,1)S(1)} %get-tuple-element.48), channel_id=1, source_target_pairs={{0,6},{1,7},{2,0},{3,1},{4,2},{5,3},{6,4},{7,5},{8,14},{9,15},{10,... | collective-permute-start | bytes 589832 | tf_op jit(solution)/shard_map/ppermute | solution.py:320
  113.4 3.1 %collective-permute-start.12 = (bf16[768,128]{1,0:T(8,128)(2,1)S(1)}, bf16[768,128]{1,0:T(8,128)(2,1)S(1)}, u32[]{:S(2)}, u32[]{:S(2)}) collective-permute-start(bf16[768,128]{1,0:T(8,128)(2,1)S(1)} %get-tuple-element.49), channel_id=1, source_target_pairs={{0,4},{1,5},{2,6},{3,7},{4,0},{5,1},{6,2},{7,3},{8,12},{9,13},{10,... | collective-permute-start | bytes 589832 | tf_op jit(solution)/shard_map/ppermute | solution.py:320
  117.3 5.3 %collective-permute-done.12.refs_3_.far_ref = bf16[768,128]{1,0:T(8,128)(2,1)S(1)} collective-permute-done((bf16[768,128]{1,0:T(8,128)(2,1)S(1)}, bf16[768,128]{1,0:T(8,128)(2,1)S(1)}, u32[]{:S(2)}, u32[]{:S(2)}) %collective-permute-start.12) | collective-permute-done | bytes 196640 | tf_op jit(solution)/shard_map/ppermute | solution.py:320
  122.6 3.4 %collective-permute-start.13 = (bf16[4,640,128]{2,1,0:T(8,128)(2,1)S(1)}, bf16[4,640,128]{2,1,0:T(8,128)(2,1)S(1)}, u32[]{:S(2)}, u32[]{:S(2)}) collective-permute-start(bf16[4,640,128]{2,1,0:T(8,128)(2,1)S(1)} %shard_map.164), channel_id=1, source_target_pairs={{0,1},{1,0},{2,3},{3,2},{4,5},{5,4},{6,7},{7,6},{8,9},{9,8},{10,11... | collective-permute-start | bytes 1966088 | tf_op jit(solution)/shard_map/ppermute | solution.py:324
  129.3 12.6 %all-to-all-start.2 = ((bf16[64,32,128]{2,1,0:T(8,128)(2,1)}), bf16[64,32,128]{2,1,0:T(8,128)(2,1)S(1)}, u32[]{:S(2)}, u32[]{:S(2)}) async-start(bf16[64,32,128]{2,1,0:T(8,128)(2,1)} %shard_map.165), calls=%async_computation.2 | async-start | bytes 1048576 | tf_op jit(solution)/shard_map/all_to_all | solution.py:395
  143.4 3.3 %collective-permute-start.14 = (bf16[320,128]{1,0:T(8,128)(2,1)S(1)}, bf16[320,128]{1,0:T(8,128)(2,1)S(1)}, u32[]{:S(2)}, u32[]{:S(2)}) collective-permute-start(bf16[320,128]{1,0:T(8,128)(2,1)S(1)} %get-tuple-element.53), channel_id=1, source_target_pairs={{0,2},{1,3},{2,4},{3,5},{4,6},{5,7},{6,0},{7,1},{8,10},{9,11},{10,... | collective-permute-start | bytes 245768 | tf_op jit(solution)/shard_map/ppermute | solution.py:320
  146.7 3.2 %collective-permute-start.15 = (bf16[320,128]{1,0:T(8,128)(2,1)S(1)}, bf16[320,128]{1,0:T(8,128)(2,1)S(1)}, u32[]{:S(2)}, u32[]{:S(2)}) collective-permute-start(bf16[320,128]{1,0:T(8,128)(2,1)S(1)} %get-tuple-element.54), channel_id=1, source_target_pairs={{0,6},{1,7},{2,0},{3,1},{4,2},{5,3},{6,4},{7,5},{8,14},{9,15},{10,... | collective-permute-start | bytes 245768 | tf_op jit(solution)/shard_map/ppermute | solution.py:320
  152.4 4.5 %collective-permute-done.16.refs_3_.far_ref = bf16[320,128]{1,0:T(8,128)(2,1)S(1)} collective-permute-done((bf16[320,128]{1,0:T(8,128)(2,1)S(1)}, bf16[320,128]{1,0:T(8,128)(2,1)S(1)}, u32[]{:S(2)}, u32[]{:S(2)}) %collective-permute-start.16) | collective-permute-done | bytes 81952 | tf_op jit(solution)/shard_map/ppermute | solution.py:320
  156.9 4.0 %collective-permute-start.17 = (bf16[4,192,128]{2,1,0:T(8,128)(2,1)S(1)}, bf16[4,192,128]{2,1,0:T(8,128)(2,1)S(1)}, u32[]{:S(2)}, u32[]{:S(2)}) collective-permute-start(bf16[4,192,128]{2,1,0:T(8,128)(2,1)S(1)} %shard_map.168), channel_id=1, source_target_pairs={{0,1},{1,0},{2,3},{3,2},{4,5},{5,4},{6,7},{7,6},{8,9},{9,8},{10,11... | collective-permute-start | bytes 589832 | tf_op jit(solution)/shard_map/ppermute | solution.py:324
  (52 shorter events, 37.6 us)
Async XLA Ops:
  0.6 19.8 %copy-start.1 = (f32[32,4096]{1,0:T(8,128)S(1)}, f32[32,4096]{1,0:T(8,128)}, u32[]{:S(2)}) copy-start(f32[32,4096]{1,0:T(8,128)} %g_ref.1) | copy-start | bytes 1572868
  0.6 19.8 %copy-start.2 = (f32[32,4096]{1,0:T(8,128)S(1)}, f32[32,4096]{1,0:T(8,128)}, u32[]{:S(2)}) copy-start(f32[32,4096]{1,0:T(8,128)} %u_ref.1) | copy-start | bytes 1572868
  3.3 39.2 %all-to-all-start = ((bf16[64,40,128]{2,1,0:T(8,128)(2,1)}), bf16[64,40,128]{2,1,0:T(8,128)(2,1)S(1)}, u32[]{:S(2)}, u32[]{:S(2)}) async-start(bf16[64,40,128]{2,1,0:T(8,128)(2,1)} %get-tuple-element.38), calls=%async_computation | async-start | bytes 1310720 | tf_op jit(solution)/shard_map/all_to_all | solution.py:351
  21.9 4.2 %collective-permute-start.6 = (bf16[4,8,48,128]{3,2,1,0:T(8,128)(2,1)S(1)}, bf16[4,8,48,128]{3,2,1,0:T(8,128)(2,1)S(1)}, u32[]{:S(2)}, u32[]{:S(2)}) collective-permute-start(bf16[4,8,48,128]{3,2,1,0:T(8,128)(2,1)S(1)} %get-tuple-element.41), channel_id=1, source_target_pairs={{0,1},{1,0},{2,3},{3,2},{4,5},{5,4},{6,7},{7,6},{8,9},{9,8},{10,11... | collective-permute-start | bytes 1179656 | tf_op jit(solution)/shard_map/ppermute | solution.py:324
  26.1 9.9 %collective-permute-start.7 = (bf16[16,48,128]{2,1,0:T(8,128)(2,1)S(1)}, bf16[16,48,128]{2,1,0:T(8,128)(2,1)S(1)}, u32[]{:S(2)}, u32[]{:S(2)}) collective-permute-start(bf16[16,48,128]{2,1,0:T(8,128)(2,1)S(1)} %get-tuple-element.43), channel_id=1, source_target_pairs={{0,2},{1,3},{2,4},{3,5},{4,6},{5,7},{6,0},{7,1},{8,10},{9,11},{10,... | collective-permute-start | bytes 589832 | tf_op jit(solution)/shard_map/ppermute | solution.py:320
  29.3 7.7 %collective-permute-start.8 = (bf16[16,48,128]{2,1,0:T(8,128)(2,1)S(1)}, bf16[16,48,128]{2,1,0:T(8,128)(2,1)S(1)}, u32[]{:S(2)}, u32[]{:S(2)}) collective-permute-start(bf16[16,48,128]{2,1,0:T(8,128)(2,1)S(1)} %get-tuple-element.44), channel_id=1, source_target_pairs={{0,6},{1,7},{2,0},{3,1},{4,2},{5,3},{6,4},{7,5},{8,14},{9,15},{10,... | collective-permute-start | bytes 589832 | tf_op jit(solution)/shard_map/ppermute | solution.py:320
  32.6 8.9 %collective-permute-start.9 = (bf16[16,48,128]{2,1,0:T(8,128)(2,1)S(1)}, bf16[16,48,128]{2,1,0:T(8,128)(2,1)S(1)}, u32[]{:S(2)}, u32[]{:S(2)}) collective-permute-start(bf16[16,48,128]{2,1,0:T(8,128)(2,1)S(1)} %get-tuple-element.45), channel_id=1, source_target_pairs={{0,4},{1,5},{2,6},{3,7},{4,0},{5,1},{6,2},{7,3},{8,12},{9,13},{10,... | collective-permute-start | bytes 589832 | tf_op jit(solution)/shard_map/ppermute | solution.py:320
  42.5 37.9 %all-to-all-start.1 = ((bf16[64,48,128]{2,1,0:T(8,128)(2,1)}), bf16[64,48,128]{2,1,0:T(8,128)(2,1)S(1)}, u32[]{:S(2)}, u32[]{:S(2)}) async-start(bf16[64,48,128]{2,1,0:T(8,128)(2,1)} %shard_map.162), calls=%async_computation.1 | async-start | bytes 1572864 | tf_op jit(solution)/shard_map/all_to_all | solution.py:366
  55.7 14.5 %collective-permute-start = (bf16[64,32,128]{2,1,0:T(8,128)(2,1)S(1)}, bf16[64,32,128]{2,1,0:T(8,128)(2,1)S(1)}, u32[]{:S(2)}, u32[]{:S(2)}) collective-permute-start(bf16[64,32,128]{2,1,0:T(8,128)(2,1)S(1)} %get-tuple-element.39.refs_0_.own_ref), channel_id=1, source_target_pairs={{0,2},{1,3},{2,4},{3,5},{4,6},{5,7},{6,0},{7,1},{8,10},{9,11},{10,... | collective-permute-start | bytes 1572872 | tf_op jit(solution)/shard_map/ppermute | solution.py:320
  59.0 13.3 %collective-permute-start.1 = (bf16[64,32,128]{2,1,0:T(8,128)(2,1)S(1)}, bf16[64,32,128]{2,1,0:T(8,128)(2,1)S(1)}, u32[]{:S(2)}, u32[]{:S(2)}) collective-permute-start(bf16[64,32,128]{2,1,0:T(8,128)(2,1)S(1)} %get-tuple-element.39.refs_0_.own_ref), channel_id=1, source_target_pairs={{0,6},{1,7},{2,0},{3,1},{4,2},{5,3},{6,4},{7,5},{8,14},{9,15},{10,... | collective-permute-start | bytes 1572872 | tf_op jit(solution)/shard_map/ppermute | solution.py:320
  73.6 29.6 %collective-permute-start.4 = (bf16[192,32,128]{2,1,0:T(8,128)(2,1)}, bf16[192,32,128]{2,1,0:T(8,128)(2,1)}, u32[]{:S(2)}, u32[]{:S(2)}) collective-permute-start(bf16[192,32,128]{2,1,0:T(8,128)(2,1)} %shard_map.159), channel_id=1, source_target_pairs={{0,1},{1,0},{2,3},{3,2},{4,5},{5,4},{6,7},{7,6},{8,9},{9,8},{10,11... | collective-permute-start | bytes 4718600 | tf_op jit(solution)/shard_map/ppermute | solution.py:324
  80.5 48.8 %all-to-all-start.3 = ((bf16[8,64,8,128]{3,2,1,0:T(8,128)(2,1)}), bf16[8,64,8,128]{3,2,1,0:T(8,128)(2,1)S(1)}, u32[]{:S(2)}, u32[]{:S(2)}) async-start(bf16[8,64,8,128]{3,2,1,0:T(8,128)(2,1)} %shard_map.166), calls=%async_computation.3 | async-start | bytes 2097152 | tf_op jit(solution)/shard_map/all_to_all | solution.py:379
  86.7 10.7 %collective-permute-start.2 = (bf16[32,32,128]{2,1,0:T(8,128)(2,1)S(1)}, bf16[32,32,128]{2,1,0:T(8,128)(2,1)S(1)}, u32[]{:S(2)}, u32[]{:S(2)}) collective-permute-start(bf16[32,32,128]{2,1,0:T(8,128)(2,1)S(1)} %shard_map.156), channel_id=1, source_target_pairs={{0,2},{1,3},{2,4},{3,5},{4,6},{5,7},{6,0},{7,1},{8,10},{9,11},{10,... | collective-permute-start | bytes 786440 | tf_op jit(solution)/shard_map/ppermute | solution.py:320
  88.8 9.5 %collective-permute-start.3 = (bf16[32,32,128]{2,1,0:T(8,128)(2,1)S(1)}, bf16[32,32,128]{2,1,0:T(8,128)(2,1)S(1)}, u32[]{:S(2)}, u32[]{:S(2)}) collective-permute-start(bf16[32,32,128]{2,1,0:T(8,128)(2,1)S(1)} %shard_map.157), channel_id=1, source_target_pairs={{0,6},{1,7},{2,0},{3,1},{4,2},{5,3},{6,4},{7,5},{8,14},{9,15},{10,... | collective-permute-start | bytes 786440 | tf_op jit(solution)/shard_map/ppermute | solution.py:320
  98.3 4.9 %collective-permute-start.5 = (bf16[64,32,128]{2,1,0:T(8,128)(2,1)S(1)}, bf16[64,32,128]{2,1,0:T(8,128)(2,1)S(1)}, u32[]{:S(2)}, u32[]{:S(2)}) collective-permute-start(bf16[64,32,128]{2,1,0:T(8,128)(2,1)S(1)} %shard_map.158.across_ref), channel_id=1, source_target_pairs={{0,1},{1,0},{2,3},{3,2},{4,5},{5,4},{6,7},{7,6},{8,9},{9,8},{10,11... | collective-permute-start | bytes 1572872 | tf_op jit(solution)/shard_map/ppermute | solution.py:324
  106.1 10.4 %collective-permute-start.10 = (bf16[768,128]{1,0:T(8,128)(2,1)S(1)}, bf16[768,128]{1,0:T(8,128)(2,1)S(1)}, u32[]{:S(2)}, u32[]{:S(2)}) collective-permute-start(bf16[768,128]{1,0:T(8,128)(2,1)S(1)} %get-tuple-element.47), channel_id=1, source_target_pairs={{0,2},{1,3},{2,4},{3,5},{4,6},{5,7},{6,0},{7,1},{8,10},{9,11},{10,... | collective-permute-start | bytes 589832 | tf_op jit(solution)/shard_map/ppermute | solution.py:320
  109.4 7.8 %collective-permute-start.11 = (bf16[768,128]{1,0:T(8,128)(2,1)S(1)}, bf16[768,128]{1,0:T(8,128)(2,1)S(1)}, u32[]{:S(2)}, u32[]{:S(2)}) collective-permute-start(bf16[768,128]{1,0:T(8,128)(2,1)S(1)} %get-tuple-element.48), channel_id=1, source_target_pairs={{0,6},{1,7},{2,0},{3,1},{4,2},{5,3},{6,4},{7,5},{8,14},{9,15},{10,... | collective-permute-start | bytes 589832 | tf_op jit(solution)/shard_map/ppermute | solution.py:320
  113.4 9.2 %collective-permute-start.12 = (bf16[768,128]{1,0:T(8,128)(2,1)S(1)}, bf16[768,128]{1,0:T(8,128)(2,1)S(1)}, u32[]{:S(2)}, u32[]{:S(2)}) collective-permute-start(bf16[768,128]{1,0:T(8,128)(2,1)S(1)} %get-tuple-element.49), channel_id=1, source_target_pairs={{0,4},{1,5},{2,6},{3,7},{4,0},{5,1},{6,2},{7,3},{8,12},{9,13},{10,... | collective-permute-start | bytes 589832 | tf_op jit(solution)/shard_map/ppermute | solution.py:320
  122.6 5.1 %collective-permute-start.13 = (bf16[4,640,128]{2,1,0:T(8,128)(2,1)S(1)}, bf16[4,640,128]{2,1,0:T(8,128)(2,1)S(1)}, u32[]{:S(2)}, u32[]{:S(2)}) collective-permute-start(bf16[4,640,128]{2,1,0:T(8,128)(2,1)S(1)} %shard_map.164), channel_id=1, source_target_pairs={{0,1},{1,0},{2,3},{3,2},{4,5},{5,4},{6,7},{7,6},{8,9},{9,8},{10,11... | collective-permute-start | bytes 1966088 | tf_op jit(solution)/shard_map/ppermute | solution.py:324
  129.3 36.3 %all-to-all-start.2 = ((bf16[64,32,128]{2,1,0:T(8,128)(2,1)}), bf16[64,32,128]{2,1,0:T(8,128)(2,1)S(1)}, u32[]{:S(2)}, u32[]{:S(2)}) async-start(bf16[64,32,128]{2,1,0:T(8,128)(2,1)} %shard_map.165), calls=%async_computation.2 | async-start | bytes 1048576 | tf_op jit(solution)/shard_map/all_to_all | solution.py:395
  143.4 9.0 %collective-permute-start.14 = (bf16[320,128]{1,0:T(8,128)(2,1)S(1)}, bf16[320,128]{1,0:T(8,128)(2,1)S(1)}, u32[]{:S(2)}, u32[]{:S(2)}) collective-permute-start(bf16[320,128]{1,0:T(8,128)(2,1)S(1)} %get-tuple-element.53), channel_id=1, source_target_pairs={{0,2},{1,3},{2,4},{3,5},{4,6},{5,7},{6,0},{7,1},{8,10},{9,11},{10,... | collective-permute-start | bytes 245768 | tf_op jit(solution)/shard_map/ppermute | solution.py:320
  146.7 5.7 %collective-permute-start.15 = (bf16[320,128]{1,0:T(8,128)(2,1)S(1)}, bf16[320,128]{1,0:T(8,128)(2,1)S(1)}, u32[]{:S(2)}, u32[]{:S(2)}) collective-permute-start(bf16[320,128]{1,0:T(8,128)(2,1)S(1)} %get-tuple-element.54), channel_id=1, source_target_pairs={{0,6},{1,7},{2,0},{3,1},{4,2},{5,3},{6,4},{7,5},{8,14},{9,15},{10,... | collective-permute-start | bytes 245768 | tf_op jit(solution)/shard_map/ppermute | solution.py:320
  149.9 7.0 %collective-permute-start.16 = (bf16[320,128]{1,0:T(8,128)(2,1)S(1)}, bf16[320,128]{1,0:T(8,128)(2,1)S(1)}, u32[]{:S(2)}, u32[]{:S(2)}) collective-permute-start(bf16[320,128]{1,0:T(8,128)(2,1)S(1)} %get-tuple-element.55), channel_id=1, source_target_pairs={{0,4},{1,5},{2,6},{3,7},{4,0},{5,1},{6,2},{7,3},{8,12},{9,13},{10,... | collective-permute-start | bytes 245768 | tf_op jit(solution)/shard_map/ppermute | solution.py:320
  156.9 8.3 %collective-permute-start.17 = (bf16[4,192,128]{2,1,0:T(8,128)(2,1)S(1)}, bf16[4,192,128]{2,1,0:T(8,128)(2,1)S(1)}, u32[]{:S(2)}, u32[]{:S(2)}) collective-permute-start(bf16[4,192,128]{2,1,0:T(8,128)(2,1)S(1)} %shard_map.168), channel_id=1, source_target_pairs={{0,1},{1,0},{2,3},{3,2},{4,5},{5,4},{6,7},{7,6},{8,9},{9,8},{10,11... | collective-permute-start | bytes 589832 | tf_op jit(solution)/shard_map/ppermute | solution.py:324
  (4 other events, 43.3 us)

commit v4 on v3

--- a/solution.py
+++ b/solution.py
@@ -93,8 +93,7 @@
     slot = dot(named.astype(bf16), earlier)
     pos = jnp.where(named > 0.0, slot, -1.0)
     pos_ref[...] = pos
-    expand = jnp.where((iota((ROWS, E), 0) >> 4) == iota((ROWS, E), 1), 1.0, 0.0).astype(bf16)
-    at = dot(expand, pos.astype(bf16))
+    at = jnp.concatenate([jnp.broadcast_to(pos[e : e + 1, :], (CAP, TOK)) for e in range(E)], axis=0)
     pick = jnp.where(at == (iota((ROWS, TOK), 0) & 15).astype(f32), 1.0, 0.0).astype(bf16)
     mine = normed_ref[:, pl.ds(pl.multiple_of(m * COLS, COLS), COLS)]
     rows = dot(pick, mine).astype(bf16)
@@ -396,7 +395,7 @@
 
     message = shape(64 + 2 * LANES, LANES)
     common, mine, to_right, to_left, to_far = call(
-        common_hidden_body, (shape(64, 48, LANES),) + (message,) * 4, 3, 1, far=(1,)
+        common_hidden_body, (shape(64, 48, LANES),) + (message,) * 4, 3, 1
     )(m, normed, common)
     c_far = shift(to_far, 4)
     c_left = shift(to_right, 2)

time: 168 us -> 167 us (level)
  no operation moved by 1% of the time
where the time goes in v4:
time: 167 us; the launch traced here: 166 us
  starting transfers between devices  109 us (65%)
  waiting for transfers between devices  35.9 us (21%)
  Pallas kernels  19.7 us (12%)
    ppermute x13, starting transfers between devices, shift(): return lax.ppermute(x, 'tp', [(i, (i + step) % N_TP) for i in range(N_TP)])  42.2 us
    ppermute x13, waiting for transfers between devices, shift(): return lax.ppermute(x, 'tp', [(i, (i + step) % N_TP) for i in range(N_TP)])  31.3 us
    pallas_call x20, Pallas kernels, run(): return fn(*placed)  19.7 us
    ppermute x5, starting transfers between devices, swap(): return lax.ppermute(x, 'tp', [(i, i ^ k) for i in range(N_TP)])  18.5 us
    all_to_all x1, starting transfers between devices, local(): got = lax.all_to_all(send, 'fs', 0, 0, tiled=True)  17.1 us
    all_to_all x1, starting transfers between devices, local(): returned = lax.all_to_all(expert_out, 'fs', 0, 0, tiled=True)  12.6 us
    all_to_all x1, starting transfers between devices, local(): weights = lax.all_to_all(spread, 'fs', 0, 0, tiled=True)  12.4 us
    all_to_all x1, starting transfers between devices, local(): lax.all_to_all(common_send, 'fs', 0, 0, axis_index_groups=COLUMNS, tiled=...  6.2 us
  transfers between devices with their start and end apart: 22, of which 12 were waited for; matrix products, arithmetic and copies ran while one was open for 0% of the time, Pallas kernels for 10%

profile of v4, /device:TPU:1, one launch (start us, length us, event | category | flops | bytes accessed | tf_op | source)
XLA Modules:
  0.0 165.7 jit_solution(8824434477137047667)
XLA Ops:
  3.2 17.1 %all-to-all-start = ((bf16[64,40,128]{2,1,0:T(8,128)(2,1)}), bf16[64,40,128]{2,1,0:T(8,128)(2,1)S(1)}, u32[]{:S(2)}, u32[]{:S(2)}) async-start(bf16[64,40,128]{2,1,0:T(8,128)(2,1)} %get-tuple-element.38), calls=%async_computation | async-start | bytes 1310720 | tf_op jit(solution)/shard_map/all_to_all | solution.py:350
  26.1 3.1 %collective-permute-start.7 = (bf16[16,48,128]{2,1,0:T(8,128)(2,1)S(1)}, bf16[16,48,128]{2,1,0:T(8,128)(2,1)S(1)}, u32[]{:S(2)}, u32[]{:S(2)}) collective-permute-start(bf16[16,48,128]{2,1,0:T(8,128)(2,1)S(1)} %get-tuple-element.43), channel_id=1, source_target_pairs={{0,2},{1,3},{2,4},{3,5},{4,6},{5,7},{6,0},{7,1},{8,10},{9,11},{10,... | collective-permute-start | bytes 589832 | tf_op jit(solution)/shard_map/ppermute | solution.py:319
  29.2 3.4 %collective-permute-start.8 = (bf16[16,48,128]{2,1,0:T(8,128)(2,1)S(1)}, bf16[16,48,128]{2,1,0:T(8,128)(2,1)S(1)}, u32[]{:S(2)}, u32[]{:S(2)}) collective-permute-start(bf16[16,48,128]{2,1,0:T(8,128)(2,1)S(1)} %get-tuple-element.44), channel_id=1, source_target_pairs={{0,6},{1,7},{2,0},{3,1},{4,2},{5,3},{6,4},{7,5},{8,14},{9,15},{10,... | collective-permute-start | bytes 589832 | tf_op jit(solution)/shard_map/ppermute | solution.py:319
  32.6 3.4 %collective-permute-start.9 = (bf16[16,48,128]{2,1,0:T(8,128)(2,1)S(1)}, bf16[16,48,128]{2,1,0:T(8,128)(2,1)S(1)}, u32[]{:S(2)}, u32[]{:S(2)}) collective-permute-start(bf16[16,48,128]{2,1,0:T(8,128)(2,1)S(1)} %get-tuple-element.45), channel_id=1, source_target_pairs={{0,4},{1,5},{2,6},{3,7},{4,0},{5,1},{6,2},{7,3},{8,12},{9,13},{10,... | collective-permute-start | bytes 589832 | tf_op jit(solution)/shard_map/ppermute | solution.py:319
  36.9 4.6 %collective-permute-done.9.far_ref = bf16[16,48,128]{2,1,0:T(8,128)(2,1)S(1)} collective-permute-done((bf16[16,48,128]{2,1,0:T(8,128)(2,1)S(1)}, bf16[16,48,128]{2,1,0:T(8,128)(2,1)S(1)}, u32[]{:S(2)}, u32[]{:S(2)}) %collective-permute-start.9) | collective-permute-done | bytes 196640 | tf_op jit(solution)/shard_map/ppermute | solution.py:319
  42.5 12.4 %all-to-all-start.1 = ((bf16[64,48,128]{2,1,0:T(8,128)(2,1)}), bf16[64,48,128]{2,1,0:T(8,128)(2,1)S(1)}, u32[]{:S(2)}, u32[]{:S(2)}) async-start(bf16[64,48,128]{2,1,0:T(8,128)(2,1)} %shard_map.162), calls=%async_computation.1 | async-start | bytes 1572864 | tf_op jit(solution)/shard_map/all_to_all | solution.py:365
  55.6 3.3 %collective-permute-start = (bf16[64,32,128]{2,1,0:T(8,128)(2,1)S(1)}, bf16[64,32,128]{2,1,0:T(8,128)(2,1)S(1)}, u32[]{:S(2)}, u32[]{:S(2)}) collective-permute-start(bf16[64,32,128]{2,1,0:T(8,128)(2,1)S(1)} %get-tuple-element.39.refs_0_.own_ref), channel_id=1, source_target_pairs={{0,2},{1,3},{2,4},{3,5},{4,6},{5,7},{6,0},{7,1},{8,10},{9,11},{10,... | collective-permute-start | bytes 1572872 | tf_op jit(solution)/shard_map/ppermute | solution.py:319
  59.0 3.1 %collective-permute-start.1 = (bf16[64,32,128]{2,1,0:T(8,128)(2,1)S(1)}, bf16[64,32,128]{2,1,0:T(8,128)(2,1)S(1)}, u32[]{:S(2)}, u32[]{:S(2)}) collective-permute-start(bf16[64,32,128]{2,1,0:T(8,128)(2,1)S(1)} %get-tuple-element.39.refs_0_.own_ref), channel_id=1, source_target_pairs={{0,6},{1,7},{2,0},{3,1},{4,2},{5,3},{6,4},{7,5},{8,14},{9,15},{10,... | collective-permute-start | bytes 1572872 | tf_op jit(solution)/shard_map/ppermute | solution.py:319
  62.1 8.0 %collective-permute-done.in_ref.refs_1_.left_ref = bf16[64,32,128]{2,1,0:T(8,128)(2,1)S(1)} collective-permute-done((bf16[64,32,128]{2,1,0:T(8,128)(2,1)S(1)}, bf16[64,32,128]{2,1,0:T(8,128)(2,1)S(1)}, u32[]{:S(2)}, u32[]{:S(2)}) %collective-permute-start) | collective-permute-done | bytes 524320 | tf_op jit(solution)/shard_map/ppermute | solution.py:319
  73.5 4.8 %collective-permute-start.4 = (bf16[192,32,128]{2,1,0:T(8,128)(2,1)}, bf16[192,32,128]{2,1,0:T(8,128)(2,1)}, u32[]{:S(2)}, u32[]{:S(2)}) collective-permute-start(bf16[192,32,128]{2,1,0:T(8,128)(2,1)} %shard_map.159), channel_id=1, source_target_pairs={{0,1},{1,0},{2,3},{3,2},{4,5},{5,4},{6,7},{7,6},{8,9},{9,8},{10,11... | collective-permute-start | bytes 4718600 | tf_op jit(solution)/shard_map/ppermute | solution.py:323
  80.4 6.2 %all-to-all-start.3 = ((bf16[8,64,8,128]{3,2,1,0:T(8,128)(2,1)}), bf16[8,64,8,128]{3,2,1,0:T(8,128)(2,1)S(1)}, u32[]{:S(2)}, u32[]{:S(2)}) async-start(bf16[8,64,8,128]{3,2,1,0:T(8,128)(2,1)} %shard_map.166), calls=%async_computation.3 | async-start | bytes 2097152 | tf_op jit(solution)/shard_map/all_to_all | solution.py:378
  88.8 4.4 %collective-permute-start.3 = (bf16[32,32,128]{2,1,0:T(8,128)(2,1)S(1)}, bf16[32,32,128]{2,1,0:T(8,128)(2,1)S(1)}, u32[]{:S(2)}, u32[]{:S(2)}) collective-permute-start(bf16[32,32,128]{2,1,0:T(8,128)(2,1)S(1)} %shard_map.157), channel_id=1, source_target_pairs={{0,6},{1,7},{2,0},{3,1},{4,2},{5,3},{6,4},{7,5},{8,14},{9,15},{10,... | collective-permute-start | bytes 786440 | tf_op jit(solution)/shard_map/ppermute | solution.py:319
  93.2 4.1 %collective-permute-done.2.refs_0_ = bf16[32,32,128]{2,1,0:T(8,128)(2,1)S(1)} collective-permute-done((bf16[32,32,128]{2,1,0:T(8,128)(2,1)S(1)}, bf16[32,32,128]{2,1,0:T(8,128)(2,1)S(1)}, u32[]{:S(2)}, u32[]{:S(2)}) %collective-permute-start.2) | collective-permute-done | bytes 262176 | tf_op jit(solution)/shard_map/ppermute | solution.py:319
  98.3 3.3 %collective-permute-start.5 = (bf16[64,32,128]{2,1,0:T(8,128)(2,1)S(1)}, bf16[64,32,128]{2,1,0:T(8,128)(2,1)S(1)}, u32[]{:S(2)}, u32[]{:S(2)}) collective-permute-start(bf16[64,32,128]{2,1,0:T(8,128)(2,1)S(1)} %shard_map.158.across_ref), channel_id=1, source_target_pairs={{0,1},{1,0},{2,3},{3,2},{4,5},{5,4},{6,7},{7,6},{8,9},{9,8},{10,11... | collective-permute-start | bytes 1572872 | tf_op jit(solution)/shard_map/ppermute | solution.py:323
  106.1 3.3 %collective-permute-start.10 = (bf16[768,128]{1,0:T(8,128)(2,1)S(1)}, bf16[768,128]{1,0:T(8,128)(2,1)S(1)}, u32[]{:S(2)}, u32[]{:S(2)}) collective-permute-start(bf16[768,128]{1,0:T(8,128)(2,1)S(1)} %get-tuple-element.47), channel_id=1, source_target_pairs={{0,2},{1,3},{2,4},{3,5},{4,6},{5,7},{6,0},{7,1},{8,10},{9,11},{10,... | collective-permute-start | bytes 589832 | tf_op jit(solution)/shard_map/ppermute | solution.py:319
  109.4 4.0 %collective-permute-start.11 = (bf16[768,128]{1,0:T(8,128)(2,1)S(1)}, bf16[768,128]{1,0:T(8,128)(2,1)S(1)}, u32[]{:S(2)}, u32[]{:S(2)}) collective-permute-start(bf16[768,128]{1,0:T(8,128)(2,1)S(1)} %get-tuple-element.48), channel_id=1, source_target_pairs={{0,6},{1,7},{2,0},{3,1},{4,2},{5,3},{6,4},{7,5},{8,14},{9,15},{10,... | collective-permute-start | bytes 589832 | tf_op jit(solution)/shard_map/ppermute | solution.py:319
  113.3 3.1 %collective-permute-start.12 = (bf16[768,128]{1,0:T(8,128)(2,1)S(1)}, bf16[768,128]{1,0:T(8,128)(2,1)S(1)}, u32[]{:S(2)}, u32[]{:S(2)}) collective-permute-start(bf16[768,128]{1,0:T(8,128)(2,1)S(1)} %get-tuple-element.49), channel_id=1, source_target_pairs={{0,4},{1,5},{2,6},{3,7},{4,0},{5,1},{6,2},{7,3},{8,12},{9,13},{10,... | collective-permute-start | bytes 589832 | tf_op jit(solution)/shard_map/ppermute | solution.py:319
  117.2 5.3 %collective-permute-done.12.refs_3_.far_ref = bf16[768,128]{1,0:T(8,128)(2,1)S(1)} collective-permute-done((bf16[768,128]{1,0:T(8,128)(2,1)S(1)}, bf16[768,128]{1,0:T(8,128)(2,1)S(1)}, u32[]{:S(2)}, u32[]{:S(2)}) %collective-permute-start.12) | collective-permute-done | bytes 196640 | tf_op jit(solution)/shard_map/ppermute | solution.py:319
  122.6 3.6 %collective-permute-start.13 = (bf16[4,640,128]{2,1,0:T(8,128)(2,1)S(1)}, bf16[4,640,128]{2,1,0:T(8,128)(2,1)S(1)}, u32[]{:S(2)}, u32[]{:S(2)}) collective-permute-start(bf16[4,640,128]{2,1,0:T(8,128)(2,1)S(1)} %shard_map.164), channel_id=1, source_target_pairs={{0,1},{1,0},{2,3},{3,2},{4,5},{5,4},{6,7},{7,6},{8,9},{9,8},{10,11... | collective-permute-start | bytes 1966088 | tf_op jit(solution)/shard_map/ppermute | solution.py:323
  129.3 12.6 %all-to-all-start.2 = ((bf16[64,32,128]{2,1,0:T(8,128)(2,1)}), bf16[64,32,128]{2,1,0:T(8,128)(2,1)S(1)}, u32[]{:S(2)}, u32[]{:S(2)}) async-start(bf16[64,32,128]{2,1,0:T(8,128)(2,1)} %shard_map.165), calls=%async_computation.2 | async-start | bytes 1048576 | tf_op jit(solution)/shard_map/all_to_all | solution.py:394
  142.4 3.3 %collective-permute-start.14 = (bf16[320,128]{1,0:T(8,128)(2,1)S(1)}, bf16[320,128]{1,0:T(8,128)(2,1)S(1)}, u32[]{:S(2)}, u32[]{:S(2)}) collective-permute-start(bf16[320,128]{1,0:T(8,128)(2,1)S(1)} %get-tuple-element.53), channel_id=1, source_target_pairs={{0,2},{1,3},{2,4},{3,5},{4,6},{5,7},{6,0},{7,1},{8,10},{9,11},{10,... | collective-permute-start | bytes 245768 | tf_op jit(solution)/shard_map/ppermute | solution.py:319
  145.7 3.2 %collective-permute-start.15 = (bf16[320,128]{1,0:T(8,128)(2,1)S(1)}, bf16[320,128]{1,0:T(8,128)(2,1)S(1)}, u32[]{:S(2)}, u32[]{:S(2)}) collective-permute-start(bf16[320,128]{1,0:T(8,128)(2,1)S(1)} %get-tuple-element.54), channel_id=1, source_target_pairs={{0,6},{1,7},{2,0},{3,1},{4,2},{5,3},{6,4},{7,5},{8,14},{9,15},{10,... | collective-permute-start | bytes 245768 | tf_op jit(solution)/shard_map/ppermute | solution.py:319
  151.4 4.5 %collective-permute-done.16.refs_3_.far_ref = bf16[320,128]{1,0:T(8,128)(2,1)S(1)} collective-permute-done((bf16[320,128]{1,0:T(8,128)(2,1)S(1)}, bf16[320,128]{1,0:T(8,128)(2,1)S(1)}, u32[]{:S(2)}, u32[]{:S(2)}) %collective-permute-start.16) | collective-permute-done | bytes 81952 | tf_op jit(solution)/shard_map/ppermute | solution.py:319
  155.9 4.0 %collective-permute-start.17 = (bf16[4,192,128]{2,1,0:T(8,128)(2,1)S(1)}, bf16[4,192,128]{2,1,0:T(8,128)(2,1)S(1)}, u32[]{:S(2)}, u32[]{:S(2)}) collective-permute-start(bf16[4,192,128]{2,1,0:T(8,128)(2,1)S(1)} %shard_map.168), channel_id=1, source_target_pairs={{0,1},{1,0},{2,3},{3,2},{4,5},{5,4},{6,7},{7,6},{8,9},{9,8},{10,11... | collective-permute-start | bytes 589832 | tf_op jit(solution)/shard_map/ppermute | solution.py:323
  (54 shorter events, 36.4 us)
Async XLA Ops:
  0.6 19.8 %copy-start.2 = (f32[32,4096]{1,0:T(8,128)S(1)}, f32[32,4096]{1,0:T(8,128)}, u32[]{:S(2)}) copy-start(f32[32,4096]{1,0:T(8,128)} %g_ref.1) | copy-start | bytes 1572868
  0.6 19.8 %copy-start.3 = (f32[32,4096]{1,0:T(8,128)S(1)}, f32[32,4096]{1,0:T(8,128)}, u32[]{:S(2)}) copy-start(f32[32,4096]{1,0:T(8,128)} %u_ref.1) | copy-start | bytes 1572868
  3.2 39.2 %all-to-all-start = ((bf16[64,40,128]{2,1,0:T(8,128)(2,1)}), bf16[64,40,128]{2,1,0:T(8,128)(2,1)S(1)}, u32[]{:S(2)}, u32[]{:S(2)}) async-start(bf16[64,40,128]{2,1,0:T(8,128)(2,1)} %get-tuple-element.38), calls=%async_computation | async-start | bytes 1310720 | tf_op jit(solution)/shard_map/all_to_all | solution.py:350
  21.8 4.2 %collective-permute-start.6 = (bf16[4,8,48,128]{3,2,1,0:T(8,128)(2,1)S(1)}, bf16[4,8,48,128]{3,2,1,0:T(8,128)(2,1)S(1)}, u32[]{:S(2)}, u32[]{:S(2)}) collective-permute-start(bf16[4,8,48,128]{3,2,1,0:T(8,128)(2,1)S(1)} %get-tuple-element.41), channel_id=1, source_target_pairs={{0,1},{1,0},{2,3},{3,2},{4,5},{5,4},{6,7},{7,6},{8,9},{9,8},{10,11... | collective-permute-start | bytes 1179656 | tf_op jit(solution)/shard_map/ppermute | solution.py:323
  26.1 9.9 %collective-permute-start.7 = (bf16[16,48,128]{2,1,0:T(8,128)(2,1)S(1)}, bf16[16,48,128]{2,1,0:T(8,128)(2,1)S(1)}, u32[]{:S(2)}, u32[]{:S(2)}) collective-permute-start(bf16[16,48,128]{2,1,0:T(8,128)(2,1)S(1)} %get-tuple-element.43), channel_id=1, source_target_pairs={{0,2},{1,3},{2,4},{3,5},{4,6},{5,7},{6,0},{7,1},{8,10},{9,11},{10,... | collective-permute-start | bytes 589832 | tf_op jit(solution)/shard_map/ppermute | solution.py:319
  29.2 7.7 %collective-permute-start.8 = (bf16[16,48,128]{2,1,0:T(8,128)(2,1)S(1)}, bf16[16,48,128]{2,1,0:T(8,128)(2,1)S(1)}, u32[]{:S(2)}, u32[]{:S(2)}) collective-permute-start(bf16[16,48,128]{2,1,0:T(8,128)(2,1)S(1)} %get-tuple-element.44), channel_id=1, source_target_pairs={{0,6},{1,7},{2,0},{3,1},{4,2},{5,3},{6,4},{7,5},{8,14},{9,15},{10,... | collective-permute-start | bytes 589832 | tf_op jit(solution)/shard_map/ppermute | solution.py:319
  32.6 8.9 %collective-permute-start.9 = (bf16[16,48,128]{2,1,0:T(8,128)(2,1)S(1)}, bf16[16,48,128]{2,1,0:T(8,128)(2,1)S(1)}, u32[]{:S(2)}, u32[]{:S(2)}) collective-permute-start(bf16[16,48,128]{2,1,0:T(8,128)(2,1)S(1)} %get-tuple-element.45), channel_id=1, source_target_pairs={{0,4},{1,5},{2,6},{3,7},{4,0},{5,1},{6,2},{7,3},{8,12},{9,13},{10,... | collective-permute-start | bytes 589832 | tf_op jit(solution)/shard_map/ppermute | solution.py:319
  42.5 37.9 %all-to-all-start.1 = ((bf16[64,48,128]{2,1,0:T(8,128)(2,1)}), bf16[64,48,128]{2,1,0:T(8,128)(2,1)S(1)}, u32[]{:S(2)}, u32[]{:S(2)}) async-start(bf16[64,48,128]{2,1,0:T(8,128)(2,1)} %shard_map.162), calls=%async_computation.1 | async-start | bytes 1572864 | tf_op jit(solution)/shard_map/all_to_all | solution.py:365
  55.6 14.5 %collective-permute-start = (bf16[64,32,128]{2,1,0:T(8,128)(2,1)S(1)}, bf16[64,32,128]{2,1,0:T(8,128)(2,1)S(1)}, u32[]{:S(2)}, u32[]{:S(2)}) collective-permute-start(bf16[64,32,128]{2,1,0:T(8,128)(2,1)S(1)} %get-tuple-element.39.refs_0_.own_ref), channel_id=1, source_target_pairs={{0,2},{1,3},{2,4},{3,5},{4,6},{5,7},{6,0},{7,1},{8,10},{9,11},{10,... | collective-permute-start | bytes 1572872 | tf_op jit(solution)/shard_map/ppermute | solution.py:319
  59.0 13.3 %collective-permute-start.1 = (bf16[64,32,128]{2,1,0:T(8,128)(2,1)S(1)}, bf16[64,32,128]{2,1,0:T(8,128)(2,1)S(1)}, u32[]{:S(2)}, u32[]{:S(2)}) collective-permute-start(bf16[64,32,128]{2,1,0:T(8,128)(2,1)S(1)} %get-tuple-element.39.refs_0_.own_ref), channel_id=1, source_target_pairs={{0,6},{1,7},{2,0},{3,1},{4,2},{5,3},{6,4},{7,5},{8,14},{9,15},{10,... | collective-permute-start | bytes 1572872 | tf_op jit(solution)/shard_map/ppermute | solution.py:319
  73.5 29.6 %collective-permute-start.4 = (bf16[192,32,128]{2,1,0:T(8,128)(2,1)}, bf16[192,32,128]{2,1,0:T(8,128)(2,1)}, u32[]{:S(2)}, u32[]{:S(2)}) collective-permute-start(bf16[192,32,128]{2,1,0:T(8,128)(2,1)} %shard_map.159), channel_id=1, source_target_pairs={{0,1},{1,0},{2,3},{3,2},{4,5},{5,4},{6,7},{7,6},{8,9},{9,8},{10,11... | collective-permute-start | bytes 4718600 | tf_op jit(solution)/shard_map/ppermute | solution.py:323
  80.4 48.9 %all-to-all-start.3 = ((bf16[8,64,8,128]{3,2,1,0:T(8,128)(2,1)}), bf16[8,64,8,128]{3,2,1,0:T(8,128)(2,1)S(1)}, u32[]{:S(2)}, u32[]{:S(2)}) async-start(bf16[8,64,8,128]{3,2,1,0:T(8,128)(2,1)} %shard_map.166), calls=%async_computation.3 | async-start | bytes 2097152 | tf_op jit(solution)/shard_map/all_to_all | solution.py:378
  86.6 10.7 %collective-permute-start.2 = (bf16[32,32,128]{2,1,0:T(8,128)(2,1)S(1)}, bf16[32,32,128]{2,1,0:T(8,128)(2,1)S(1)}, u32[]{:S(2)}, u32[]{:S(2)}) collective-permute-start(bf16[32,32,128]{2,1,0:T(8,128)(2,1)S(1)} %shard_map.156), channel_id=1, source_target_pairs={{0,2},{1,3},{2,4},{3,5},{4,6},{5,7},{6,0},{7,1},{8,10},{9,11},{10,... | collective-permute-start | bytes 786440 | tf_op jit(solution)/shard_map/ppermute | solution.py:319
  88.8 9.5 %collective-permute-start.3 = (bf16[32,32,128]{2,1,0:T(8,128)(2,1)S(1)}, bf16[32,32,128]{2,1,0:T(8,128)(2,1)S(1)}, u32[]{:S(2)}, u32[]{:S(2)}) collective-permute-start(bf16[32,32,128]{2,1,0:T(8,128)(2,1)S(1)} %shard_map.157), channel_id=1, source_target_pairs={{0,6},{1,7},{2,0},{3,1},{4,2},{5,3},{6,4},{7,5},{8,14},{9,15},{10,... | collective-permute-start | bytes 786440 | tf_op jit(solution)/shard_map/ppermute | solution.py:319
  98.3 4.9 %collective-permute-start.5 = (bf16[64,32,128]{2,1,0:T(8,128)(2,1)S(1)}, bf16[64,32,128]{2,1,0:T(8,128)(2,1)S(1)}, u32[]{:S(2)}, u32[]{:S(2)}) collective-permute-start(bf16[64,32,128]{2,1,0:T(8,128)(2,1)S(1)} %shard_map.158.across_ref), channel_id=1, source_target_pairs={{0,1},{1,0},{2,3},{3,2},{4,5},{5,4},{6,7},{7,6},{8,9},{9,8},{10,11... | collective-permute-start | bytes 1572872 | tf_op jit(solution)/shard_map/ppermute | solution.py:323
  106.1 10.4 %collective-permute-start.10 = (bf16[768,128]{1,0:T(8,128)(2,1)S(1)}, bf16[768,128]{1,0:T(8,128)(2,1)S(1)}, u32[]{:S(2)}, u32[]{:S(2)}) collective-permute-start(bf16[768,128]{1,0:T(8,128)(2,1)S(1)} %get-tuple-element.47), channel_id=1, source_target_pairs={{0,2},{1,3},{2,4},{3,5},{4,6},{5,7},{6,0},{7,1},{8,10},{9,11},{10,... | collective-permute-start | bytes 589832 | tf_op jit(solution)/shard_map/ppermute | solution.py:319
  109.4 7.8 %collective-permute-start.11 = (bf16[768,128]{1,0:T(8,128)(2,1)S(1)}, bf16[768,128]{1,0:T(8,128)(2,1)S(1)}, u32[]{:S(2)}, u32[]{:S(2)}) collective-permute-start(bf16[768,128]{1,0:T(8,128)(2,1)S(1)} %get-tuple-element.48), channel_id=1, source_target_pairs={{0,6},{1,7},{2,0},{3,1},{4,2},{5,3},{6,4},{7,5},{8,14},{9,15},{10,... | collective-permute-start | bytes 589832 | tf_op jit(solution)/shard_map/ppermute | solution.py:319
  113.3 9.2 %collective-permute-start.12 = (bf16[768,128]{1,0:T(8,128)(2,1)S(1)}, bf16[768,128]{1,0:T(8,128)(2,1)S(1)}, u32[]{:S(2)}, u32[]{:S(2)}) collective-permute-start(bf16[768,128]{1,0:T(8,128)(2,1)S(1)} %get-tuple-element.49), channel_id=1, source_target_pairs={{0,4},{1,5},{2,6},{3,7},{4,0},{5,1},{6,2},{7,3},{8,12},{9,13},{10,... | collective-permute-start | bytes 589832 | tf_op jit(solution)/shard_map/ppermute | solution.py:319
  122.6 5.3 %collective-permute-start.13 = (bf16[4,640,128]{2,1,0:T(8,128)(2,1)S(1)}, bf16[4,640,128]{2,1,0:T(8,128)(2,1)S(1)}, u32[]{:S(2)}, u32[]{:S(2)}) collective-permute-start(bf16[4,640,128]{2,1,0:T(8,128)(2,1)S(1)} %shard_map.164), channel_id=1, source_target_pairs={{0,1},{1,0},{2,3},{3,2},{4,5},{5,4},{6,7},{7,6},{8,9},{9,8},{10,11... | collective-permute-start | bytes 1966088 | tf_op jit(solution)/shard_map/ppermute | solution.py:323
  129.3 35.2 %all-to-all-start.2 = ((bf16[64,32,128]{2,1,0:T(8,128)(2,1)}), bf16[64,32,128]{2,1,0:T(8,128)(2,1)S(1)}, u32[]{:S(2)}, u32[]{:S(2)}) async-start(bf16[64,32,128]{2,1,0:T(8,128)(2,1)} %shard_map.165), calls=%async_computation.2 | async-start | bytes 1048576 | tf_op jit(solution)/shard_map/all_to_all | solution.py:394
  142.4 9.0 %collective-permute-start.14 = (bf16[320,128]{1,0:T(8,128)(2,1)S(1)}, bf16[320,128]{1,0:T(8,128)(2,1)S(1)}, u32[]{:S(2)}, u32[]{:S(2)}) collective-permute-start(bf16[320,128]{1,0:T(8,128)(2,1)S(1)} %get-tuple-element.53), channel_id=1, source_target_pairs={{0,2},{1,3},{2,4},{3,5},{4,6},{5,7},{6,0},{7,1},{8,10},{9,11},{10,... | collective-permute-start | bytes 245768 | tf_op jit(solution)/shard_map/ppermute | solution.py:319
  145.7 5.7 %collective-permute-start.15 = (bf16[320,128]{1,0:T(8,128)(2,1)S(1)}, bf16[320,128]{1,0:T(8,128)(2,1)S(1)}, u32[]{:S(2)}, u32[]{:S(2)}) collective-permute-start(bf16[320,128]{1,0:T(8,128)(2,1)S(1)} %get-tuple-element.54), channel_id=1, source_target_pairs={{0,6},{1,7},{2,0},{3,1},{4,2},{5,3},{6,4},{7,5},{8,14},{9,15},{10,... | collective-permute-start | bytes 245768 | tf_op jit(solution)/shard_map/ppermute | solution.py:319
  148.9 7.0 %collective-permute-start.16 = (bf16[320,128]{1,0:T(8,128)(2,1)S(1)}, bf16[320,128]{1,0:T(8,128)(2,1)S(1)}, u32[]{:S(2)}, u32[]{:S(2)}) collective-permute-start(bf16[320,128]{1,0:T(8,128)(2,1)S(1)} %get-tuple-element.55), channel_id=1, source_target_pairs={{0,4},{1,5},{2,6},{3,7},{4,0},{5,1},{6,2},{7,3},{8,12},{9,13},{10,... | collective-permute-start | bytes 245768 | tf_op jit(solution)/shard_map/ppermute | solution.py:319
  155.9 8.3 %collective-permute-start.17 = (bf16[4,192,128]{2,1,0:T(8,128)(2,1)S(1)}, bf16[4,192,128]{2,1,0:T(8,128)(2,1)S(1)}, u32[]{:S(2)}, u32[]{:S(2)}) collective-permute-start(bf16[4,192,128]{2,1,0:T(8,128)(2,1)S(1)} %shard_map.168), channel_id=1, source_target_pairs={{0,1},{1,0},{2,3},{3,2},{4,5},{5,4},{6,7},{7,6},{8,9},{9,8},{10,11... | collective-permute-start | bytes 589832 | tf_op jit(solution)/shard_map/ppermute | solution.py:323
  (5 other events, 62.6 us)

commit v5 on v4

--- a/solution.py
+++ b/solution.py
@@ -101,13 +101,12 @@
     send_ref[:, 16:32, :] = rows[:, LANES:].reshape(E, CAP, LANES)
 
 
-def own_rows_body(got_ref, own_ref, part_ref):
+def own_rows_body(got_ref, own_ref):
     own_ref[...] = got_ref[:, 0:32, :]
-    part_ref[...] = got_ref[:, 32:40, :]
-
-
-def spread_body(part_ref, parts_ref):
-    parts = part_ref[...]
+
+
+def spread_body(got_ref, parts_ref):
+    parts = got_ref[:, 32:40, :]
     for y in range(PARTS):
         parts_ref[y] = parts
 
@@ -364,8 +363,8 @@
     )
     weights = lax.all_to_all(spread, "fs", 0, 0, tiled=True)
 
-    own, part = call(own_rows_body, (shape(64, 32, LANES), shape(64, 8, LANES)), 1, keep=(0,))(got)
-    common_send = call(spread_body, shape(8, 64, 8, LANES), 1, far=(0,), keep=())(part)
+    own = call(own_rows_body, shape(64, 32, LANES), 1)(got)
+    common_send = call(spread_body, shape(8, 64, 8, LANES), 1, keep=())(got)
     left = shift(own, 2)
     right = shift(own, -2)
     far_a = shift(call(part_body(0), shape(32, 32, LANES), 1)(left), 2)

time: 167 us -> 165 us (0.988)
  transfers between devices with their start and end apart: 22 -> 22, of which waited for: 12 -> 12; matrix products, arithmetic and copies ran while one was open for 0% -> 0% of each run, Pallas kernels for 10% -> 9%
where the time goes in v5:
time: 165 us; the launch traced here: 164 us
  starting transfers between devices  109 us (66%)
  waiting for transfers between devices  35.9 us (22%)
  Pallas kernels  18.2 us (11%)
    ppermute x13, starting transfers between devices, shift(): return lax.ppermute(x, 'tp', [(i, (i + step) % N_TP) for i in range(N_TP)])  42.2 us
    ppermute x13, waiting for transfers between devices, shift(): return lax.ppermute(x, 'tp', [(i, (i + step) % N_TP) for i in range(N_TP)])  31.3 us
    ppermute x5, starting transfers between devices, swap(): return lax.ppermute(x, 'tp', [(i, i ^ k) for i in range(N_TP)])  18.6 us
    pallas_call x20, Pallas kernels, run(): return fn(*placed)  18.2 us
    all_to_all x1, starting transfers between devices, local(): got = lax.all_to_all(send, 'fs', 0, 0, tiled=True)  17.1 us
    all_to_all x1, starting transfers between devices, local(): returned = lax.all_to_all(expert_out, 'fs', 0, 0, tiled=True)  12.6 us
    all_to_all x1, starting transfers between devices, local(): weights = lax.all_to_all(spread, 'fs', 0, 0, tiled=True)  12.4 us
    all_to_all x1, starting transfers between devices, local(): lax.all_to_all(common_send, 'fs', 0, 0, axis_index_groups=COLUMNS, tiled=...  6.2 us
  transfers between devices with their start and end apart: 22, of which 12 were waited for; matrix products, arithmetic and copies ran while one was open for 0% of the time, Pallas kernels for 9%

profile of v5, /device:TPU:1, one launch (start us, length us, event | category | flops | bytes accessed | tf_op | source)
XLA Modules:
  0.0 164.1 jit_solution(16168582752831346088)
XLA Ops:
  3.2 17.1 %all-to-all-start = ((bf16[64,40,128]{2,1,0:T(8,128)(2,1)}), bf16[64,40,128]{2,1,0:T(8,128)(2,1)S(1)}, u32[]{:S(2)}, u32[]{:S(2)}) async-start(bf16[64,40,128]{2,1,0:T(8,128)(2,1)} %get-tuple-element.36), calls=%async_computation | async-start | bytes 1310720 | tf_op jit(solution)/shard_map/all_to_all | solution.py:349
  26.1 3.1 %collective-permute-start.7 = (bf16[16,48,128]{2,1,0:T(8,128)(2,1)S(1)}, bf16[16,48,128]{2,1,0:T(8,128)(2,1)S(1)}, u32[]{:S(2)}, u32[]{:S(2)}) collective-permute-start(bf16[16,48,128]{2,1,0:T(8,128)(2,1)S(1)} %get-tuple-element.40), channel_id=1, source_target_pairs={{0,2},{1,3},{2,4},{3,5},{4,6},{5,7},{6,0},{7,1},{8,10},{9,11},{10,... | collective-permute-start | bytes 589832 | tf_op jit(solution)/shard_map/ppermute | solution.py:318
  29.2 3.4 %collective-permute-start.8 = (bf16[16,48,128]{2,1,0:T(8,128)(2,1)S(1)}, bf16[16,48,128]{2,1,0:T(8,128)(2,1)S(1)}, u32[]{:S(2)}, u32[]{:S(2)}) collective-permute-start(bf16[16,48,128]{2,1,0:T(8,128)(2,1)S(1)} %get-tuple-element.41), channel_id=1, source_target_pairs={{0,6},{1,7},{2,0},{3,1},{4,2},{5,3},{6,4},{7,5},{8,14},{9,15},{10,... | collective-permute-start | bytes 589832 | tf_op jit(solution)/shard_map/ppermute | solution.py:318
  32.6 3.4 %collective-permute-start.9 = (bf16[16,48,128]{2,1,0:T(8,128)(2,1)S(1)}, bf16[16,48,128]{2,1,0:T(8,128)(2,1)S(1)}, u32[]{:S(2)}, u32[]{:S(2)}) collective-permute-start(bf16[16,48,128]{2,1,0:T(8,128)(2,1)S(1)} %get-tuple-element.42), channel_id=1, source_target_pairs={{0,4},{1,5},{2,6},{3,7},{4,0},{5,1},{6,2},{7,3},{8,12},{9,13},{10,... | collective-permute-start | bytes 589832 | tf_op jit(solution)/shard_map/ppermute | solution.py:318
  36.9 4.6 %collective-permute-done.9.far_ref = bf16[16,48,128]{2,1,0:T(8,128)(2,1)S(1)} collective-permute-done((bf16[16,48,128]{2,1,0:T(8,128)(2,1)S(1)}, bf16[16,48,128]{2,1,0:T(8,128)(2,1)S(1)}, u32[]{:S(2)}, u32[]{:S(2)}) %collective-permute-start.9) | collective-permute-done | bytes 196640 | tf_op jit(solution)/shard_map/ppermute | solution.py:318
  42.5 12.4 %all-to-all-start.1 = ((bf16[64,48,128]{2,1,0:T(8,128)(2,1)}), bf16[64,48,128]{2,1,0:T(8,128)(2,1)S(1)}, u32[]{:S(2)}, u32[]{:S(2)}) async-start(bf16[64,48,128]{2,1,0:T(8,128)(2,1)} %shard_map.162), calls=%async_computation.1 | async-start | bytes 1572864 | tf_op jit(solution)/shard_map/all_to_all | solution.py:364
  55.0 3.4 %collective-permute-start = (bf16[64,32,128]{2,1,0:T(8,128)(2,1)S(1)}, bf16[64,32,128]{2,1,0:T(8,128)(2,1)S(1)}, u32[]{:S(2)}, u32[]{:S(2)}) collective-permute-start(bf16[64,32,128]{2,1,0:T(8,128)(2,1)S(1)} %shard_map.155.refs_0_.own_ref), channel_id=1, source_target_pairs={{0,2},{1,3},{2,4},{3,5},{4,6},{5,7},{6,0},{7,1},{8,10},{9,11},{10,... | collective-permute-start | bytes 1572872 | tf_op jit(solution)/shard_map/ppermute | solution.py:318
  58.3 3.1 %collective-permute-start.1 = (bf16[64,32,128]{2,1,0:T(8,128)(2,1)S(1)}, bf16[64,32,128]{2,1,0:T(8,128)(2,1)S(1)}, u32[]{:S(2)}, u32[]{:S(2)}) collective-permute-start(bf16[64,32,128]{2,1,0:T(8,128)(2,1)S(1)} %shard_map.155.refs_0_.own_ref), channel_id=1, source_target_pairs={{0,6},{1,7},{2,0},{3,1},{4,2},{5,3},{6,4},{7,5},{8,14},{9,15},{10,... | collective-permute-start | bytes 1572872 | tf_op jit(solution)/shard_map/ppermute | solution.py:318
  61.5 8.0 %collective-permute-done.in_ref.refs_1_.left_ref = bf16[64,32,128]{2,1,0:T(8,128)(2,1)S(1)} collective-permute-done((bf16[64,32,128]{2,1,0:T(8,128)(2,1)S(1)}, bf16[64,32,128]{2,1,0:T(8,128)(2,1)S(1)}, u32[]{:S(2)}, u32[]{:S(2)}) %collective-permute-start) | collective-permute-done | bytes 524320 | tf_op jit(solution)/shard_map/ppermute | solution.py:318
  72.9 4.8 %collective-permute-start.4 = (bf16[192,32,128]{2,1,0:T(8,128)(2,1)}, bf16[192,32,128]{2,1,0:T(8,128)(2,1)}, u32[]{:S(2)}, u32[]{:S(2)}) collective-permute-start(bf16[192,32,128]{2,1,0:T(8,128)(2,1)} %shard_map.159), channel_id=1, source_target_pairs={{0,1},{1,0},{2,3},{3,2},{4,5},{5,4},{6,7},{7,6},{8,9},{9,8},{10,11... | collective-permute-start | bytes 4718600 | tf_op jit(solution)/shard_map/ppermute | solution.py:322
  78.9 6.2 %all-to-all-start.3 = ((bf16[8,64,8,128]{3,2,1,0:T(8,128)(2,1)}), bf16[8,64,8,128]{3,2,1,0:T(8,128)(2,1)S(1)}, u32[]{:S(2)}, u32[]{:S(2)}) async-start(bf16[8,64,8,128]{3,2,1,0:T(8,128)(2,1)} %shard_map.166), calls=%async_computation.3 | async-start | bytes 2097152 | tf_op jit(solution)/shard_map/all_to_all | solution.py:377
  87.2 4.4 %collective-permute-start.3 = (bf16[32,32,128]{2,1,0:T(8,128)(2,1)S(1)}, bf16[32,32,128]{2,1,0:T(8,128)(2,1)S(1)}, u32[]{:S(2)}, u32[]{:S(2)}) collective-permute-start(bf16[32,32,128]{2,1,0:T(8,128)(2,1)S(1)} %shard_map.157), channel_id=1, source_target_pairs={{0,6},{1,7},{2,0},{3,1},{4,2},{5,3},{6,4},{7,5},{8,14},{9,15},{10,... | collective-permute-start | bytes 786440 | tf_op jit(solution)/shard_map/ppermute | solution.py:318
  91.6 4.1 %collective-permute-done.2.refs_0_ = bf16[32,32,128]{2,1,0:T(8,128)(2,1)S(1)} collective-permute-done((bf16[32,32,128]{2,1,0:T(8,128)(2,1)S(1)}, bf16[32,32,128]{2,1,0:T(8,128)(2,1)S(1)}, u32[]{:S(2)}, u32[]{:S(2)}) %collective-permute-start.2) | collective-permute-done | bytes 262176 | tf_op jit(solution)/shard_map/ppermute | solution.py:318
  96.7 3.3 %collective-permute-start.5 = (bf16[64,32,128]{2,1,0:T(8,128)(2,1)S(1)}, bf16[64,32,128]{2,1,0:T(8,128)(2,1)S(1)}, u32[]{:S(2)}, u32[]{:S(2)}) collective-permute-start(bf16[64,32,128]{2,1,0:T(8,128)(2,1)S(1)} %shard_map.158.across_ref), channel_id=1, source_target_pairs={{0,1},{1,0},{2,3},{3,2},{4,5},{5,4},{6,7},{7,6},{8,9},{9,8},{10,11... | collective-permute-start | bytes 1572872 | tf_op jit(solution)/shard_map/ppermute | solution.py:322
  104.5 3.3 %collective-permute-start.10 = (bf16[768,128]{1,0:T(8,128)(2,1)S(1)}, bf16[768,128]{1,0:T(8,128)(2,1)S(1)}, u32[]{:S(2)}, u32[]{:S(2)}) collective-permute-start(bf16[768,128]{1,0:T(8,128)(2,1)S(1)} %get-tuple-element.44), channel_id=1, source_target_pairs={{0,2},{1,3},{2,4},{3,5},{4,6},{5,7},{6,0},{7,1},{8,10},{9,11},{10,... | collective-permute-start | bytes 589832 | tf_op jit(solution)/shard_map/ppermute | solution.py:318
  107.8 4.0 %collective-permute-start.11 = (bf16[768,128]{1,0:T(8,128)(2,1)S(1)}, bf16[768,128]{1,0:T(8,128)(2,1)S(1)}, u32[]{:S(2)}, u32[]{:S(2)}) collective-permute-start(bf16[768,128]{1,0:T(8,128)(2,1)S(1)} %get-tuple-element.45), channel_id=1, source_target_pairs={{0,6},{1,7},{2,0},{3,1},{4,2},{5,3},{6,4},{7,5},{8,14},{9,15},{10,... | collective-permute-start | bytes 589832 | tf_op jit(solution)/shard_map/ppermute | solution.py:318
  111.8 3.1 %collective-permute-start.12 = (bf16[768,128]{1,0:T(8,128)(2,1)S(1)}, bf16[768,128]{1,0:T(8,128)(2,1)S(1)}, u32[]{:S(2)}, u32[]{:S(2)}) collective-permute-start(bf16[768,128]{1,0:T(8,128)(2,1)S(1)} %get-tuple-element.46), channel_id=1, source_target_pairs={{0,4},{1,5},{2,6},{3,7},{4,0},{5,1},{6,2},{7,3},{8,12},{9,13},{10,... | collective-permute-start | bytes 589832 | tf_op jit(solution)/shard_map/ppermute | solution.py:318
  115.6 5.3 %collective-permute-done.12.refs_3_.far_ref = bf16[768,128]{1,0:T(8,128)(2,1)S(1)} collective-permute-done((bf16[768,128]{1,0:T(8,128)(2,1)S(1)}, bf16[768,128]{1,0:T(8,128)(2,1)S(1)}, u32[]{:S(2)}, u32[]{:S(2)}) %collective-permute-start.12) | collective-permute-done | bytes 196640 | tf_op jit(solution)/shard_map/ppermute | solution.py:318
  121.0 3.6 %collective-permute-start.13 = (bf16[4,640,128]{2,1,0:T(8,128)(2,1)S(1)}, bf16[4,640,128]{2,1,0:T(8,128)(2,1)S(1)}, u32[]{:S(2)}, u32[]{:S(2)}) collective-permute-start(bf16[4,640,128]{2,1,0:T(8,128)(2,1)S(1)} %shard_map.164), channel_id=1, source_target_pairs={{0,1},{1,0},{2,3},{3,2},{4,5},{5,4},{6,7},{7,6},{8,9},{9,8},{10,11... | collective-permute-start | bytes 1966088 | tf_op jit(solution)/shard_map/ppermute | solution.py:322
  127.8 12.6 %all-to-all-start.2 = ((bf16[64,32,128]{2,1,0:T(8,128)(2,1)}), bf16[64,32,128]{2,1,0:T(8,128)(2,1)S(1)}, u32[]{:S(2)}, u32[]{:S(2)}) async-start(bf16[64,32,128]{2,1,0:T(8,128)(2,1)} %shard_map.165), calls=%async_computation.2 | async-start | bytes 1048576 | tf_op jit(solution)/shard_map/all_to_all | solution.py:393
  140.8 3.3 %collective-permute-start.14 = (bf16[320,128]{1,0:T(8,128)(2,1)S(1)}, bf16[320,128]{1,0:T(8,128)(2,1)S(1)}, u32[]{:S(2)}, u32[]{:S(2)}) collective-permute-start(bf16[320,128]{1,0:T(8,128)(2,1)S(1)} %get-tuple-element.49), channel_id=1, source_target_pairs={{0,2},{1,3},{2,4},{3,5},{4,6},{5,7},{6,0},{7,1},{8,10},{9,11},{10,... | collective-permute-start | bytes 245768 | tf_op jit(solution)/shard_map/ppermute | solution.py:318
  144.1 3.2 %collective-permute-start.15 = (bf16[320,128]{1,0:T(8,128)(2,1)S(1)}, bf16[320,128]{1,0:T(8,128)(2,1)S(1)}, u32[]{:S(2)}, u32[]{:S(2)}) collective-permute-start(bf16[320,128]{1,0:T(8,128)(2,1)S(1)} %get-tuple-element.50), channel_id=1, source_target_pairs={{0,6},{1,7},{2,0},{3,1},{4,2},{5,3},{6,4},{7,5},{8,14},{9,15},{10,... | collective-permute-start | bytes 245768 | tf_op jit(solution)/shard_map/ppermute | solution.py:318
  149.8 4.5 %collective-permute-done.16.refs_3_.far_ref = bf16[320,128]{1,0:T(8,128)(2,1)S(1)} collective-permute-done((bf16[320,128]{1,0:T(8,128)(2,1)S(1)}, bf16[320,128]{1,0:T(8,128)(2,1)S(1)}, u32[]{:S(2)}, u32[]{:S(2)}) %collective-permute-start.16) | collective-permute-done | bytes 81952 | tf_op jit(solution)/shard_map/ppermute | solution.py:318
  154.4 4.0 %collective-permute-start.17 = (bf16[4,192,128]{2,1,0:T(8,128)(2,1)S(1)}, bf16[4,192,128]{2,1,0:T(8,128)(2,1)S(1)}, u32[]{:S(2)}, u32[]{:S(2)}) collective-permute-start(bf16[4,192,128]{2,1,0:T(8,128)(2,1)S(1)} %shard_map.168), channel_id=1, source_target_pairs={{0,1},{1,0},{2,3},{3,2},{4,5},{5,4},{6,7},{7,6},{8,9},{9,8},{10,11... | collective-permute-start | bytes 589832 | tf_op jit(solution)/shard_map/ppermute | solution.py:322
  (54 shorter events, 34.8 us)
Async XLA Ops:
  0.6 19.8 %copy-start.2 = (f32[32,4096]{1,0:T(8,128)S(1)}, f32[32,4096]{1,0:T(8,128)}, u32[]{:S(2)}) copy-start(f32[32,4096]{1,0:T(8,128)} %g_ref.1) | copy-start | bytes 1572868
  0.6 19.8 %copy-start.3 = (f32[32,4096]{1,0:T(8,128)S(1)}, f32[32,4096]{1,0:T(8,128)}, u32[]{:S(2)}) copy-start(f32[32,4096]{1,0:T(8,128)} %u_ref.1) | copy-start | bytes 1572868
  3.2 39.2 %all-to-all-start = ((bf16[64,40,128]{2,1,0:T(8,128)(2,1)}), bf16[64,40,128]{2,1,0:T(8,128)(2,1)S(1)}, u32[]{:S(2)}, u32[]{:S(2)}) async-start(bf16[64,40,128]{2,1,0:T(8,128)(2,1)} %get-tuple-element.36), calls=%async_computation | async-start | bytes 1310720 | tf_op jit(solution)/shard_map/all_to_all | solution.py:349
  21.8 4.2 %collective-permute-start.6 = (bf16[4,8,48,128]{3,2,1,0:T(8,128)(2,1)S(1)}, bf16[4,8,48,128]{3,2,1,0:T(8,128)(2,1)S(1)}, u32[]{:S(2)}, u32[]{:S(2)}) collective-permute-start(bf16[4,8,48,128]{3,2,1,0:T(8,128)(2,1)S(1)} %get-tuple-element.38), channel_id=1, source_target_pairs={{0,1},{1,0},{2,3},{3,2},{4,5},{5,4},{6,7},{7,6},{8,9},{9,8},{10,11... | collective-permute-start | bytes 1179656 | tf_op jit(solution)/shard_map/ppermute | solution.py:322
  26.1 9.9 %collective-permute-start.7 = (bf16[16,48,128]{2,1,0:T(8,128)(2,1)S(1)}, bf16[16,48,128]{2,1,0:T(8,128)(2,1)S(1)}, u32[]{:S(2)}, u32[]{:S(2)}) collective-permute-start(bf16[16,48,128]{2,1,0:T(8,128)(2,1)S(1)} %get-tuple-element.40), channel_id=1, source_target_pairs={{0,2},{1,3},{2,4},{3,5},{4,6},{5,7},{6,0},{7,1},{8,10},{9,11},{10,... | collective-permute-start | bytes 589832 | tf_op jit(solution)/shard_map/ppermute | solution.py:318
  29.2 7.7 %collective-permute-start.8 = (bf16[16,48,128]{2,1,0:T(8,128)(2,1)S(1)}, bf16[16,48,128]{2,1,0:T(8,128)(2,1)S(1)}, u32[]{:S(2)}, u32[]{:S(2)}) collective-permute-start(bf16[16,48,128]{2,1,0:T(8,128)(2,1)S(1)} %get-tuple-element.41), channel_id=1, source_target_pairs={{0,6},{1,7},{2,0},{3,1},{4,2},{5,3},{6,4},{7,5},{8,14},{9,15},{10,... | collective-permute-start | bytes 589832 | tf_op jit(solution)/shard_map/ppermute | solution.py:318
  32.6 8.9 %collective-permute-start.9 = (bf16[16,48,128]{2,1,0:T(8,128)(2,1)S(1)}, bf16[16,48,128]{2,1,0:T(8,128)(2,1)S(1)}, u32[]{:S(2)}, u32[]{:S(2)}) collective-permute-start(bf16[16,48,128]{2,1,0:T(8,128)(2,1)S(1)} %get-tuple-element.42), channel_id=1, source_target_pairs={{0,4},{1,5},{2,6},{3,7},{4,0},{5,1},{6,2},{7,3},{8,12},{9,13},{10,... | collective-permute-start | bytes 589832 | tf_op jit(solution)/shard_map/ppermute | solution.py:318
  42.5 36.4 %all-to-all-start.1 = ((bf16[64,48,128]{2,1,0:T(8,128)(2,1)}), bf16[64,48,128]{2,1,0:T(8,128)(2,1)S(1)}, u32[]{:S(2)}, u32[]{:S(2)}) async-start(bf16[64,48,128]{2,1,0:T(8,128)(2,1)} %shard_map.162), calls=%async_computation.1 | async-start | bytes 1572864 | tf_op jit(solution)/shard_map/all_to_all | solution.py:364
  55.0 14.5 %collective-permute-start = (bf16[64,32,128]{2,1,0:T(8,128)(2,1)S(1)}, bf16[64,32,128]{2,1,0:T(8,128)(2,1)S(1)}, u32[]{:S(2)}, u32[]{:S(2)}) collective-permute-start(bf16[64,32,128]{2,1,0:T(8,128)(2,1)S(1)} %shard_map.155.refs_0_.own_ref), channel_id=1, source_target_pairs={{0,2},{1,3},{2,4},{3,5},{4,6},{5,7},{6,0},{7,1},{8,10},{9,11},{10,... | collective-permute-start | bytes 1572872 | tf_op jit(solution)/shard_map/ppermute | solution.py:318
  58.3 13.3 %collective-permute-start.1 = (bf16[64,32,128]{2,1,0:T(8,128)(2,1)S(1)}, bf16[64,32,128]{2,1,0:T(8,128)(2,1)S(1)}, u32[]{:S(2)}, u32[]{:S(2)}) collective-permute-start(bf16[64,32,128]{2,1,0:T(8,128)(2,1)S(1)} %shard_map.155.refs_0_.own_ref), channel_id=1, source_target_pairs={{0,6},{1,7},{2,0},{3,1},{4,2},{5,3},{6,4},{7,5},{8,14},{9,15},{10,... | collective-permute-start | bytes 1572872 | tf_op jit(solution)/shard_map/ppermute | solution.py:318
  72.9 28.7 %collective-permute-start.4 = (bf16[192,32,128]{2,1,0:T(8,128)(2,1)}, bf16[192,32,128]{2,1,0:T(8,128)(2,1)}, u32[]{:S(2)}, u32[]{:S(2)}) collective-permute-start(bf16[192,32,128]{2,1,0:T(8,128)(2,1)} %shard_map.159), channel_id=1, source_target_pairs={{0,1},{1,0},{2,3},{3,2},{4,5},{5,4},{6,7},{7,6},{8,9},{9,8},{10,11... | collective-permute-start | bytes 4718600 | tf_op jit(solution)/shard_map/ppermute | solution.py:322
  78.9 48.9 %all-to-all-start.3 = ((bf16[8,64,8,128]{3,2,1,0:T(8,128)(2,1)}), bf16[8,64,8,128]{3,2,1,0:T(8,128)(2,1)S(1)}, u32[]{:S(2)}, u32[]{:S(2)}) async-start(bf16[8,64,8,128]{3,2,1,0:T(8,128)(2,1)} %shard_map.166), calls=%async_computation.3 | async-start | bytes 2097152 | tf_op jit(solution)/shard_map/all_to_all | solution.py:377
  85.1 10.7 %collective-permute-start.2 = (bf16[32,32,128]{2,1,0:T(8,128)(2,1)S(1)}, bf16[32,32,128]{2,1,0:T(8,128)(2,1)S(1)}, u32[]{:S(2)}, u32[]{:S(2)}) collective-permute-start(bf16[32,32,128]{2,1,0:T(8,128)(2,1)S(1)} %shard_map.156), channel_id=1, source_target_pairs={{0,2},{1,3},{2,4},{3,5},{4,6},{5,7},{6,0},{7,1},{8,10},{9,11},{10,... | collective-permute-start | bytes 786440 | tf_op jit(solution)/shard_map/ppermute | solution.py:318
  87.2 9.5 %collective-permute-start.3 = (bf16[32,32,128]{2,1,0:T(8,128)(2,1)S(1)}, bf16[32,32,128]{2,1,0:T(8,128)(2,1)S(1)}, u32[]{:S(2)}, u32[]{:S(2)}) collective-permute-start(bf16[32,32,128]{2,1,0:T(8,128)(2,1)S(1)} %shard_map.157), channel_id=1, source_target_pairs={{0,6},{1,7},{2,0},{3,1},{4,2},{5,3},{6,4},{7,5},{8,14},{9,15},{10,... | collective-permute-start | bytes 786440 | tf_op jit(solution)/shard_map/ppermute | solution.py:318
  96.7 4.9 %collective-permute-start.5 = (bf16[64,32,128]{2,1,0:T(8,128)(2,1)S(1)}, bf16[64,32,128]{2,1,0:T(8,128)(2,1)S(1)}, u32[]{:S(2)}, u32[]{:S(2)}) collective-permute-start(bf16[64,32,128]{2,1,0:T(8,128)(2,1)S(1)} %shard_map.158.across_ref), channel_id=1, source_target_pairs={{0,1},{1,0},{2,3},{3,2},{4,5},{5,4},{6,7},{7,6},{8,9},{9,8},{10,11... | collective-permute-start | bytes 1572872 | tf_op jit(solution)/shard_map/ppermute | solution.py:322
  104.5 10.4 %collective-permute-start.10 = (bf16[768,128]{1,0:T(8,128)(2,1)S(1)}, bf16[768,128]{1,0:T(8,128)(2,1)S(1)}, u32[]{:S(2)}, u32[]{:S(2)}) collective-permute-start(bf16[768,128]{1,0:T(8,128)(2,1)S(1)} %get-tuple-element.44), channel_id=1, source_target_pairs={{0,2},{1,3},{2,4},{3,5},{4,6},{5,7},{6,0},{7,1},{8,10},{9,11},{10,... | collective-permute-start | bytes 589832 | tf_op jit(solution)/shard_map/ppermute | solution.py:318
  107.8 7.8 %collective-permute-start.11 = (bf16[768,128]{1,0:T(8,128)(2,1)S(1)}, bf16[768,128]{1,0:T(8,128)(2,1)S(1)}, u32[]{:S(2)}, u32[]{:S(2)}) collective-permute-start(bf16[768,128]{1,0:T(8,128)(2,1)S(1)} %get-tuple-element.45), channel_id=1, source_target_pairs={{0,6},{1,7},{2,0},{3,1},{4,2},{5,3},{6,4},{7,5},{8,14},{9,15},{10,... | collective-permute-start | bytes 589832 | tf_op jit(solution)/shard_map/ppermute | solution.py:318
  111.8 9.2 %collective-permute-start.12 = (bf16[768,128]{1,0:T(8,128)(2,1)S(1)}, bf16[768,128]{1,0:T(8,128)(2,1)S(1)}, u32[]{:S(2)}, u32[]{:S(2)}) collective-permute-start(bf16[768,128]{1,0:T(8,128)(2,1)S(1)} %get-tuple-element.46), channel_id=1, source_target_pairs={{0,4},{1,5},{2,6},{3,7},{4,0},{5,1},{6,2},{7,3},{8,12},{9,13},{10,... | collective-permute-start | bytes 589832 | tf_op jit(solution)/shard_map/ppermute | solution.py:318
  121.0 5.3 %collective-permute-start.13 = (bf16[4,640,128]{2,1,0:T(8,128)(2,1)S(1)}, bf16[4,640,128]{2,1,0:T(8,128)(2,1)S(1)}, u32[]{:S(2)}, u32[]{:S(2)}) collective-permute-start(bf16[4,640,128]{2,1,0:T(8,128)(2,1)S(1)} %shard_map.164), channel_id=1, source_target_pairs={{0,1},{1,0},{2,3},{3,2},{4,5},{5,4},{6,7},{7,6},{8,9},{9,8},{10,11... | collective-permute-start | bytes 1966088 | tf_op jit(solution)/shard_map/ppermute | solution.py:322
  127.8 35.3 %all-to-all-start.2 = ((bf16[64,32,128]{2,1,0:T(8,128)(2,1)}), bf16[64,32,128]{2,1,0:T(8,128)(2,1)S(1)}, u32[]{:S(2)}, u32[]{:S(2)}) async-start(bf16[64,32,128]{2,1,0:T(8,128)(2,1)} %shard_map.165), calls=%async_computation.2 | async-start | bytes 1048576 | tf_op jit(solution)/shard_map/all_to_all | solution.py:393
  140.8 9.0 %collective-permute-start.14 = (bf16[320,128]{1,0:T(8,128)(2,1)S(1)}, bf16[320,128]{1,0:T(8,128)(2,1)S(1)}, u32[]{:S(2)}, u32[]{:S(2)}) collective-permute-start(bf16[320,128]{1,0:T(8,128)(2,1)S(1)} %get-tuple-element.49), channel_id=1, source_target_pairs={{0,2},{1,3},{2,4},{3,5},{4,6},{5,7},{6,0},{7,1},{8,10},{9,11},{10,... | collective-permute-start | bytes 245768 | tf_op jit(solution)/shard_map/ppermute | solution.py:318
  144.1 5.7 %collective-permute-start.15 = (bf16[320,128]{1,0:T(8,128)(2,1)S(1)}, bf16[320,128]{1,0:T(8,128)(2,1)S(1)}, u32[]{:S(2)}, u32[]{:S(2)}) collective-permute-start(bf16[320,128]{1,0:T(8,128)(2,1)S(1)} %get-tuple-element.50), channel_id=1, source_target_pairs={{0,6},{1,7},{2,0},{3,1},{4,2},{5,3},{6,4},{7,5},{8,14},{9,15},{10,... | collective-permute-start | bytes 245768 | tf_op jit(solution)/shard_map/ppermute | solution.py:318
  147.4 7.0 %collective-permute-start.16 = (bf16[320,128]{1,0:T(8,128)(2,1)S(1)}, bf16[320,128]{1,0:T(8,128)(2,1)S(1)}, u32[]{:S(2)}, u32[]{:S(2)}) collective-permute-start(bf16[320,128]{1,0:T(8,128)(2,1)S(1)} %get-tuple-element.51), channel_id=1, source_target_pairs={{0,4},{1,5},{2,6},{3,7},{4,0},{5,1},{6,2},{7,3},{8,12},{9,13},{10,... | collective-permute-start | bytes 245768 | tf_op jit(solution)/shard_map/ppermute | solution.py:318
  154.4 8.3 %collective-permute-start.17 = (bf16[4,192,128]{2,1,0:T(8,128)(2,1)S(1)}, bf16[4,192,128]{2,1,0:T(8,128)(2,1)S(1)}, u32[]{:S(2)}, u32[]{:S(2)}) collective-permute-start(bf16[4,192,128]{2,1,0:T(8,128)(2,1)S(1)} %shard_map.168), channel_id=1, source_target_pairs={{0,1},{1,0},{2,3},{3,2},{4,5},{5,4},{6,7},{7,6},{8,9},{9,8},{10,11... | collective-permute-start | bytes 589832 | tf_op jit(solution)/shard_map/ppermute | solution.py:322
  (5 other events, 62.6 us)
